TPU v7x, 256 devices: a whole 4x4x8 slice. The times are simulated.
256 devices in a mesh: sp: 32 (over z, x), tp: 8 (over y, core).
Axes of the slice: x: 4, y: 4, z: 8, core: 2. Of those that a mesh axis runs over, the one named last changes fastest.
Arguments:
- queries: bfloat16 [24576, 2048], P('sp', 'tp'), may hold values from -110 to 110
- key_rows: bfloat16 [24576, 512], P('sp', 'tp'), may hold values from -4.5 to 4.5
- values: bfloat16 [24576, 512], P('sp', 'tp'), may hold values from -6 to 6
- sink_logits: float32 [32], P('tp'), may hold values from 2 to 7
- doc_ids: int32 [24576], P('sp'), may hold values from 0 to 15, as said below
- residual: bfloat16 [24576, 2048], P('sp'), may hold values from -20 to 20
- w_out: bfloat16 [2048, 2048], P('tp'), may hold values from -2.390625 to 2.390625
- norm_gain: float32 [2048], replicated, may hold values from 0.1 to 1.9
- w_value_up: bfloat16 [2048, 5632], P('sp', 'tp'), may hold values from -0.125 to 0.125
- w_gate_up: bfloat16 [2048, 5632], P('sp', 'tp'), may hold values from -0.125 to 0.125
- conv_taps: bfloat16 [3, 5632], P(None, 'tp'), may hold values from -3.5 to 3.5
- w_down_t: bfloat16 [2048, 5632], P('sp', 'tp'), may hold values from -0.078125 to 0.078125
Outputs:
- layer_out: bfloat16 [24576, 2048], P('sp', 'tp')
Inputs may be any that keep to these rules, and one draw needn't show every extreme that they name: `doc_ids`: document numbers never fall along the sequence and every one of the 16 documents is present; each document has 2 or more positions.
All inputs are finite; a program needn't handle non-finite values.
Results may differ from a plain program's by a relative error of at most 0.017.
Values may be sent and summed in bfloat16 or wider, within the bound.
No kernel may reach another device: no remote copies, remote signals or barrier semaphores. Data moves between devices by JAX's collectives and lax.ppermute only.
A program may use at most 64 MiB of HBM per device.

v0:
```python
import jax
import jax.numpy as jnp
from jax import lax
from jax.experimental import pallas as pl
from jax.experimental.pallas import tpu as pltpu
from jax.sharding import Mesh
from jax.sharding import PartitionSpec as P

HEAD_DIM = 64
WINDOW = 128
EPS = 1e-06
NEG = -1e30

NZ, NX, NY, NC = 8, 4, 4, 2
AXES = ("z", "x", "y", "core")
MB = 1 << 20


def shift_x(k):
    return [(x, (x + k) % NX) for x in range(NX)]


def swap(block):
    return lax.ppermute(block, "core", [(0, 1), (1, 0)])


def after(value, *others):
    return lax.optimization_barrier((value,) + others)[0]


def put(block, piece, *at):
    piece = piece.reshape((1,) * (block.ndim - piece.ndim) + piece.shape)
    start = list(at) + [0] * (block.ndim - len(at))
    return lax.dynamic_update_slice(block, piece, start)


def attention_kernel(
    at_ref, sink_ref, q_ref, kt_ref, vt_ref, lab_ref, low_ref, high_ref, w_ref,
    att_ref, theirs_ref, kx_ref, vx_ref, row_ref, col_ref,
):
    rows = q_ref.shape[0]
    heads = q_ref.shape[1] // HEAD_DIM
    span = theirs_ref.shape[2]
    kx_ref[...] = jnp.zeros_like(kx_ref)
    vx_ref[...] = jnp.zeros_like(vx_ref)
    pieces = (
        (0, WINDOW, low_ref[:HEAD_DIM], low_ref[HEAD_DIM : 2 * HEAD_DIM]),
        (WINDOW, rows, kt_ref[...], vt_ref[...]),
        (WINDOW + rows, WINDOW, high_ref[:HEAD_DIM], high_ref[HEAD_DIM : 2 * HEAD_DIM]),
    )
    for start, width, keys, vals in pieces:
        vals_t = vals.astype(jnp.float32).T.astype(jnp.bfloat16)
        for h in range(heads):
            kx_ref[h, h * HEAD_DIM : (h + 1) * HEAD_DIM, start : start + width] = keys
            vx_ref[h, start : start + width, h * HEAD_DIM : (h + 1) * HEAD_DIM] = vals_t
    row_ref[:, :WINDOW] = jnp.broadcast_to(
        low_ref[2 * HEAD_DIM :].astype(jnp.float32), (8, WINDOW)
    )
    row_ref[:, WINDOW : WINDOW + rows] = jnp.broadcast_to(lab_ref[...], (8, rows))
    row_ref[:, WINDOW + rows :] = jnp.broadcast_to(
        high_ref[2 * HEAD_DIM :].astype(jnp.float32), (8, WINDOW)
    )
    for n in range(rows // WINDOW):
        part = row_ref[:, (n + 1) * WINDOW : (n + 2) * WINDOW]
        col_ref[n * WINDOW : (n + 1) * WINDOW, :] = jnp.broadcast_to(
            part[:1], (WINDOW, WINDOW)
        ).T

    def step(n, carry):
        base = pl.multiple_of(n * WINDOW, WINDOW)
        here = pl.ds(base, WINDOW)
        window = pl.ds(base, 3 * WINDOW)
        q = q_ref[here, :] * jnp.bfloat16(HEAD_DIM ** (-0.5))
        offsets = (
            lax.broadcasted_iota(jnp.int32, (WINDOW, 3 * WINDOW), 1)
            - WINDOW
            - lax.broadcasted_iota(jnp.int32, (WINDOW, 3 * WINDOW), 0)
        )
        mine = col_ref[here, :1]
        allowed = (jnp.abs(offsets) <= WINDOW) & (row_ref[:1, window] == mine)
        acc = None
        for h in range(heads):
            score = jnp.dot(q, kx_ref[h, :, window], preferred_element_type=jnp.float32)
            score = jnp.where(allowed, score, NEG)
            highest = jnp.maximum(jnp.max(score, axis=1, keepdims=True), sink_ref[h])
            raw = jnp.exp(score - highest)
            total = jnp.sum(raw, axis=1, keepdims=True) + jnp.exp(sink_ref[h] - highest)
            probs = (raw * (1.0 / total)).astype(jnp.bfloat16)
            part = jnp.dot(probs, vx_ref[h, window, :], preferred_element_type=jnp.float32)
            acc = part if acc is None else acc + part
        att_ref[here, :] = acc.astype(jnp.bfloat16)
        return carry

    lax.fori_loop(0, rows // WINDOW, step, 0)
    for k in range(NY):
        cols = pl.ds(pl.multiple_of(at_ref[NY + k] * span, span), span)
        theirs_ref[k] = jnp.dot(
            att_ref[...], w_ref[:, cols], preferred_element_type=jnp.float32
        ).astype(jnp.bfloat16)


def vmem_specs(count):
    return [pl.BlockSpec(memory_space=pltpu.VMEM)] * count


def smem_specs(count):
    return [pl.BlockSpec(memory_space=pltpu.SMEM)] * count


def attention(order, sink, queries, keys_t, vals_t, labels, low, high, w_out):
    rows, cols = queries.shape
    span = w_out.shape[1] // (NY * NC)
    reach = rows + 2 * WINDOW
    heads = cols // HEAD_DIM
    return pl.pallas_call(
        attention_kernel,
        out_shape=[
            jax.ShapeDtypeStruct((rows, cols), jnp.bfloat16),
            jax.ShapeDtypeStruct((NY, rows, span), jnp.bfloat16),
        ],
        in_specs=smem_specs(2) + vmem_specs(7),
        out_specs=vmem_specs(2),
        scratch_shapes=[
            pltpu.VMEM((heads, cols, reach), jnp.bfloat16),
            pltpu.VMEM((heads, reach, cols), jnp.bfloat16),
            pltpu.VMEM((8, reach), jnp.float32),
            pltpu.VMEM((rows, WINDOW), jnp.float32),
        ],
        compiler_params=pltpu.CompilerParams(vmem_limit_bytes=12 * MB),
        cost_estimate=pl.CostEstimate(flops=4 * 10**9, bytes_accessed=4 * MB, transcendentals=0),
        name="attention",
    )(order, sink, queries, keys_t, vals_t, labels, low, high, w_out)


def pair_kernel(at_ref, left_ref, w_ref, got_ref, s0, s1, s2, s3):
    span = s0.shape[1]
    for k, out in enumerate((s0, s1, s2, s3)):
        cols = pl.ds(pl.multiple_of(at_ref[k] * span, span), span)
        out[...] = (
            jnp.dot(left_ref[...], w_ref[:, cols], preferred_element_type=jnp.float32)
            + got_ref[k].astype(jnp.float32)
        ).astype(jnp.bfloat16)


def pair_sums(order, left, w_out, got):
    return pl.pallas_call(
        pair_kernel,
        out_shape=[jax.ShapeDtypeStruct(got.shape[1:], jnp.bfloat16)] * NY,
        in_specs=smem_specs(1) + vmem_specs(3),
        out_specs=vmem_specs(NY),
        compiler_params=pltpu.CompilerParams(vmem_limit_bytes=8 * MB),
        cost_estimate=pl.CostEstimate(flops=10**9, bytes_accessed=4 * MB, transcendentals=0),
        name="pair_sums",
    )(order, left, w_out, got)


def to_owners(pairs):
    return [lax.ppermute(pairs[k], "y", [(y, (y + k) % NY) for y in range(NY)]) for k in range(1, NY)]


def per_device(
    queries,
    key_rows,
    values,
    sink_logits,
    doc_ids,
    residual,
    w_out,
    norm_gain,
    w_value_up,
    w_gate_up,
    conv_taps,
    w_down_t,
):
    rows_here = queries.shape[0]
    model_width = residual.shape[1]
    span = model_width // (NY * NC)
    ff = w_value_up.shape[1]
    _, x, y, core = (lax.axis_index(axis) for axis in AXES)
    tp = y * NC + core
    order = jnp.stack(
        [((y + k) % NY) * NC + who for who in (core, 1 - core) for k in range(NY)]
    )
    count = NZ * NX
    forward = [(i, i + 1) for i in range(count - 1)]
    backward = [(target, source) for source, target in forward]

    keys_t, vals_t = key_rows.T, values.T
    labels = (doc_ids + 1).astype(jnp.float32)[None, :]
    packed = jnp.concatenate([keys_t, vals_t, labels.astype(jnp.bfloat16)], axis=0)
    low = lax.ppermute(packed[:, -WINDOW:], ("z", "x"), forward)
    high = lax.ppermute(packed[:, :WINDOW], ("z", "x"), backward)

    share = jnp.concatenate([after(w_value_up, packed), w_gate_up, w_down_t], axis=1)
    rows_w, width = share.shape
    gathered = []
    for k in range(1, NX):
        gathered.append(lax.ppermute(share, "x", shift_x(k)))

    attended, theirs = attention(
        order, sink_logits, queries, keys_t, vals_t, labels, low, high, w_out
    )
    got = swap(theirs)

    block = put(jnp.zeros((NX, rows_w, width), share.dtype), share, x)
    gathered = lax.optimization_barrier((*gathered, theirs))[:-1]
    for k, piece in enumerate(gathered):
        block = put(block, piece, (x - k - 1) % NX)
    full = lax.all_gather(block.reshape(NX * rows_w, width), "z", axis=0, tiled=True)

    pairs = pair_sums(order, attended, w_out, got)
    sent = to_owners(pairs)

    own_res = lax.dynamic_slice_in_dim(residual, tp * span, span, 1)
    total = own_res.astype(jnp.float32)
    summed = pairs[0].astype(jnp.float32)
    for block in sent:
        summed = summed + block.astype(jnp.float32)
    mixed_own = (total + summed).astype(jnp.bfloat16)

    parts = [mixed_own] + to_owners([mixed_own] * NY)
    others = [swap(mixed_own)]
    rest = swap(jnp.stack(parts[1:]))
    others += [rest[k] for k in range(NY - 1)]

    mixed = jnp.zeros((rows_here, model_width), jnp.bfloat16)
    for k in range(NY):
        at = ((y - k) % NY) * NC
        mixed = lax.dynamic_update_slice(mixed, parts[k], (0, (at + core) * span))
        mixed = lax.dynamic_update_slice(mixed, others[k], (0, (at + 1 - core) * span))
    mixed_f = mixed.astype(jnp.float32)
    mean_sq = jnp.mean(mixed_f * mixed_f, axis=1, keepdims=True)
    normed = (mixed_f * lax.rsqrt(mean_sq + EPS) * norm_gain).astype(jnp.bfloat16)

    up_value = jnp.dot(normed, full[:, :ff], preferred_element_type=jnp.float32).astype(
        jnp.bfloat16
    )
    before = lax.ppermute(up_value[-1:], ("z", "x"), forward)
    behind = lax.ppermute(up_value[:1], ("z", "x"), backward)
    up_gate = after(
        jnp.dot(normed, full[:, ff : 2 * ff], preferred_element_type=jnp.float32).astype(
            jnp.bfloat16
        ),
        up_value,
    )
    rim_value = jnp.concatenate([before, up_value, behind], axis=0).astype(jnp.float32)
    edge = jnp.concatenate([low[-1:, -1:], packed[-1:], high[-1:, :1]], axis=1)[0]
    prev_same = (edge[:-2] == edge[1:-1])[:, None]
    next_same = (edge[2:] == edge[1:-1])[:, None]
    tap_f = conv_taps.astype(jnp.float32)
    conv = (
        tap_f[0] * jnp.where(prev_same, rim_value[:-2], 0.0)
        + tap_f[1] * up_value.astype(jnp.float32)
        + tap_f[2] * jnp.where(next_same, rim_value[2:], 0.0)
    )
    hidden = (jax.nn.silu(conv) * up_gate.astype(jnp.float32)).astype(jnp.bfloat16)

    def down(who):
        weights = jnp.concatenate(
            [
                lax.dynamic_slice(
                    full, ((((y + k) % NY) * NC + who) * span, 2 * ff), (span, ff)
                )
                for k in range(NY)
            ],
            axis=0,
        )
        return lax.dot_general(
            hidden, weights, (((1,), (1,)), ((), ())), preferred_element_type=jnp.float32
        )

    got = swap(down(1 - core).astype(jnp.bfloat16))
    pair = (down(core) + got.astype(jnp.float32)).astype(jnp.bfloat16)
    pairs = [pair[:, k * span : (k + 1) * span] for k in range(NY)]
    ffn_cols = pairs[0].astype(jnp.float32)
    for block in to_owners(pairs):
        ffn_cols = ffn_cols + block.astype(jnp.float32)
    return (mixed_own.astype(jnp.float32) + ffn_cols).astype(jnp.bfloat16)


def solution(mesh):
    grid = Mesh(mesh.devices.reshape(NZ, NX, NY, NC), AXES)
    sp, tp = ("z", "x"), ("y", "core")
    placed = (
        P(sp, tp),
        P(sp, tp),
        P(sp, tp),
        P(tp),
        P(sp),
        P(sp, None),
        P(tp, None),
        P(),
        P(sp, tp),
        P(sp, tp),
        P(None, tp),
        P(sp, tp),
    )
    return jax.shard_map(
        per_device, mesh=grid, in_specs=placed, out_specs=P(sp, tp), check_vma=False
    )
```

profile of v0, /device:TPU:2, one launch (start us, length us, event | category | flops | bytes accessed | tf_op | source)
XLA Modules:
  0.0 198.9 jit_solution(1400551656745479857)
XLA Ops:
  7.4 1.0 pad_maximum_fusion.1
  8.4 1.8 concatenate.24
  10.2 1.5 collective-permute-start.11
  11.7 2.8 %collective-permute-start.12 = (bf16[64,2112]{1,0:T(8,128)(2,1)}, bf16[64,2112]{1,0:T(8,128)(2,1)}, u32[]{:S(2)}, u32[]{:S(2)}) collective-permute-start(bf16[64,2112]{1,0:T(8,128)(2,1)} %concatenate.24), channel_id=1, source_target_pairs={{0,16},{8,24},{16,0},{24,8},{1,17},{9,25},{17,1},{25,9},{2,18},{10... | collective-permute-start | bytes 811016 | tf_op jit(solution)/shard_map/ppermute | solution.py:198
  15.0 3.5 %collective-permute-start = (bf16[129,128]{1,0:T(8,128)(2,1)S(1)}, bf16[129,128]{1,0:T(8,128)(2,1)S(1)}, u32[]{:S(2)}, u32[]{:S(2)}) collective-permute-start(bf16[129,128]{1,0:T(8,128)(2,1)S(1)} %get-tuple-element.48), channel_id=1, source_target_pairs={{0,8},{8,16},{16,24},{24,32},{32,40},{40,48},{48,56},{56,64},{64,7... | collective-permute-start | bytes 99080 | tf_op jit(solution)/shard_map/ppermute | solution.py:191
  18.5 2.4 %collective-permute-start.1 = (bf16[129,128]{1,0:T(8,128)(2,1)S(1)}, bf16[129,128]{1,0:T(8,128)(2,1)S(1)}, u32[]{:S(2)}, u32[]{:S(2)}) collective-permute-start(bf16[129,128]{1,0:T(8,128)(2,1)S(1)} %get-tuple-element.47), channel_id=1, source_target_pairs={{8,0},{16,8},{24,16},{32,24},{40,32},{48,40},{56,48},{64,56},{72,6... | collective-permute-start | bytes 99080 | tf_op jit(solution)/shard_map/ppermute | solution.py:192
  20.8 1.1 broadcast_in_dim.34
  21.9 1.7 bitcast_dynamic-update-slice_fusion.3
  23.7 1.9 collective-permute-done.low_ref
  25.6 1.8 collective-permute-done.1.high_ref
  27.4 7.3 %attention.1 = (bf16[768,256]{1,0:T(8,128)(2,1)S(1)}, bf16[4,768,256]{2,1,0:T(8,128)(2,1)S(1)}) custom-call(s32[8]{0:T(128)S(1)} %stack.47.at_ref, f32[4]{0:T(128)S(1)} %copy-done.4, bf16[768,256]{1,0:T(8,128)(2,1)S(1)} %copy-done.3, bf16[64,768]{1,0:T(8,128)(2,1)S(1)} %bitcast.37, bf16[64,768]{1,0:T(8,128)(2,1)S(1)} %bitcast.39, ...), custom_call_target="tpu_custom_call" | custom-call | flops 4000000000 | bytes 4194304 | tf_op jit(solution)/shard_map/attention/pallas_call | solution.py:115
  35.5 1.7 bitcast_dynamic-update-slice_fusion.2
  37.2 1.7 bitcast_dynamic-update-slice_fusion.1
  38.9 1.7 bitcast_dynamic-update-slice_fusion
  40.7 3.4 %collective-permute-done.2.got_ref = bf16[4,768,256]{2,1,0:T(8,128)(2,1)S(1)} collective-permute-done((bf16[4,768,256]{2,1,0:T(8,128)(2,1)S(1)}, bf16[4,768,256]{2,1,0:T(8,128)(2,1)S(1)}, u32[]{:S(2)}, u32[]{:S(2)}) %collective-permute-start.2) | collective-permute-done | bytes 1572896 | tf_op jit(solution)/shard_map/ppermute | solution.py:24
  44.1 1.1 pair_sums.1
  45.2 1.9 collective-permute-start.3
  47.1 2.9 %collective-permute-start.4 = (bf16[768,256]{1,0:T(8,128)(2,1)S(1)}, bf16[768,256]{1,0:T(8,128)(2,1)S(1)}, u32[]{:S(2)}, u32[]{:S(2)}) collective-permute-start(bf16[768,256]{1,0:T(8,128)(2,1)S(1)} %get-tuple-element.20), channel_id=1, source_target_pairs={{0,4},{2,6},{4,0},{6,2},{1,5},{3,7},{5,1},{7,3},{8,12},{10,14},{12... | collective-permute-start | bytes 1179656 | tf_op jit(solution)/shard_map/ppermute | solution.py:158
  50.0 1.3 collective-permute-start.5
  51.3 6.6 %collective-permute-done.3 = bf16[768,256]{1,0:T(8,128)(2,1)S(1)} collective-permute-done((bf16[768,256]{1,0:T(8,128)(2,1)S(1)}, bf16[768,256]{1,0:T(8,128)(2,1)S(1)}, u32[]{:S(2)}, u32[]{:S(2)}) %collective-permute-start.3) | collective-permute-done | bytes 393248 | tf_op jit(solution)/shard_map/ppermute | solution.py:158
  57.9 9.6 %collective-permute-done.4 = bf16[768,256]{1,0:T(8,128)(2,1)S(1)} collective-permute-done((bf16[768,256]{1,0:T(8,128)(2,1)S(1)}, bf16[768,256]{1,0:T(8,128)(2,1)S(1)}, u32[]{:S(2)}, u32[]{:S(2)}) %collective-permute-start.4) | collective-permute-done | bytes 393248 | tf_op jit(solution)/shard_map/ppermute | solution.py:158
  67.5 2.0 %broadcast_in_dim.33 = bf16[768,2048]{1,0:T(8,128)(2,1)} broadcast(bf16[]{:T(256)} %constant.115.clone.1), dimensions={} | broadcast | bytes 3145730 | tf_op jit(solution)/shard_map/broadcast_in_dim | solution.py:226
  69.6 2.1 %constant_dynamic-update-slice_fusion.4 = (bf16[768,2048]{1,0:T(8,128)(2,1)}, bf16[768,256]{1,0:T(8,128)(2,1)S(1)}) fusion(bf16[768,2048]{1,0:T(8,128)(2,1)} %broadcast_in_dim.33, s32[]{:T(128)S(6)} %select_n.142, bf16[768,256]{1,0:T(8,128)(2,1)S(1)} %collective-permute-done.5, bf16[768,256]{1,0:T(8,128)(2,1)S(1)} %collective-permute-done.4, ...), kind=kLoop, calls=%fused_computation.56 | loop fusion | flops 1966080 | bytes 2752520 | tf_op jit(solution)/shard_map/dynamic_update_slice | solution.py:229
  71.7 1.2 collective-permute-start.7
  72.9 2.4 %collective-permute-start.8 = (bf16[768,256]{1,0:T(8,128)(2,1)S(1)}, bf16[768,256]{1,0:T(8,128)(2,1)S(1)}, u32[]{:S(2)}, u32[]{:S(2)}) collective-permute-start(bf16[768,256]{1,0:T(8,128)(2,1)S(1)} %get-tuple-element.33), channel_id=1, source_target_pairs={{0,4},{2,6},{4,0},{6,2},{1,5},{3,7},{5,1},{7,3},{8,12},{10,14},{12... | collective-permute-start | bytes 1179656 | tf_op jit(solution)/shard_map/ppermute | solution.py:158
  75.3 1.5 collective-permute-start.9
  76.8 6.4 %collective-permute-done.7 = bf16[768,256]{1,0:T(8,128)(2,1)S(1)} collective-permute-done((bf16[768,256]{1,0:T(8,128)(2,1)S(1)}, bf16[768,256]{1,0:T(8,128)(2,1)S(1)}, u32[]{:S(2)}, u32[]{:S(2)}) %collective-permute-start.7) | collective-permute-done | bytes 393248 | tf_op jit(solution)/shard_map/ppermute | solution.py:158
  83.2 9.6 %collective-permute-done.8 = bf16[768,256]{1,0:T(8,128)(2,1)S(1)} collective-permute-done((bf16[768,256]{1,0:T(8,128)(2,1)S(1)}, bf16[768,256]{1,0:T(8,128)(2,1)S(1)}, u32[]{:S(2)}, u32[]{:S(2)}) %collective-permute-start.8) | collective-permute-done | bytes 393248 | tf_op jit(solution)/shard_map/ppermute | solution.py:158
  94.8 1.4 fusion.39
  98.1 1.8 fusion.38
  100.8 1.8 fusion.37
  103.4 1.8 fusion.36
  105.2 2.6 %fusion = f32[768]{0:T(1024)S(1)} fusion(bf16[768,2048]{1,0:T(8,128)(2,1)} %fusion.36), kind=kLoop, calls=%fused_computation.2 | loop fusion | flops 4717824 | bytes 3148800 | tf_op jit(solution)/shard_map/reduce_sum | solution.py:232
  107.8 34.9 %all-gather.2.cloned.1.call-done = bf16[2048,2112]{1,0:T(8,128)(2,1)} async-done(((bf16[256,2112]{1,0:T(8,128)(2,1)}), bf16[2048,2112]{1,0:T(8,128)(2,1)}) %all-gather.2.cloned.1.call-update) | async-done | bytes 8650768 | tf_op jit(solution)/shard_map/all_gather | solution.py:209
  142.7 5.6 %fusion.26 = bf16[768,704]{0,1:T(8,128)(2,1)S(1)} fusion(bf16[2048,2112]{1,0:T(8,128)(2,1)} %all-gather.2.cloned.1.call-done, bf16[768,2048]{1,0:T(8,128)(2,1)} %fusion.36, f32[2048]{0:T(1024)S(1)} %copy-done.9, f32[768]{0:T(1024)S(1)} %add_rsqrt_fusion), kind=kOutput, calls=%fused_computation.33 | convolution fusion | flops 2221424640 | bytes 7384064 | tf_op jit(solution)/shard_map/dot_general | solution.py:235
  148.5 3.4 %collective-permute-start.14 = (bf16[1,704]{0,1:T(8,128)(2,1)S(1)}, bf16[1,704]{0,1:T(8,128)(2,1)S(1)}, u32[]{:S(2)}, u32[]{:S(2)}) collective-permute-start(bf16[1,704]{0,1:T(8,128)(2,1)S(1)} %get-tuple-element.45), channel_id=1, source_target_pairs={{0,8},{8,16},{16,24},{24,32},{32,40},{40,48},{48,56},{56,64},{64,7... | collective-permute-start | bytes 4232 | tf_op jit(solution)/shard_map/ppermute | solution.py:238
  151.8 2.5 %collective-permute-start.15 = (bf16[1,704]{0,1:T(8,128)(2,1)S(1)}, bf16[1,704]{0,1:T(8,128)(2,1)S(1)}, u32[]{:S(2)}, u32[]{:S(2)}) collective-permute-start(bf16[1,704]{0,1:T(8,128)(2,1)S(1)} %get-tuple-element.46), channel_id=1, source_target_pairs={{8,0},{16,8},{24,16},{32,24},{40,32},{48,40},{56,48},{64,56},{72,6... | collective-permute-start | bytes 4232 | tf_op jit(solution)/shard_map/ppermute | solution.py:239
  154.3 5.6 %fusion.29 = bf16[768,704]{0,1:T(8,128)(2,1)S(1)} fusion(bf16[2048,2112]{1,0:T(8,128)(2,1)S(1)} %copy-done.7, bf16[768,2048]{1,0:T(8,128)(2,1)} %fusion.36, f32[2048]{0:T(1024)S(1)} %copy-done.9, f32[768]{0:T(1024)S(1)} %add_rsqrt_fusion), kind=kOutput, calls=%fused_computation.34 | convolution fusion | flops 2221424640 | bytes 7385088 | tf_op jit(solution)/shard_map/dot_general | solution.py:241
  160.8 1.7 multiply_convert_fusion
  162.5 1.4 convolution_convert_fusion
  164.3 3.4 %collective-permute-done.16 = bf16[768,1024]{1,0:T(8,128)(2,1)S(1)} collective-permute-done((bf16[768,1024]{1,0:T(8,128)(2,1)S(1)}, bf16[768,1024]{1,0:T(8,128)(2,1)S(1)}, u32[]{:S(2)}, u32[]{:S(2)}) %collective-permute-start.16) | collective-permute-done | bytes 1572896 | tf_op jit(solution)/shard_map/ppermute | solution.py:24
  167.7 1.5 add_convert_fusion
  169.3 1.6 collective-permute-start.17
  170.8 2.7 %collective-permute-start.18 = (bf16[768,256]{1,0:T(8,128)(2,1)S(1)}, bf16[768,256]{1,0:T(8,128)(2,1)S(1)}, u32[]{:S(2)}, u32[]{:S(2)}) collective-permute-start(bf16[768,256]{1,0:T(8,128)(2,1)S(1)} %get-tuple-element.44), channel_id=1, source_target_pairs={{0,4},{2,6},{4,0},{6,2},{1,5},{3,7},{5,1},{7,3},{8,12},{10,14},{12... | collective-permute-start | bytes 1179656 | tf_op jit(solution)/shard_map/ppermute | solution.py:158
  173.5 1.4 collective-permute-start.19
  175.0 6.7 %collective-permute-done.17 = bf16[768,256]{1,0:T(8,128)(2,1)S(1)} collective-permute-done((bf16[768,256]{1,0:T(8,128)(2,1)S(1)}, bf16[768,256]{1,0:T(8,128)(2,1)S(1)}, u32[]{:S(2)}, u32[]{:S(2)}) %collective-permute-start.17) | collective-permute-done | bytes 393248 | tf_op jit(solution)/shard_map/ppermute | solution.py:158
  181.7 9.4 %collective-permute-done.18 = bf16[768,256]{1,0:T(8,128)(2,1)S(1)} collective-permute-done((bf16[768,256]{1,0:T(8,128)(2,1)S(1)}, bf16[768,256]{1,0:T(8,128)(2,1)S(1)}, u32[]{:S(2)}, u32[]{:S(2)}) %collective-permute-start.18) | collective-permute-done | bytes 393248 | tf_op jit(solution)/shard_map/ppermute | solution.py:158
  191.1 1.0 add_convert_fusion.1
  (57 shorter events, 9.1 us)
Async XLA Ops:
  6.5 20.9 %copy-start = (bf16[768,64]{0,1:T(8,128)(2,1)S(1)}, bf16[768,64]{0,1:T(8,128)(2,1)}, u32[]{:S(2)}) copy-start(bf16[768,64]{0,1:T(8,128)(2,1)} %param.13) | copy-start | bytes 294916
  6.5 20.9 %copy-start.1 = (bf16[768,64]{0,1:T(8,128)(2,1)S(1)}, bf16[768,64]{0,1:T(8,128)(2,1)}, u32[]{:S(2)}) copy-start(bf16[768,64]{0,1:T(8,128)(2,1)} %param.14) | copy-start | bytes 294916
  6.5 20.9 %copy-start.3 = (bf16[768,256]{1,0:T(8,128)(2,1)S(1)}, bf16[768,256]{1,0:T(8,128)(2,1)}, u32[]{:S(2)}) copy-start(bf16[768,256]{1,0:T(8,128)(2,1)} %q_ref.1) | copy-start | bytes 1179652
  6.5 20.9 %copy-start.4 = (f32[4]{0:T(128)S(1)}, f32[4]{0:T(128)}, u32[]{:S(2)}) copy-start(f32[4]{0:T(128)} %sink_ref.1) | copy-start | bytes 52
  6.5 20.9 %copy-start.2 = (bf16[256,2048]{1,0:T(8,128)(2,1)S(1)}, bf16[256,2048]{1,0:T(8,128)(2,1)}, u32[]{:S(2)}) copy-start(bf16[256,2048]{1,0:T(8,128)(2,1)} %w_ref.3) | copy-start | bytes 3145732
  6.5 136.1 %all-gather.2.cloned.1.call-start = ((), (), s32[]{:S(2)}) async-start(), calls=%async_computation | async-start | bytes 10027008 | tf_op jit(solution)/shard_map/all_gather | solution.py:209
  10.2 25.3 %collective-permute-start.11 = (bf16[64,2112]{1,0:T(8,128)(2,1)}, bf16[64,2112]{1,0:T(8,128)(2,1)}, u32[]{:S(2)}, u32[]{:S(2)}) collective-permute-start(bf16[64,2112]{1,0:T(8,128)(2,1)} %concatenate.24), channel_id=1, source_target_pairs={{0,8},{8,16},{16,24},{24,0},{1,9},{9,17},{17,25},{25,1},{2,10},{10... | collective-permute-start | bytes 811016 | tf_op jit(solution)/shard_map/ppermute | solution.py:198
  11.7 23.8 %collective-permute-start.12 = (bf16[64,2112]{1,0:T(8,128)(2,1)}, bf16[64,2112]{1,0:T(8,128)(2,1)}, u32[]{:S(2)}, u32[]{:S(2)}) collective-permute-start(bf16[64,2112]{1,0:T(8,128)(2,1)} %concatenate.24), channel_id=1, source_target_pairs={{0,16},{8,24},{16,0},{24,8},{1,17},{9,25},{17,1},{25,9},{2,18},{10... | collective-permute-start | bytes 811016 | tf_op jit(solution)/shard_map/ppermute | solution.py:198
  14.5 21.0 %collective-permute-start.13 = (bf16[64,2112]{1,0:T(8,128)(2,1)}, bf16[64,2112]{1,0:T(8,128)(2,1)}, u32[]{:S(2)}, u32[]{:S(2)}) collective-permute-start(bf16[64,2112]{1,0:T(8,128)(2,1)} %concatenate.24), channel_id=1, source_target_pairs={{0,24},{8,0},{16,8},{24,16},{1,25},{9,1},{17,9},{25,17},{2,26},{10... | collective-permute-start | bytes 811016 | tf_op jit(solution)/shard_map/ppermute | solution.py:198
  15.0 10.6 %collective-permute-start = (bf16[129,128]{1,0:T(8,128)(2,1)S(1)}, bf16[129,128]{1,0:T(8,128)(2,1)S(1)}, u32[]{:S(2)}, u32[]{:S(2)}) collective-permute-start(bf16[129,128]{1,0:T(8,128)(2,1)S(1)} %get-tuple-element.48), channel_id=1, source_target_pairs={{0,8},{8,16},{16,24},{24,32},{32,40},{40,48},{48,56},{56,64},{64,7... | collective-permute-start | bytes 99080 | tf_op jit(solution)/shard_map/ppermute | solution.py:191
  18.5 8.9 %collective-permute-start.1 = (bf16[129,128]{1,0:T(8,128)(2,1)S(1)}, bf16[129,128]{1,0:T(8,128)(2,1)S(1)}, u32[]{:S(2)}, u32[]{:S(2)}) collective-permute-start(bf16[129,128]{1,0:T(8,128)(2,1)S(1)} %get-tuple-element.47), channel_id=1, source_target_pairs={{8,0},{16,8},{24,16},{32,24},{40,32},{48,40},{56,48},{64,56},{72,6... | collective-permute-start | bytes 99080 | tf_op jit(solution)/shard_map/ppermute | solution.py:192
  34.7 0.7 copy-start.5
  35.5 8.6 %copy-start.6 = (bf16[768,256]{1,0:T(8,128)(2,1)S(1)}, bf16[768,256]{1,0:T(8,128)(2,1)}, u32[]{:S(2)}) copy-start(bf16[768,256]{1,0:T(8,128)(2,1)} %copy-done.5) | copy-start | bytes 1179652
  40.6 3.5 %collective-permute-start.2 = (bf16[4,768,256]{2,1,0:T(8,128)(2,1)S(1)}, bf16[4,768,256]{2,1,0:T(8,128)(2,1)S(1)}, u32[]{:S(2)}, u32[]{:S(2)}) collective-permute-start(bf16[4,768,256]{2,1,0:T(8,128)(2,1)S(1)} %get-tuple-element.17), channel_id=1, source_target_pairs={{0,1},{1,0},{2,3},{3,2},{4,5},{5,4},{6,7},{7,6},{8,9},{9,8},{10,11... | collective-permute-start | bytes 4718600 | tf_op jit(solution)/shard_map/ppermute | solution.py:24
  45.2 12.7 %collective-permute-start.3 = (bf16[768,256]{1,0:T(8,128)(2,1)S(1)}, bf16[768,256]{1,0:T(8,128)(2,1)S(1)}, u32[]{:S(2)}, u32[]{:S(2)}) collective-permute-start(bf16[768,256]{1,0:T(8,128)(2,1)S(1)} %get-tuple-element.19), channel_id=1, source_target_pairs={{0,2},{2,4},{4,6},{6,0},{1,3},{3,5},{5,7},{7,1},{8,10},{10,12},{12... | collective-permute-start | bytes 1179656 | tf_op jit(solution)/shard_map/ppermute | solution.py:158
  47.1 20.5 %collective-permute-start.4 = (bf16[768,256]{1,0:T(8,128)(2,1)S(1)}, bf16[768,256]{1,0:T(8,128)(2,1)S(1)}, u32[]{:S(2)}, u32[]{:S(2)}) collective-permute-start(bf16[768,256]{1,0:T(8,128)(2,1)S(1)} %get-tuple-element.20), channel_id=1, source_target_pairs={{0,4},{2,6},{4,0},{6,2},{1,5},{3,7},{5,1},{7,3},{8,12},{10,14},{12... | collective-permute-start | bytes 1179656 | tf_op jit(solution)/shard_map/ppermute | solution.py:158
  50.0 17.6 %collective-permute-start.5 = (bf16[768,256]{1,0:T(8,128)(2,1)S(1)}, bf16[768,256]{1,0:T(8,128)(2,1)S(1)}, u32[]{:S(2)}, u32[]{:S(2)}) collective-permute-start(bf16[768,256]{1,0:T(8,128)(2,1)S(1)} %get-tuple-element.21), channel_id=1, source_target_pairs={{0,6},{2,0},{4,2},{6,4},{1,7},{3,1},{5,3},{7,5},{8,14},{10,8},{12,... | collective-permute-start | bytes 1179656 | tf_op jit(solution)/shard_map/ppermute | solution.py:158
  69.6 24.0 %copy-start.8 = (bf16[3,704]{1,0:T(4,128)(2,1)S(1)}, bf16[3,704]{1,0:T(4,128)(2,1)}, u32[]{:S(2)}) copy-start(bf16[3,704]{1,0:T(4,128)(2,1)} %param.22) | copy-start | bytes 12676
  71.7 11.6 %collective-permute-start.7 = (bf16[768,256]{1,0:T(8,128)(2,1)S(1)}, bf16[768,256]{1,0:T(8,128)(2,1)S(1)}, u32[]{:S(2)}, u32[]{:S(2)}) collective-permute-start(bf16[768,256]{1,0:T(8,128)(2,1)S(1)} %get-tuple-element.33), channel_id=1, source_target_pairs={{0,2},{2,4},{4,6},{6,0},{1,3},{3,5},{5,7},{7,1},{8,10},{10,12},{12... | collective-permute-start | bytes 1179656 | tf_op jit(solution)/shard_map/ppermute | solution.py:158
  72.9 20.0 %collective-permute-start.8 = (bf16[768,256]{1,0:T(8,128)(2,1)S(1)}, bf16[768,256]{1,0:T(8,128)(2,1)S(1)}, u32[]{:S(2)}, u32[]{:S(2)}) collective-permute-start(bf16[768,256]{1,0:T(8,128)(2,1)S(1)} %get-tuple-element.33), channel_id=1, source_target_pairs={{0,4},{2,6},{4,0},{6,2},{1,5},{3,7},{5,1},{7,3},{8,12},{10,14},{12... | collective-permute-start | bytes 1179656 | tf_op jit(solution)/shard_map/ppermute | solution.py:158
  75.3 17.5 %collective-permute-start.9 = (bf16[768,256]{1,0:T(8,128)(2,1)S(1)}, bf16[768,256]{1,0:T(8,128)(2,1)S(1)}, u32[]{:S(2)}, u32[]{:S(2)}) collective-permute-start(bf16[768,256]{1,0:T(8,128)(2,1)S(1)} %get-tuple-element.33), channel_id=1, source_target_pairs={{0,6},{2,0},{4,2},{6,4},{1,7},{3,1},{5,3},{7,5},{8,14},{10,8},{12,... | collective-permute-start | bytes 1179656 | tf_op jit(solution)/shard_map/ppermute | solution.py:158
  93.0 5.2 %collective-permute-start.10 = (bf16[3,768,256]{2,1,0:T(8,128)(2,1)S(1)}, bf16[3,768,256]{2,1,0:T(8,128)(2,1)}, u32[]{:S(2)}, u32[]{:S(2)}) collective-permute-start(bf16[3,768,256]{2,1,0:T(8,128)(2,1)S(1)} %pad_maximum_fusion), channel_id=1, source_target_pairs={{0,1},{1,0},{2,3},{3,2},{4,5},{5,4},{6,7},{7,6},{8,9},{9,8},{10,11... | collective-permute-start | bytes 3538952 | tf_op jit(solution)/shard_map/ppermute | solution.py:24
  93.1 3.4 %collective-permute-start.6 = (bf16[768,256]{1,0:T(8,128)(2,1)S(1)}, bf16[768,256]{1,0:T(8,128)(2,1)S(1)}, u32[]{:S(2)}, u32[]{:S(2)}) collective-permute-start(bf16[768,256]{1,0:T(8,128)(2,1)S(1)} %get-tuple-element.33), channel_id=1, source_target_pairs={{0,1},{1,0},{2,3},{3,2},{4,5},{5,4},{6,7},{7,6},{8,9},{9,8},{10,11... | collective-permute-start | bytes 1179656 | tf_op jit(solution)/shard_map/ppermute | solution.py:24
  103.4 39.3 %copy-start.9 = (f32[2048]{0:T(1024)S(1)}, f32[2048]{0:T(1024)}, u32[]{:S(2)}) copy-start(f32[2048]{0:T(1024)} %param.19) | copy-start | bytes 24580
  142.7 11.6 %copy-start.7 = (bf16[2048,2112]{1,0:T(8,128)(2,1)S(1)}, bf16[2048,2112]{1,0:T(8,128)(2,1)}, u32[]{:S(2)}) copy-start(bf16[2048,2112]{1,0:T(8,128)(2,1)} %all-gather.2.cloned.1.call-done) | copy-start | bytes 25952260
  148.5 11.8 %collective-permute-start.14 = (bf16[1,704]{0,1:T(8,128)(2,1)S(1)}, bf16[1,704]{0,1:T(8,128)(2,1)S(1)}, u32[]{:S(2)}, u32[]{:S(2)}) collective-permute-start(bf16[1,704]{0,1:T(8,128)(2,1)S(1)} %get-tuple-element.45), channel_id=1, source_target_pairs={{0,8},{8,16},{16,24},{24,32},{32,40},{40,48},{48,56},{56,64},{64,7... | collective-permute-start | bytes 4232 | tf_op jit(solution)/shard_map/ppermute | solution.py:238
  151.8 8.4 %collective-permute-start.15 = (bf16[1,704]{0,1:T(8,128)(2,1)S(1)}, bf16[1,704]{0,1:T(8,128)(2,1)S(1)}, u32[]{:S(2)}, u32[]{:S(2)}) collective-permute-start(bf16[1,704]{0,1:T(8,128)(2,1)S(1)} %get-tuple-element.46), channel_id=1, source_target_pairs={{8,0},{16,8},{24,16},{32,24},{40,32},{48,40},{56,48},{64,56},{72,6... | collective-permute-start | bytes 4232 | tf_op jit(solution)/shard_map/ppermute | solution.py:239
  164.0 3.7 %collective-permute-start.16 = (bf16[768,1024]{1,0:T(8,128)(2,1)S(1)}, bf16[768,1024]{1,0:T(8,128)(2,1)S(1)}, u32[]{:S(2)}, u32[]{:S(2)}) collective-permute-start(bf16[768,1024]{1,0:T(8,128)(2,1)S(1)} %convolution_convert_fusion), channel_id=1, source_target_pairs={{0,1},{1,0},{2,3},{3,2},{4,5},{5,4},{6,7},{7,6},{8,9},{9,8},{10,11... | collective-permute-start | bytes 4718600 | tf_op jit(solution)/shard_map/ppermute | solution.py:24
  169.3 12.4 %collective-permute-start.17 = (bf16[768,256]{1,0:T(8,128)(2,1)S(1)}, bf16[768,256]{1,0:T(8,128)(2,1)S(1)}, u32[]{:S(2)}, u32[]{:S(2)}) collective-permute-start(bf16[768,256]{1,0:T(8,128)(2,1)S(1)} %get-tuple-element.42), channel_id=1, source_target_pairs={{0,2},{2,4},{4,6},{6,0},{1,3},{3,5},{5,7},{7,1},{8,10},{10,12},{12... | collective-permute-start | bytes 1179656 | tf_op jit(solution)/shard_map/ppermute | solution.py:158
  170.8 20.3 %collective-permute-start.18 = (bf16[768,256]{1,0:T(8,128)(2,1)S(1)}, bf16[768,256]{1,0:T(8,128)(2,1)S(1)}, u32[]{:S(2)}, u32[]{:S(2)}) collective-permute-start(bf16[768,256]{1,0:T(8,128)(2,1)S(1)} %get-tuple-element.44), channel_id=1, source_target_pairs={{0,4},{2,6},{4,0},{6,2},{1,5},{3,7},{5,1},{7,3},{8,12},{10,14},{12... | collective-permute-start | bytes 1179656 | tf_op jit(solution)/shard_map/ppermute | solution.py:158
  173.5 17.6 %collective-permute-start.19 = (bf16[768,256]{1,0:T(8,128)(2,1)S(1)}, bf16[768,256]{1,0:T(8,128)(2,1)S(1)}, u32[]{:S(2)}, u32[]{:S(2)}) collective-permute-start(bf16[768,256]{1,0:T(8,128)(2,1)S(1)} %get-tuple-element.43), channel_id=1, source_target_pairs={{0,6},{2,0},{4,2},{6,4},{1,7},{3,1},{5,3},{7,5},{8,14},{10,8},{12,... | collective-permute-start | bytes 1179656 | tf_op jit(solution)/shard_map/ppermute | solution.py:158
Sparse Core Ops, SparseCore 0:
  40.7 101.9 all-gather.1
where the time goes:
time: 200 us; the launch traced here: 199 us
  waiting for transfers between devices  94.1 us (47%)
  starting transfers between devices  34.5 us (17%)
  local copies, waits for them, and re-layouts  22.9 us (11%)
  matrix products  14.2 us (7%)
  between operations  13.7 us (7%)
  other arithmetic  11.3 us (6%)
  Pallas kernels  8.44 us (4%)
    ppermute x9, waiting for transfers between devices, to_owners(): lax.ppermute(pairs[k], 'y', [(y, (y + k) % NY) for y in range(NY)])  48.3 us
    all_gather x1, waiting for transfers between devices, per_device(): lax.all_gather(block.reshape(NX * rows_w, width), 'z', axis=0, tiled=True)  34.9 us
    ppermute x9, starting transfers between devices, to_owners(): lax.ppermute(pairs[k], 'y', [(y, (y + k) % NY) for y in range(NY)])  17 us
    pallas_call x1, Pallas kernels, attention(): pl.pallas_call(attention_kernel, out_shape=[jax.ShapeDtypeStruct((rows, c...  7.31 us
    ppermute x4, waiting for transfers between devices, swap(): return lax.ppermute(block, 'core', [(0, 1), (1, 0)])  7.08 us
    dynamic_update_slice x4, local copies, waits for them, and re-layouts, put(): return lax.dynamic_update_slice(block, piece, start)  6.74 us
    dynamic_update_slice x4, local copies, waits for them, and re-layouts, per_device(): lax.dynamic_update_slice(mixed, others[k], (0, (at + 1 - core) * span))  6.23 us
    dot_general x1, matrix products, per_device(): jnp.dot(normed, full[:, :ff], preferred_element_type=jnp.float32)  5.64 us
  transfers between devices with their start and end apart: 21, of which 12 were waited for; matrix products, arithmetic and copies ran while one was open for 13% of the time, Pallas kernels for 4%

commit v1 on v0

--- a/solution.py
+++ b/solution.py
@@ -1,3 +1,5 @@
+import functools
+
 import jax
 import jax.numpy as jnp
 from jax import lax
@@ -16,8 +18,27 @@
 MB = 1 << 20
 
 
-def shift_x(k):
-    return [(x, (x + k) % NX) for x in range(NX)]
+def index_of(z, x, y, c):
+    return (((z % NZ) * NX + x % NX) * NY + y % NY) * NC + c
+
+
+def send_apart(block, dz, dx):
+    pairs = [
+        (index_of(z, x, y, c), index_of(z + s * dz, x + s * dx, y, c))
+        for z in range(NZ)
+        for x in range(NX)
+        for y in range(NY)
+        for c, s in ((0, 1), (1, -1))
+    ]
+    return lax.ppermute(block, AXES, pairs)
+
+
+def send_z(block, k):
+    return lax.ppermute(block, "z", [(z, (z + k) % NZ) for z in range(NZ)])
+
+
+def send_x(block, k):
+    return lax.ppermute(block, "x", [(x, (x + k) % NX) for x in range(NX)])
 
 
 def swap(block):
@@ -154,8 +175,127 @@
     )(order, left, w_out, got)
 
 
+def norm_kernel(at_ref, p0, p1, p2, p3, rest_ref, gain_ref, out_ref):
+    rows, span = p0.shape
+    width = out_ref.shape[1]
+
+    def step(n, carry):
+        here = pl.ds(pl.multiple_of(n * 64, 64), 64)
+        mine = [ref[here, :].astype(jnp.float32) for ref in (p0, p1, p2, p3)]
+        theirs = [rest_ref[k, here, :].astype(jnp.float32) for k in range(NY)]
+        square = sum(block * block for block in mine + theirs)
+        mean_sq = jnp.sum(square, axis=1, keepdims=True) * (1.0 / width)
+        scale = lax.rsqrt(mean_sq + EPS)
+        for k, block in enumerate(mine + theirs):
+            cols = pl.ds(pl.multiple_of(at_ref[2 * NY + k] * span, span), span)
+            out_ref[here, cols] = (block * scale * gain_ref[:, cols]).astype(jnp.bfloat16)
+        return carry
+
+    lax.fori_loop(0, rows // 64, step, 0)
+
+
+def normalised(order, parts, rest, gain):
+    rows, _ = parts[0].shape
+    return pl.pallas_call(
+        norm_kernel,
+        out_shape=jax.ShapeDtypeStruct((rows, gain.shape[1]), jnp.bfloat16),
+        in_specs=smem_specs(1) + vmem_specs(NY + 2),
+        out_specs=pl.BlockSpec(memory_space=pltpu.VMEM),
+        compiler_params=pltpu.CompilerParams(vmem_limit_bytes=10 * MB),
+        cost_estimate=pl.CostEstimate(flops=2 * 10**9, bytes_accessed=6 * MB, transcendentals=0),
+        name="normalise",
+    )(order, *parts, rest, gain)
+
+
+def up_kernel(start, left_ref, w_ref, out_ref):
+    width = out_ref.shape[1]
+
+    def step(n, carry):
+        here = pl.ds(pl.multiple_of(n * 256, 256), 256)
+        out_ref[here, :] = jnp.dot(
+            left_ref[here, :], w_ref[:, start : start + width], preferred_element_type=jnp.float32
+        ).astype(jnp.bfloat16)
+        return carry
+
+    lax.fori_loop(0, left_ref.shape[0] // 256, step, 0)
+
+
+def up(left, weights, start, width):
+    return pl.pallas_call(
+        functools.partial(up_kernel, start),
+        out_shape=jax.ShapeDtypeStruct((left.shape[0], width), jnp.bfloat16),
+        in_specs=vmem_specs(2),
+        out_specs=pl.BlockSpec(memory_space=pltpu.VMEM),
+        compiler_params=pltpu.CompilerParams(vmem_limit_bytes=14 * MB),
+        cost_estimate=pl.CostEstimate(flops=3 * 10**9, bytes_accessed=8 * MB, transcendentals=0),
+    )(left, weights)
+
+
+def hidden_kernel(value_ref, gate_ref, same_ref, before_ref, behind_ref, taps_ref, out_ref):
+    rows, ff = out_ref.shape
+    tail = gate_ref.shape[1]
+    width = value_ref.shape[1]
+    chunk = 64
+    count = rows // chunk
+    row = lax.broadcasted_iota(jnp.int32, (chunk, 128), 0)
+
+    for at in range(0, width, 128):
+        cols = slice(at, at + 128)
+        if at < tail:
+            low, high = before_ref[:, cols], behind_ref[:, cols]
+            taps = taps_ref[:, cols].astype(jnp.float32)
+        else:
+            pad = ((0, 0), (0, at + 128 - ff))
+            low, high = jnp.pad(before_ref[:, at:ff], pad), jnp.pad(behind_ref[:, at:ff], pad)
+            taps = jnp.pad(taps_ref[:, at:ff].astype(jnp.float32), pad)
+        low, high = low.astype(jnp.float32), high.astype(jnp.float32)
+
+        def step(n, above):
+            base = pl.multiple_of(n * chunk, chunk)
+            here = pl.ds(base, chunk)
+            value = value_ref[here, cols].astype(jnp.float32)
+            following = pl.ds(pl.multiple_of(jnp.minimum(base + chunk, rows - 16), 16), 16)
+            below = value_ref[following, cols].astype(jnp.float32)[:1]
+            below = jnp.where(n == count - 1, high, below)
+            prior = jnp.where(row == 0, above, pltpu.roll(value, 1, 0))
+            after_ = jnp.where(row == chunk - 1, below, pltpu.roll(value, chunk - 1, 0))
+            prev_same, next_same = same_ref[here, :1] > 0.5, same_ref[here, 1:2] > 0.5
+            conv = (
+                taps[0:1] * jnp.where(prev_same, prior, 0.0)
+                + taps[1:2] * value
+                + taps[2:3] * jnp.where(next_same, after_, 0.0)
+            )
+            act = conv * lax.logistic(conv)
+            if at < tail:
+                out_ref[here, cols] = (act * gate_ref[here, cols].astype(jnp.float32)).astype(
+                    jnp.bfloat16
+                )
+            else:
+                gate = pltpu.roll(value, 64, 1)
+                out_ref[here, at:ff] = (act * gate).astype(jnp.bfloat16)[:, : ff - at]
+            return value[chunk - 1 :]
+
+        lax.fori_loop(0, count, step, low)
+
+
+def hidden_units(value, gate, same, before, behind, taps):
+    rows, ff = value.shape[0], taps.shape[1]
+    return pl.pallas_call(
+        hidden_kernel,
+        out_shape=jax.ShapeDtypeStruct((rows, ff), jnp.bfloat16),
+        in_specs=vmem_specs(6),
+        out_specs=pl.BlockSpec(memory_space=pltpu.VMEM),
+        compiler_params=pltpu.CompilerParams(vmem_limit_bytes=8 * MB),
+        cost_estimate=pl.CostEstimate(flops=2 * 10**9, bytes_accessed=4 * MB, transcendentals=0),
+        name="hidden_units",
+    )(value, gate, same, before, behind, taps)
+
+
 def to_owners(pairs):
-    return [lax.ppermute(pairs[k], "y", [(y, (y + k) % NY) for y in range(NY)]) for k in range(1, NY)]
+    got = []
+    for k in range(1, NY):
+        got.append(lax.ppermute(pairs[k], "y", [(y, (y + k) % NY) for y in range(NY)]))
+    return got
 
 
 def per_device(
@@ -172,14 +312,14 @@
     conv_taps,
     w_down_t,
 ):
-    rows_here = queries.shape[0]
     model_width = residual.shape[1]
     span = model_width // (NY * NC)
     ff = w_value_up.shape[1]
-    _, x, y, core = (lax.axis_index(axis) for axis in AXES)
+    z, x, y, core = (lax.axis_index(axis) for axis in AXES)
     tp = y * NC + core
     order = jnp.stack(
         [((y + k) % NY) * NC + who for who in (core, 1 - core) for k in range(NY)]
+        + [((y - k) % NY) * NC + who for who in (core, 1 - core) for k in range(NY)]
     )
     count = NZ * NX
     forward = [(i, i + 1) for i in range(count - 1)]
@@ -191,25 +331,54 @@
     low = lax.ppermute(packed[:, -WINDOW:], ("z", "x"), forward)
     high = lax.ppermute(packed[:, :WINDOW], ("z", "x"), backward)
 
-    share = jnp.concatenate([after(w_value_up, packed), w_gate_up, w_down_t], axis=1)
+    tail = ff - ff % 128
+    first = after(w_value_up, packed)
+    share = jnp.concatenate(
+        [w_gate_up[:, :tail], first, w_gate_up[:, tail:]], axis=1
+    )
     rows_w, width = share.shape
     gathered = []
     for k in range(1, NX):
-        gathered.append(lax.ppermute(share, "x", shift_x(k)))
+        gathered.append(send_x(share, k))
 
     attended, theirs = attention(
         order, sink_logits, queries, keys_t, vals_t, labels, low, high, w_out
     )
     got = swap(theirs)
 
+    gathered = lax.optimization_barrier((*gathered, theirs))[:-1]
     block = put(jnp.zeros((NX, rows_w, width), share.dtype), share, x)
-    gathered = lax.optimization_barrier((*gathered, theirs))[:-1]
     for k, piece in enumerate(gathered):
         block = put(block, piece, (x - k - 1) % NX)
-    full = lax.all_gather(block.reshape(NX * rows_w, width), "z", axis=0, tiled=True)
+    block = block.reshape(NX * rows_w, width)
+    full = put(jnp.zeros((NZ, NX * rows_w, width), share.dtype), block, z)
+
+    def ring_step(plus, minus):
+        plus = send_z(plus, 1)
+        minus = send_z(minus, -1)
+        return plus, minus
+
+    def keep(full, plus, minus, k):
+        return put(put(full, plus, (z - k) % NZ), minus, (z + k) % NZ)
+
+    plus1, minus1 = ring_step(block, block)
 
     pairs = pair_sums(order, attended, w_out, got)
     sent = to_owners(pairs)
+
+    down1 = after(w_down_t, pairs[0])
+    near = ring_step(down1, down1)
+    far_plus = send_z(down1, 2)
+    far_minus = send_z(down1, -2)
+
+    plus2, minus2 = ring_step(plus1, minus1)
+    third = ring_step(far_plus, far_minus)
+    last = send_apart(jnp.where(core == 0, far_plus, far_minus), 2, 0)
+    whole = put(jnp.zeros((NZ,) + w_down_t.shape, w_down_t.dtype), w_down_t, z)
+    whole = keep(whole, *near, 1)
+    whole = keep(whole, far_plus, far_minus, 2)
+    whole = keep(whole, *third, 3)
+    whole = put(whole, last, (z + NZ // 2) % NZ)
 
     own_res = lax.dynamic_slice_in_dim(residual, tp * span, span, 1)
     total = own_res.astype(jnp.float32)
@@ -219,47 +388,39 @@
     mixed_own = (total + summed).astype(jnp.bfloat16)
 
     parts = [mixed_own] + to_owners([mixed_own] * NY)
-    others = [swap(mixed_own)]
-    rest = swap(jnp.stack(parts[1:]))
-    others += [rest[k] for k in range(NY - 1)]
-
-    mixed = jnp.zeros((rows_here, model_width), jnp.bfloat16)
-    for k in range(NY):
-        at = ((y - k) % NY) * NC
-        mixed = lax.dynamic_update_slice(mixed, parts[k], (0, (at + core) * span))
-        mixed = lax.dynamic_update_slice(mixed, others[k], (0, (at + 1 - core) * span))
-    mixed_f = mixed.astype(jnp.float32)
-    mean_sq = jnp.mean(mixed_f * mixed_f, axis=1, keepdims=True)
-    normed = (mixed_f * lax.rsqrt(mean_sq + EPS) * norm_gain).astype(jnp.bfloat16)
-
-    up_value = jnp.dot(normed, full[:, :ff], preferred_element_type=jnp.float32).astype(
-        jnp.bfloat16
-    )
-    before = lax.ppermute(up_value[-1:], ("z", "x"), forward)
-    behind = lax.ppermute(up_value[:1], ("z", "x"), backward)
-    up_gate = after(
-        jnp.dot(normed, full[:, ff : 2 * ff], preferred_element_type=jnp.float32).astype(
-            jnp.bfloat16
-        ),
-        up_value,
-    )
-    rim_value = jnp.concatenate([before, up_value, behind], axis=0).astype(jnp.float32)
+    plus3, minus3 = ring_step(plus2, minus2)
+    full = keep(after(full, mixed_own), plus1, minus1, 1)
+    whole_plus = send_x(whole, 1)
+    whole_minus = send_x(whole, -1)
+
+    rest = swap(jnp.stack(parts))
+    last = send_apart(jnp.where(core == 0, plus3, minus3), 1, 0)
+    full = keep(after(full, rest), plus2, minus2, 2)
+    full = keep(full, plus3, minus3, 3)
+    full = put(full, last, (z + NZ // 2) % NZ).reshape(model_width, width)
+
+    whole_far = send_apart(jnp.where(core == 0, whole_plus, whole_minus), 0, 1)
+    full_down = jnp.zeros((NZ, NX, rows_w, ff), w_down_t.dtype)
+    full_down = put(full_down, whole[:, None], 0, x)
+    full_down = put(full_down, whole_plus[:, None], 0, (x - 1) % NX)
+    full_down = put(full_down, whole_minus[:, None], 0, (x + 1) % NX)
+    full_down = put(full_down, whole_far[:, None], 0, (x + 2) % NX).reshape(model_width, ff)
+
+    normed = normalised(order, parts, rest, norm_gain[None])
+    up_value = up(normed, full, tail, width - tail)
+    before = lax.ppermute(up_value[-1:, :ff], ("z", "x"), forward)
+    behind = lax.ppermute(up_value[:1, :ff], ("z", "x"), backward)
+    up_gate = up(normed, full, 0, tail)
     edge = jnp.concatenate([low[-1:, -1:], packed[-1:], high[-1:, :1]], axis=1)[0]
-    prev_same = (edge[:-2] == edge[1:-1])[:, None]
-    next_same = (edge[2:] == edge[1:-1])[:, None]
-    tap_f = conv_taps.astype(jnp.float32)
-    conv = (
-        tap_f[0] * jnp.where(prev_same, rim_value[:-2], 0.0)
-        + tap_f[1] * up_value.astype(jnp.float32)
-        + tap_f[2] * jnp.where(next_same, rim_value[2:], 0.0)
-    )
-    hidden = (jax.nn.silu(conv) * up_gate.astype(jnp.float32)).astype(jnp.bfloat16)
+    same = jnp.stack([edge[:-2] == edge[1:-1], edge[2:] == edge[1:-1]], axis=1)
+    same = same.astype(jnp.float32)
+    hidden = hidden_units(up_value, up_gate, same, before, behind, conv_taps)
 
     def down(who):
         weights = jnp.concatenate(
             [
                 lax.dynamic_slice(
-                    full, ((((y + k) % NY) * NC + who) * span, 2 * ff), (span, ff)
+                    full_down, ((((y + k) % NY) * NC + who) * span, 0), (span, ff)
                 )
                 for k in range(NY)
             ],

time: 200 us -> 219 us (1.095)
  the two profiles are of different devices: /device:TPU:2 before, /device:TPU:103 now
where the time goes in v1:
time: 219 us; the launch traced here: 218 us
  waiting for transfers between devices  94.9 us (43%)
  starting transfers between devices  58.3 us (27%)
  local copies, waits for them, and re-layouts  31.1 us (14%)
  Pallas kernels  24.2 us (11%)
  other arithmetic  5.66 us (3%)
  matrix products  2.85 us (1%)
    ppermute x9, waiting for transfers between devices, to_owners(): lax.ppermute(pairs[k], 'y', [(y, (y + k) % NY) for y in range(NY)])  43.2 us
    ppermute x12, waiting for transfers between devices, send_z(): return lax.ppermute(block, 'z', [(z, (z + k) % NZ) for z in range(NZ)])  28.8 us
    dynamic_update_slice x24, local copies, waits for them, and re-layouts, put(): return lax.dynamic_update_slice(block, piece, start)  16.1 us
    ppermute x3, starting transfers between devices, swap(): return lax.ppermute(block, 'core', [(0, 1), (1, 0)])  13.6 us
    ppermute x3, waiting for transfers between devices, send_apart(): return lax.ppermute(block, AXES, pairs)  12.7 us
    ppermute x12, starting transfers between devices, send_z(): return lax.ppermute(block, 'z', [(z, (z + k) % NZ) for z in range(NZ)])  8.2 us
    ppermute x1, starting transfers between devices, per_device(): before = lax.ppermute(up_value[-1:, :ff], ('z', 'x'), forward)  8.06 us
    unnamed x24, local copies, waits for them, and re-layouts  8.01 us
  transfers between devices with their start and end apart: 36, of which 16 were waited for; matrix products, arithmetic and copies ran while one was open for 11% of the time, Pallas kernels for 6%

profile of v1, /device:TPU:103, one launch (start us, length us, event | category | flops | bytes accessed | tf_op | source)
XLA Modules:
  0.0 217.6 jit_solution(6025990136689594670)
XLA Ops:
  4.5 2.1 collective-permute-start.11
  6.7 7.1 %collective-permute-start = (bf16[129,128]{1,0:T(8,128)(2,1)S(1)}, bf16[129,128]{1,0:T(8,128)(2,1)S(1)}, u32[]{:S(2)}, u32[]{:S(2)}) collective-permute-start(bf16[129,128]{1,0:T(8,128)(2,1)S(1)} %get-tuple-element.47), channel_id=1, source_target_pairs={{0,8},{8,16},{16,24},{24,32},{32,40},{40,48},{48,56},{56,64},{64,7... | collective-permute-start | bytes 99080 | tf_op jit(solution)/shard_map/ppermute | solution.py:331
  13.8 1.9 collective-permute-start.1
  17.5 4.4 %collective-permute-done.1.high_ref = bf16[129,128]{1,0:T(8,128)(2,1)S(1)} collective-permute-done((bf16[129,128]{1,0:T(8,128)(2,1)S(1)}, bf16[129,128]{1,0:T(8,128)(2,1)S(1)}, u32[]{:S(2)}, u32[]{:S(2)}) %collective-permute-start.1) | collective-permute-done | bytes 33056 | tf_op jit(solution)/shard_map/ppermute | solution.py:332
  23.6 1.2 copy-done.2
  26.5 7.3 %attention.1 = (bf16[768,256]{1,0:T(8,128)(2,1)S(1)}, bf16[4,768,256]{2,1,0:T(8,128)(2,1)S(1)}) custom-call(s32[16]{0:T(128)S(1)} %stack.81.at_ref, f32[4]{0:T(128)S(1)} %copy-done.7, bf16[768,256]{1,0:T(8,128)(2,1)S(1)} %copy-done.4, bf16[64,768]{1,0:T(8,128)(2,1)S(1)} %bitcast.88, bf16[64,768]{1,0:T(8,128)(2,1)S(1)} %bitcast.90, ...), custom_call_target="tpu_custom_call" | custom-call | flops 4000000000 | bytes 4194304 | tf_op jit(solution)/shard_map/attention/pallas_call | solution.py:136
  34.6 2.9 %collective-permute-start.2 = (bf16[4,768,256]{2,1,0:T(8,128)(2,1)S(1)}, bf16[4,768,256]{2,1,0:T(8,128)(2,1)S(1)}, u32[]{:S(2)}, u32[]{:S(2)}) collective-permute-start(bf16[4,768,256]{2,1,0:T(8,128)(2,1)S(1)} %get-tuple-element.19), channel_id=1, source_target_pairs={{0,1},{1,0},{2,3},{3,2},{4,5},{5,4},{6,7},{7,6},{8,9},{9,8},{10,11... | collective-permute-start | bytes 4718600 | tf_op jit(solution)/shard_map/ppermute | solution.py:45
  37.5 1.6 bitcast_dynamic-update-slice_fusion.14
  39.2 1.6 bitcast_dynamic-update-slice_fusion.13
  40.8 1.6 bitcast_dynamic-update-slice_fusion.12
  42.4 1.5 collective-permute-start.14
  46.6 1.3 fusion.14
  48.2 1.2 copy-done.3
  51.6 1.3 collective-permute-start.22
  53.3 1.2 bitcast_dynamic-update-slice_fusion.11
  54.5 5.9 %collective-permute-done.13 = bf16[256,1408]{1,0:T(8,128)(2,1)} collective-permute-done((bf16[256,1408]{1,0:T(8,128)(2,1)}, bf16[256,1408]{1,0:T(8,128)(2,1)}, u32[]{:S(2)}, u32[]{:S(2)}) %collective-permute-start.13) | collective-permute-done | bytes 720928 | tf_op jit(solution)/shard_map/ppermute | solution.py:37
  60.4 1.5 collective-permute-start.15
  61.9 3.8 %collective-permute-start.24 = (bf16[64,704]{1,0:T(8,128)(2,1)S(1)}, bf16[64,704]{1,0:T(8,128)(2,1)S(1)}, u32[]{:S(2)}, u32[]{:S(2)}) collective-permute-start(bf16[64,704]{1,0:T(8,128)(2,1)S(1)} %copy-done.11), channel_id=1, source_target_pairs={{0,64},{32,96},{64,128},{96,160},{128,192},{160,224},{192,0},{224,... | collective-permute-start | bytes 270344 | tf_op jit(solution)/shard_map/ppermute | solution.py:37
  66.4 15.8 %collective-permute-done.23 = bf16[64,704]{1,0:T(8,128)(2,1)S(1)} collective-permute-done((bf16[64,704]{1,0:T(8,128)(2,1)S(1)}, bf16[64,704]{1,0:T(8,128)(2,1)S(1)}, u32[]{:S(2)}, u32[]{:S(2)}) %collective-permute-start.23) | collective-permute-done | bytes 90144 | tf_op jit(solution)/shard_map/ppermute | solution.py:37
  82.2 2.7 %collective-permute-start.5 = (bf16[768,256]{1,0:T(8,128)(2,1)S(1)}, bf16[768,256]{1,0:T(8,128)(2,1)S(1)}, u32[]{:S(2)}, u32[]{:S(2)}) collective-permute-start(bf16[768,256]{1,0:T(8,128)(2,1)S(1)} %get-tuple-element.23), channel_id=1, source_target_pairs={{0,6},{2,0},{4,2},{6,4},{1,7},{3,1},{5,3},{7,5},{8,14},{10,8},{12,... | collective-permute-start | bytes 1179656 | tf_op jit(solution)/shard_map/ppermute | solution.py:297
  87.2 3.1 %collective-permute-done.26 = bf16[64,704]{1,0:T(8,128)(2,1)S(1)} collective-permute-done((bf16[64,704]{1,0:T(8,128)(2,1)S(1)}, bf16[64,704]{1,0:T(8,128)(2,1)S(1)}, u32[]{:S(2)}, u32[]{:S(2)}) %collective-permute-start.26) | collective-permute-done | bytes 90144 | tf_op jit(solution)/shard_map/ppermute | solution.py:37
  91.0 4.0 %collective-permute-done.27 = bf16[64,704]{1,0:T(8,128)(2,1)S(1)} collective-permute-done((bf16[64,704]{1,0:T(8,128)(2,1)S(1)}, bf16[64,704]{1,0:T(8,128)(2,1)S(1)}, u32[]{:S(2)}, u32[]{:S(2)}) %collective-permute-start.27) | collective-permute-done | bytes 90144 | tf_op jit(solution)/shard_map/ppermute | solution.py:37
  95.7 6.3 %collective-permute-done.28 = bf16[64,704]{1,0:T(8,128)(2,1)S(1)} collective-permute-done((bf16[64,704]{1,0:T(8,128)(2,1)S(1)}, bf16[64,704]{1,0:T(8,128)(2,1)S(1)}, u32[]{:S(2)}, u32[]{:S(2)}) %collective-permute-start.28) | collective-permute-done | bytes 90144 | tf_op jit(solution)/shard_map/ppermute | solution.py:33
  104.7 1.4 collective-permute-start.30
  106.1 3.7 %collective-permute-done.3 = bf16[768,256]{1,0:T(8,128)(2,1)S(1)} collective-permute-done((bf16[768,256]{1,0:T(8,128)(2,1)S(1)}, bf16[768,256]{1,0:T(8,128)(2,1)S(1)}, u32[]{:S(2)}, u32[]{:S(2)}) %collective-permute-start.3) | collective-permute-done | bytes 393248 | tf_op jit(solution)/shard_map/ppermute | solution.py:297
  109.8 1.3 add_convert_fusion.2.p0
  111.2 1.4 collective-permute-start.7
  112.6 1.2 bitcast_dynamic-update-slice_fusion.10
  113.9 11.9 %collective-permute-done.6.p1 = bf16[768,256]{1,0:T(8,128)(2,1)S(1)} collective-permute-done((bf16[768,256]{1,0:T(8,128)(2,1)S(1)}, bf16[768,256]{1,0:T(8,128)(2,1)S(1)}, u32[]{:S(2)}, u32[]{:S(2)}) %collective-permute-start.6) | collective-permute-done | bytes 393248 | tf_op jit(solution)/shard_map/ppermute | solution.py:297
  125.8 1.2 bitcast_dynamic-update-slice_fusion.9
  127.0 7.7 %collective-permute-done.8.p3 = bf16[768,256]{1,0:T(8,128)(2,1)S(1)} collective-permute-done((bf16[768,256]{1,0:T(8,128)(2,1)S(1)}, bf16[768,256]{1,0:T(8,128)(2,1)S(1)}, u32[]{:S(2)}, u32[]{:S(2)}) %collective-permute-start.8) | collective-permute-done | bytes 393248 | tf_op jit(solution)/shard_map/ppermute | solution.py:297
  134.9 7.8 %collective-permute-start.9 = (bf16[4,768,256]{2,1,0:T(8,128)(2,1)S(1)}, bf16[4,768,256]{2,1,0:T(8,128)(2,1)S(1)}, u32[]{:S(2)}, u32[]{:S(2)}) collective-permute-start(bf16[4,768,256]{2,1,0:T(8,128)(2,1)S(1)} %pad_maximum_fusion), channel_id=1, source_target_pairs={{0,1},{1,0},{2,3},{3,2},{4,5},{5,4},{6,7},{7,6},{8,9},{9,8},{10,11... | collective-permute-start | bytes 4718600 | tf_op jit(solution)/shard_map/ppermute | solution.py:45
  143.3 6.5 %collective-permute-start.19 = (bf16[256,1408]{1,0:T(8,128)(2,1)S(1)}, bf16[256,1408]{1,0:T(8,128)(2,1)S(1)}, u32[]{:S(2)}, u32[]{:S(2)}) collective-permute-start(bf16[256,1408]{1,0:T(8,128)(2,1)S(1)} %broadcast_select_fusion.1), channel_id=1, source_target_pairs={{0,32},{1,225},{2,34},{3,227},{4,36},{5,229},{6,38},{7,231},{8,40}... | collective-permute-start | bytes 2162696 | tf_op jit(solution)/shard_map/ppermute | solution.py:33
  149.9 5.3 %collective-permute-done.31 = bf16[8,64,704]{2,1,0:T(8,128)(2,1)S(1)} collective-permute-done((bf16[8,64,704]{2,1,0:T(8,128)(2,1)S(1)}, bf16[8,64,704]{2,1,0:T(8,128)(2,1)S(1)}, u32[]{:S(2)}, u32[]{:S(2)}) %collective-permute-start.31) | collective-permute-done | bytes 720928 | tf_op jit(solution)/shard_map/ppermute | solution.py:33
  156.2 2.6 %normalise.1.left_ref = bf16[768,2048]{1,0:T(8,128)(2,1)S(1)} custom-call(s32[16]{0:T(128)S(1)} %stack.81.at_ref, bf16[768,256]{1,0:T(8,128)(2,1)S(1)} %add_convert_fusion.2.p0, bf16[768,256]{1,0:T(8,128)(2,1)S(1)} %collective-permute-done.6.p1, bf16[768,256]{1,0:T(8,128)(2,1)S(1)} %collective-permute-done.7.p2, ...), custom_call_target="tpu_custom_call" | custom-call | flops 2000000000 | bytes 6291456 | tf_op jit(solution)/shard_map/normalise/pallas_call | solution.py:199
  160.0 3.0 %shard_map.118.value_ref = bf16[768,768]{1,0:T(8,128)(2,1)S(1)} custom-call(bf16[768,2048]{1,0:T(8,128)(2,1)S(1)} %normalise.1.left_ref, bf16[2048,1408]{1,0:T(8,128)(2,1)S(1)} %bitcast.81), custom_call_target="tpu_custom_call" | custom-call | flops 3000000000 | bytes 8388608 | tf_op jit(solution)/shard_map/pallas_call | solution.py:224
  163.0 8.1 %collective-permute-start.20 = (bf16[1,704]{1,0:T(2,128)(2,1)S(1)}, bf16[1,704]{1,0:T(2,128)(2,1)S(1)}, u32[]{:S(2)}, u32[]{:S(2)}) collective-permute-start(bf16[1,704]{1,0:T(2,128)(2,1)S(1)} %get-tuple-element.45), channel_id=1, source_target_pairs={{0,8},{8,16},{16,24},{24,32},{32,40},{40,48},{48,56},{56,64},{64,7... | collective-permute-start | bytes 4232 | tf_op jit(solution)/shard_map/ppermute | solution.py:411
  171.1 1.9 collective-permute-start.21
  173.1 3.0 %shard_map.119.gate_ref = bf16[768,640]{1,0:T(8,128)(2,1)S(1)} custom-call(bf16[768,2048]{1,0:T(8,128)(2,1)S(1)} %normalise.1.left_ref, bf16[2048,1408]{1,0:T(8,128)(2,1)S(1)} %bitcast.82), custom_call_target="tpu_custom_call" | custom-call | flops 3000000000 | bytes 8388608 | tf_op jit(solution)/shard_map/pallas_call | solution.py:224
  176.1 2.7 %collective-permute-done.21.behind_ref = bf16[1,704]{1,0:T(2,128)(2,1)S(1)} collective-permute-done((bf16[1,704]{1,0:T(2,128)(2,1)S(1)}, bf16[1,704]{1,0:T(2,128)(2,1)S(1)}, u32[]{:S(2)}, u32[]{:S(2)}) %collective-permute-start.21) | collective-permute-done | bytes 1440 | tf_op jit(solution)/shard_map/ppermute | solution.py:412
  178.8 7.2 %hidden_units.1 = bf16[768,704]{1,0:T(8,128)(2,1)S(1)} custom-call(bf16[768,768]{1,0:T(8,128)(2,1)S(1)} %shard_map.118.value_ref, bf16[768,640]{1,0:T(8,128)(2,1)S(1)} %shard_map.119.gate_ref, f32[768,2]{1,0:T(8,128)S(1)} %copy.22.same_ref, bf16[1,704]{1,0:T(2,128)(2,1)S(1)} %collective-permute-done.20.before_ref, ...), custom_call_target="tpu_custom_call" | custom-call | flops 2000000000 | bytes 4194304 | tf_op jit(solution)/shard_map/hidden_units/pallas_call | solution.py:283
  186.0 1.4 convolution_convert_fusion
  187.4 2.9 %collective-permute-start.32 = (bf16[768,1024]{1,0:T(8,128)(2,1)S(1)}, bf16[768,1024]{1,0:T(8,128)(2,1)S(1)}, u32[]{:S(2)}, u32[]{:S(2)}) collective-permute-start(bf16[768,1024]{1,0:T(8,128)(2,1)S(1)} %convolution_convert_fusion), channel_id=1, source_target_pairs={{0,1},{1,0},{2,3},{3,2},{4,5},{5,4},{6,7},{7,6},{8,9},{9,8},{10,11... | collective-permute-start | bytes 4718600 | tf_op jit(solution)/shard_map/ppermute | solution.py:45
  190.3 3.0 %collective-permute-done.32 = bf16[768,1024]{1,0:T(8,128)(2,1)S(1)} collective-permute-done((bf16[768,1024]{1,0:T(8,128)(2,1)S(1)}, bf16[768,1024]{1,0:T(8,128)(2,1)S(1)}, u32[]{:S(2)}, u32[]{:S(2)}) %collective-permute-start.32) | collective-permute-done | bytes 1572896 | tf_op jit(solution)/shard_map/ppermute | solution.py:45
  193.3 1.4 add_convert_fusion
  196.6 8.6 %collective-permute-done.35 = bf16[768,256]{1,0:T(8,128)(2,1)S(1)} collective-permute-done((bf16[768,256]{1,0:T(8,128)(2,1)S(1)}, bf16[768,256]{1,0:T(8,128)(2,1)S(1)}, u32[]{:S(2)}, u32[]{:S(2)}) %collective-permute-start.35) | collective-permute-done | bytes 393248 | tf_op jit(solution)/shard_map/ppermute | solution.py:297
  205.2 2.4 %collective-permute-done.34 = bf16[768,256]{1,0:T(8,128)(2,1)S(1)} collective-permute-done((bf16[768,256]{1,0:T(8,128)(2,1)S(1)}, bf16[768,256]{1,0:T(8,128)(2,1)S(1)}, u32[]{:S(2)}, u32[]{:S(2)}) %collective-permute-start.34) | collective-permute-done | bytes 393248 | tf_op jit(solution)/shard_map/ppermute | solution.py:297
  207.5 9.0 %collective-permute-done.33 = bf16[768,256]{1,0:T(8,128)(2,1)S(1)} collective-permute-done((bf16[768,256]{1,0:T(8,128)(2,1)S(1)}, bf16[768,256]{1,0:T(8,128)(2,1)S(1)}, u32[]{:S(2)}, u32[]{:S(2)}) %collective-permute-start.33) | collective-permute-done | bytes 393248 | tf_op jit(solution)/shard_map/ppermute | solution.py:297
  (110 shorter events, 28.9 us)
Async XLA Ops:
  4.3 33.3 %collective-permute-start.10 = (bf16[64,1408]{1,0:T(8,128)(2,1)S(1)}, bf16[64,1408]{1,0:T(8,128)(2,1)}, u32[]{:S(2)}, u32[]{:S(2)}) collective-permute-start(bf16[64,1408]{1,0:T(8,128)(2,1)S(1)} %concatenate.20), channel_id=1, source_target_pairs={{0,8},{8,16},{16,24},{24,0},{1,9},{9,17},{17,25},{25,1},{2,10},{10... | collective-permute-start | bytes 540680 | tf_op jit(solution)/shard_map/ppermute | solution.py:41
  4.5 33.0 %collective-permute-start.11 = (bf16[64,1408]{1,0:T(8,128)(2,1)S(1)}, bf16[64,1408]{1,0:T(8,128)(2,1)}, u32[]{:S(2)}, u32[]{:S(2)}) collective-permute-start(bf16[64,1408]{1,0:T(8,128)(2,1)S(1)} %concatenate.20), channel_id=1, source_target_pairs={{0,16},{8,24},{16,0},{24,8},{1,17},{9,25},{17,1},{25,9},{2,18},{10... | collective-permute-start | bytes 540680 | tf_op jit(solution)/shard_map/ppermute | solution.py:41
  6.7 30.8 %collective-permute-start.12 = (bf16[64,1408]{1,0:T(8,128)(2,1)S(1)}, bf16[64,1408]{1,0:T(8,128)(2,1)}, u32[]{:S(2)}, u32[]{:S(2)}) collective-permute-start(bf16[64,1408]{1,0:T(8,128)(2,1)S(1)} %concatenate.20), channel_id=1, source_target_pairs={{0,24},{8,0},{16,8},{24,16},{1,25},{9,1},{17,9},{25,17},{2,26},{10... | collective-permute-start | bytes 540680 | tf_op jit(solution)/shard_map/ppermute | solution.py:41
  6.7 10.8 %collective-permute-start = (bf16[129,128]{1,0:T(8,128)(2,1)S(1)}, bf16[129,128]{1,0:T(8,128)(2,1)S(1)}, u32[]{:S(2)}, u32[]{:S(2)}) collective-permute-start(bf16[129,128]{1,0:T(8,128)(2,1)S(1)} %get-tuple-element.47), channel_id=1, source_target_pairs={{0,8},{8,16},{16,24},{24,32},{32,40},{40,48},{48,56},{56,64},{64,7... | collective-permute-start | bytes 99080 | tf_op jit(solution)/shard_map/ppermute | solution.py:331
  13.8 8.0 %collective-permute-start.1 = (bf16[129,128]{1,0:T(8,128)(2,1)S(1)}, bf16[129,128]{1,0:T(8,128)(2,1)S(1)}, u32[]{:S(2)}, u32[]{:S(2)}) collective-permute-start(bf16[129,128]{1,0:T(8,128)(2,1)S(1)} %get-tuple-element.46), channel_id=1, source_target_pairs={{8,0},{16,8},{24,16},{32,24},{40,32},{48,40},{56,48},{64,56},{72,6... | collective-permute-start | bytes 99080 | tf_op jit(solution)/shard_map/ppermute | solution.py:332
  21.8 0.9 copy-start
  22.7 0.9 copy-start.1
  23.6 1.2 copy-start.2
  24.8 1.0 copy-start.4
  25.8 0.7 copy-start.7
  26.5 18.3 %copy-start.10 = (bf16[64,704]{1,0:T(8,128)(2,1)S(1)}, bf16[64,704]{1,0:T(8,128)(2,1)}, u32[]{:S(2)}) copy-start(bf16[64,704]{1,0:T(8,128)(2,1)} %param.23) | copy-start | bytes 270340
  33.8 0.7 copy-start.8
  34.6 13.6 %collective-permute-start.2 = (bf16[4,768,256]{2,1,0:T(8,128)(2,1)S(1)}, bf16[4,768,256]{2,1,0:T(8,128)(2,1)S(1)}, u32[]{:S(2)}, u32[]{:S(2)}) collective-permute-start(bf16[4,768,256]{2,1,0:T(8,128)(2,1)S(1)} %get-tuple-element.19), channel_id=1, source_target_pairs={{0,1},{1,0},{2,3},{3,2},{4,5},{5,4},{6,7},{7,6},{8,9},{9,8},{10,11... | collective-permute-start | bytes 4718600 | tf_op jit(solution)/shard_map/ppermute | solution.py:45
  42.4 18.0 %collective-permute-start.13 = (bf16[256,1408]{1,0:T(8,128)(2,1)}, bf16[256,1408]{1,0:T(8,128)(2,1)}, u32[]{:S(2)}, u32[]{:S(2)}) collective-permute-start(bf16[256,1408]{1,0:T(8,128)(2,1)} %bitcast.26), channel_id=1, source_target_pairs={{0,32},{32,64},{64,96},{96,128},{128,160},{160,192},{192,224},{224... | collective-permute-start | bytes 2162696 | tf_op jit(solution)/shard_map/ppermute | solution.py:37
  42.4 19.5 %collective-permute-start.14 = (bf16[256,1408]{1,0:T(8,128)(2,1)}, bf16[256,1408]{1,0:T(8,128)(2,1)}, u32[]{:S(2)}, u32[]{:S(2)}) collective-permute-start(bf16[256,1408]{1,0:T(8,128)(2,1)} %bitcast.26), channel_id=1, source_target_pairs={{0,224},{32,0},{64,32},{96,64},{128,96},{160,128},{192,160},{224,1... | collective-permute-start | bytes 2162696 | tf_op jit(solution)/shard_map/ppermute | solution.py:37
  48.2 1.2 copy-start.3
  49.4 1.0 copy-start.9
  50.4 1.2 copy-start.11
  51.6 14.2 %collective-permute-start.22 = (bf16[64,704]{1,0:T(8,128)(2,1)S(1)}, bf16[64,704]{1,0:T(8,128)(2,1)S(1)}, u32[]{:S(2)}, u32[]{:S(2)}) collective-permute-start(bf16[64,704]{1,0:T(8,128)(2,1)S(1)} %copy-done.11), channel_id=1, source_target_pairs={{0,32},{32,64},{64,96},{96,128},{128,160},{160,192},{192,224},{224... | collective-permute-start | bytes 270344 | tf_op jit(solution)/shard_map/ppermute | solution.py:37
  60.4 50.8 %collective-permute-start.15 = (bf16[256,1408]{1,0:T(8,128)(2,1)}, bf16[256,1408]{1,0:T(8,128)(2,1)S(1)}, u32[]{:S(2)}, u32[]{:S(2)}) collective-permute-start(bf16[256,1408]{1,0:T(8,128)(2,1)} %collective-permute-done.13), channel_id=1, source_target_pairs={{0,32},{32,64},{64,96},{96,128},{128,160},{160,192},{192,224},{224... | collective-permute-start | bytes 2162696 | tf_op jit(solution)/shard_map/ppermute | solution.py:37
  61.9 51.9 %collective-permute-start.16 = (bf16[256,1408]{1,0:T(8,128)(2,1)}, bf16[256,1408]{1,0:T(8,128)(2,1)S(1)}, u32[]{:S(2)}, u32[]{:S(2)}) collective-permute-start(bf16[256,1408]{1,0:T(8,128)(2,1)} %collective-permute-done.14), channel_id=1, source_target_pairs={{0,224},{32,0},{64,32},{96,64},{128,96},{160,128},{192,160},{224,1... | collective-permute-start | bytes 2162696 | tf_op jit(solution)/shard_map/ppermute | solution.py:37
  61.9 20.3 %collective-permute-start.23 = (bf16[64,704]{1,0:T(8,128)(2,1)S(1)}, bf16[64,704]{1,0:T(8,128)(2,1)S(1)}, u32[]{:S(2)}, u32[]{:S(2)}) collective-permute-start(bf16[64,704]{1,0:T(8,128)(2,1)S(1)} %copy-done.11), channel_id=1, source_target_pairs={{0,224},{32,0},{64,32},{96,64},{128,96},{160,128},{192,160},{224,1... | collective-permute-start | bytes 270344 | tf_op jit(solution)/shard_map/ppermute | solution.py:37
  61.9 23.7 %collective-permute-start.24 = (bf16[64,704]{1,0:T(8,128)(2,1)S(1)}, bf16[64,704]{1,0:T(8,128)(2,1)S(1)}, u32[]{:S(2)}, u32[]{:S(2)}) collective-permute-start(bf16[64,704]{1,0:T(8,128)(2,1)S(1)} %copy-done.11), channel_id=1, source_target_pairs={{0,64},{32,96},{64,128},{96,160},{128,192},{160,224},{192,0},{224,... | collective-permute-start | bytes 270344 | tf_op jit(solution)/shard_map/ppermute | solution.py:37
  65.7 20.8 %collective-permute-start.25 = (bf16[64,704]{1,0:T(8,128)(2,1)S(1)}, bf16[64,704]{1,0:T(8,128)(2,1)S(1)}, u32[]{:S(2)}, u32[]{:S(2)}) collective-permute-start(bf16[64,704]{1,0:T(8,128)(2,1)S(1)} %copy-done.11), channel_id=1, source_target_pairs={{0,192},{32,224},{64,0},{96,32},{128,64},{160,96},{192,128},{224,1... | collective-permute-start | bytes 270344 | tf_op jit(solution)/shard_map/ppermute | solution.py:37
  82.2 22.4 %collective-permute-start.5 = (bf16[768,256]{1,0:T(8,128)(2,1)S(1)}, bf16[768,256]{1,0:T(8,128)(2,1)S(1)}, u32[]{:S(2)}, u32[]{:S(2)}) collective-permute-start(bf16[768,256]{1,0:T(8,128)(2,1)S(1)} %get-tuple-element.23), channel_id=1, source_target_pairs={{0,6},{2,0},{4,2},{6,4},{1,7},{3,1},{5,3},{7,5},{8,14},{10,8},{12,... | collective-permute-start | bytes 1179656 | tf_op jit(solution)/shard_map/ppermute | solution.py:297
  85.6 19.1 %collective-permute-start.4 = (bf16[768,256]{1,0:T(8,128)(2,1)S(1)}, bf16[768,256]{1,0:T(8,128)(2,1)S(1)}, u32[]{:S(2)}, u32[]{:S(2)}) collective-permute-start(bf16[768,256]{1,0:T(8,128)(2,1)S(1)} %get-tuple-element.22), channel_id=1, source_target_pairs={{0,4},{2,6},{4,0},{6,2},{1,5},{3,7},{5,1},{7,3},{8,12},{10,14},{12... | collective-permute-start | bytes 1179656 | tf_op jit(solution)/shard_map/ppermute | solution.py:297
  86.6 3.8 %collective-permute-start.26 = (bf16[64,704]{1,0:T(8,128)(2,1)S(1)}, bf16[64,704]{1,0:T(8,128)(2,1)S(1)}, u32[]{:S(2)}, u32[]{:S(2)}) collective-permute-start(bf16[64,704]{1,0:T(8,128)(2,1)S(1)} %collective-permute-done.24), channel_id=1, source_target_pairs={{0,32},{32,64},{64,96},{96,128},{128,160},{160,192},{192,224},{224... | collective-permute-start | bytes 270344 | tf_op jit(solution)/shard_map/ppermute | solution.py:37
  90.3 4.7 %collective-permute-start.27 = (bf16[64,704]{1,0:T(8,128)(2,1)S(1)}, bf16[64,704]{1,0:T(8,128)(2,1)S(1)}, u32[]{:S(2)}, u32[]{:S(2)}) collective-permute-start(bf16[64,704]{1,0:T(8,128)(2,1)S(1)} %collective-permute-done.25), channel_id=1, source_target_pairs={{0,224},{32,0},{64,32},{96,64},{128,96},{160,128},{192,160},{224,1... | collective-permute-start | bytes 270344 | tf_op jit(solution)/shard_map/ppermute | solution.py:37
  95.0 7.0 %collective-permute-start.28 = (bf16[64,704]{1,0:T(8,128)(2,1)S(1)}, bf16[64,704]{1,0:T(8,128)(2,1)S(1)}, u32[]{:S(2)}, u32[]{:S(2)}) collective-permute-start(bf16[64,704]{1,0:T(8,128)(2,1)S(1)} %broadcast_select_fusion.2), channel_id=1, source_target_pairs={{0,64},{1,193},{2,66},{3,195},{4,68},{5,197},{6,70},{7,199},{8,72}... | collective-permute-start | bytes 270344 | tf_op jit(solution)/shard_map/ppermute | solution.py:33
  102.0 7.8 %collective-permute-start.3 = (bf16[768,256]{1,0:T(8,128)(2,1)S(1)}, bf16[768,256]{1,0:T(8,128)(2,1)S(1)}, u32[]{:S(2)}, u32[]{:S(2)}) collective-permute-start(bf16[768,256]{1,0:T(8,128)(2,1)S(1)} %get-tuple-element.21), channel_id=1, source_target_pairs={{0,2},{2,4},{4,6},{6,0},{1,3},{3,5},{5,7},{7,1},{8,10},{10,12},{12... | collective-permute-start | bytes 1179656 | tf_op jit(solution)/shard_map/ppermute | solution.py:297
  104.6 38.2 %collective-permute-start.29 = (bf16[8,64,704]{2,1,0:T(8,128)(2,1)}, bf16[8,64,704]{2,1,0:T(8,128)(2,1)S(1)}, u32[]{:S(2)}, u32[]{:S(2)}) collective-permute-start(bf16[8,64,704]{2,1,0:T(8,128)(2,1)} %bitcast_dynamic-update-slice_fusion.16), channel_id=1, source_target_pairs={{0,8},{8,16},{16,24},{24,0},{1,9},{9,17},{17,25},{25,1},{2,10},{10... | collective-permute-start | bytes 2162696 | tf_op jit(solution)/shard_map/ppermute | solution.py:41
  104.7 38.1 %collective-permute-start.30 = (bf16[8,64,704]{2,1,0:T(8,128)(2,1)}, bf16[8,64,704]{2,1,0:T(8,128)(2,1)S(1)}, u32[]{:S(2)}, u32[]{:S(2)}) collective-permute-start(bf16[8,64,704]{2,1,0:T(8,128)(2,1)} %bitcast_dynamic-update-slice_fusion.16), channel_id=1, source_target_pairs={{0,24},{8,0},{16,8},{24,16},{1,25},{9,1},{17,9},{25,17},{2,26},{10... | collective-permute-start | bytes 2162696 | tf_op jit(solution)/shard_map/ppermute | solution.py:41
  111.1 14.7 %collective-permute-start.6 = (bf16[768,256]{1,0:T(8,128)(2,1)S(1)}, bf16[768,256]{1,0:T(8,128)(2,1)S(1)}, u32[]{:S(2)}, u32[]{:S(2)}) collective-permute-start(bf16[768,256]{1,0:T(8,128)(2,1)S(1)} %add_convert_fusion.2.p0), channel_id=1, source_target_pairs={{0,2},{2,4},{4,6},{6,0},{1,3},{3,5},{5,7},{7,1},{8,10},{10,12},{12... | collective-permute-start | bytes 1179656 | tf_op jit(solution)/shard_map/ppermute | solution.py:297
  111.2 14.6 %collective-permute-start.7 = (bf16[768,256]{1,0:T(8,128)(2,1)S(1)}, bf16[768,256]{1,0:T(8,128)(2,1)S(1)}, u32[]{:S(2)}, u32[]{:S(2)}) collective-permute-start(bf16[768,256]{1,0:T(8,128)(2,1)S(1)} %add_convert_fusion.2.p0), channel_id=1, source_target_pairs={{0,4},{2,6},{4,0},{6,2},{1,5},{3,7},{5,1},{7,3},{8,12},{10,14},{12... | collective-permute-start | bytes 1179656 | tf_op jit(solution)/shard_map/ppermute | solution.py:297
  113.8 29.3 %collective-permute-start.17 = (bf16[256,1408]{1,0:T(8,128)(2,1)S(1)}, bf16[256,1408]{1,0:T(8,128)(2,1)S(1)}, u32[]{:S(2)}, u32[]{:S(2)}) collective-permute-start(bf16[256,1408]{1,0:T(8,128)(2,1)S(1)} %collective-permute-done.15), channel_id=1, source_target_pairs={{0,32},{32,64},{64,96},{96,128},{128,160},{160,192},{192,224},{224... | collective-permute-start | bytes 2162696 | tf_op jit(solution)/shard_map/ppermute | solution.py:37
  125.8 17.4 %collective-permute-start.18 = (bf16[256,1408]{1,0:T(8,128)(2,1)S(1)}, bf16[256,1408]{1,0:T(8,128)(2,1)S(1)}, u32[]{:S(2)}, u32[]{:S(2)}) collective-permute-start(bf16[256,1408]{1,0:T(8,128)(2,1)S(1)} %collective-permute-done.16), channel_id=1, source_target_pairs={{0,224},{32,0},{64,32},{96,64},{128,96},{160,128},{192,160},{224,1... | collective-permute-start | bytes 2162696 | tf_op jit(solution)/shard_map/ppermute | solution.py:37
  125.8 8.9 %collective-permute-start.8 = (bf16[768,256]{1,0:T(8,128)(2,1)S(1)}, bf16[768,256]{1,0:T(8,128)(2,1)S(1)}, u32[]{:S(2)}, u32[]{:S(2)}) collective-permute-start(bf16[768,256]{1,0:T(8,128)(2,1)S(1)} %add_convert_fusion.2.p0), channel_id=1, source_target_pairs={{0,6},{2,0},{4,2},{6,4},{1,7},{3,1},{5,3},{7,5},{8,14},{10,8},{12,... | collective-permute-start | bytes 1179656 | tf_op jit(solution)/shard_map/ppermute | solution.py:297
  134.9 20.6 %collective-permute-start.9 = (bf16[4,768,256]{2,1,0:T(8,128)(2,1)S(1)}, bf16[4,768,256]{2,1,0:T(8,128)(2,1)S(1)}, u32[]{:S(2)}, u32[]{:S(2)}) collective-permute-start(bf16[4,768,256]{2,1,0:T(8,128)(2,1)S(1)} %pad_maximum_fusion), channel_id=1, source_target_pairs={{0,1},{1,0},{2,3},{3,2},{4,5},{5,4},{6,7},{7,6},{8,9},{9,8},{10,11... | collective-permute-start | bytes 4718600 | tf_op jit(solution)/shard_map/ppermute | solution.py:45
  142.8 12.3 %collective-permute-start.31 = (bf16[8,64,704]{2,1,0:T(8,128)(2,1)S(1)}, bf16[8,64,704]{2,1,0:T(8,128)(2,1)S(1)}, u32[]{:S(2)}, u32[]{:S(2)}) collective-permute-start(bf16[8,64,704]{2,1,0:T(8,128)(2,1)S(1)} %broadcast_select_fusion), channel_id=1, source_target_pairs={{0,8},{1,25},{2,10},{3,27},{4,12},{5,29},{6,14},{7,31},{8,16},{9,1... | collective-permute-start | bytes 2162696 | tf_op jit(solution)/shard_map/ppermute | solution.py:33
  143.3 16.6 %collective-permute-start.19 = (bf16[256,1408]{1,0:T(8,128)(2,1)S(1)}, bf16[256,1408]{1,0:T(8,128)(2,1)S(1)}, u32[]{:S(2)}, u32[]{:S(2)}) collective-permute-start(bf16[256,1408]{1,0:T(8,128)(2,1)S(1)} %broadcast_select_fusion.1), channel_id=1, source_target_pairs={{0,32},{1,225},{2,34},{3,227},{4,36},{5,229},{6,38},{7,231},{8,40}... | collective-permute-start | bytes 2162696 | tf_op jit(solution)/shard_map/ppermute | solution.py:33
  155.5 0.7 copy-start.5
  163.0 13.0 %collective-permute-start.20 = (bf16[1,704]{1,0:T(2,128)(2,1)S(1)}, bf16[1,704]{1,0:T(2,128)(2,1)S(1)}, u32[]{:S(2)}, u32[]{:S(2)}) collective-permute-start(bf16[1,704]{1,0:T(2,128)(2,1)S(1)} %get-tuple-element.45), channel_id=1, source_target_pairs={{0,8},{8,16},{16,24},{24,32},{32,40},{40,48},{48,56},{56,64},{64,7... | collective-permute-start | bytes 4232 | tf_op jit(solution)/shard_map/ppermute | solution.py:411
  171.1 7.7 %copy-start.6 = (bf16[3,704]{1,0:T(4,128)(2,1)S(1)}, bf16[3,704]{1,0:T(4,128)(2,1)}, u32[]{:S(2)}) copy-start(bf16[3,704]{1,0:T(4,128)(2,1)} %taps_ref.1) | copy-start | bytes 12676
  171.1 7.7 %collective-permute-start.21 = (bf16[1,704]{1,0:T(2,128)(2,1)S(1)}, bf16[1,704]{1,0:T(2,128)(2,1)S(1)}, u32[]{:S(2)}, u32[]{:S(2)}) collective-permute-start(bf16[1,704]{1,0:T(2,128)(2,1)S(1)} %get-tuple-element.44), channel_id=1, source_target_pairs={{8,0},{16,8},{24,16},{32,24},{40,32},{48,40},{56,48},{64,56},{72,6... | collective-permute-start | bytes 4232 | tf_op jit(solution)/shard_map/ppermute | solution.py:412
  187.4 5.9 %collective-permute-start.32 = (bf16[768,1024]{1,0:T(8,128)(2,1)S(1)}, bf16[768,1024]{1,0:T(8,128)(2,1)S(1)}, u32[]{:S(2)}, u32[]{:S(2)}) collective-permute-start(bf16[768,1024]{1,0:T(8,128)(2,1)S(1)} %convolution_convert_fusion), channel_id=1, source_target_pairs={{0,1},{1,0},{2,3},{3,2},{4,5},{5,4},{6,7},{7,6},{8,9},{9,8},{10,11... | collective-permute-start | bytes 4718600 | tf_op jit(solution)/shard_map/ppermute | solution.py:45
  194.8 10.4 %collective-permute-start.35 = (bf16[768,256]{1,0:T(8,128)(2,1)S(1)}, bf16[768,256]{1,0:T(8,128)(2,1)S(1)}, u32[]{:S(2)}, u32[]{:S(2)}) collective-permute-start(bf16[768,256]{1,0:T(8,128)(2,1)S(1)} %get-tuple-element.42), channel_id=1, source_target_pairs={{0,6},{2,0},{4,2},{6,4},{1,7},{3,1},{5,3},{7,5},{8,14},{10,8},{12,... | collective-permute-start | bytes 1179656 | tf_op jit(solution)/shard_map/ppermute | solution.py:297
  195.9 11.6 %collective-permute-start.34 = (bf16[768,256]{1,0:T(8,128)(2,1)S(1)}, bf16[768,256]{1,0:T(8,128)(2,1)S(1)}, u32[]{:S(2)}, u32[]{:S(2)}) collective-permute-start(bf16[768,256]{1,0:T(8,128)(2,1)S(1)} %get-tuple-element.43), channel_id=1, source_target_pairs={{0,4},{2,6},{4,0},{6,2},{1,5},{3,7},{5,1},{7,3},{8,12},{10,14},{12... | collective-permute-start | bytes 1179656 | tf_op jit(solution)/shard_map/ppermute | solution.py:297
  195.9 20.6 %collective-permute-start.33 = (bf16[768,256]{1,0:T(8,128)(2,1)S(1)}, bf16[768,256]{1,0:T(8,128)(2,1)S(1)}, u32[]{:S(2)}, u32[]{:S(2)}) collective-permute-start(bf16[768,256]{1,0:T(8,128)(2,1)S(1)} %get-tuple-element.41), channel_id=1, source_target_pairs={{0,2},{2,4},{4,6},{6,0},{1,3},{3,5},{5,7},{7,1},{8,10},{10,12},{12... | collective-permute-start | bytes 1179656 | tf_op jit(solution)/shard_map/ppermute | solution.py:297

commit v2 on v1

--- a/solution.py
+++ b/solution.py
@@ -56,17 +56,27 @@
 
 
 def attention_kernel(
-    at_ref, sink_ref, q_ref, kt_ref, vt_ref, lab_ref, low_ref, high_ref, w_ref,
-    att_ref, theirs_ref, kx_ref, vx_ref, row_ref, col_ref,
+    at_ref, sink_ref, q_hbm, w_hbm, packed_ref, low_ref, high_ref,
+    theirs_ref, mine_ref,
+    q_ref, w_ref, att_ref, kx_ref, vx_ref, row_ref, col_ref, sems,
 ):
+    copies = [
+        pltpu.make_async_copy(source, target, sems.at[i])
+        for i, (source, target) in enumerate(
+            ((q_hbm, q_ref), (w_hbm, w_ref))
+        )
+    ]
+    for copy in copies:
+        copy.start()
     rows = q_ref.shape[0]
     heads = q_ref.shape[1] // HEAD_DIM
     span = theirs_ref.shape[2]
     kx_ref[...] = jnp.zeros_like(kx_ref)
     vx_ref[...] = jnp.zeros_like(vx_ref)
+    copies[0].wait()
     pieces = (
         (0, WINDOW, low_ref[:HEAD_DIM], low_ref[HEAD_DIM : 2 * HEAD_DIM]),
-        (WINDOW, rows, kt_ref[...], vt_ref[...]),
+        (WINDOW, rows, packed_ref[:HEAD_DIM], packed_ref[HEAD_DIM : 2 * HEAD_DIM]),
         (WINDOW + rows, WINDOW, high_ref[:HEAD_DIM], high_ref[HEAD_DIM : 2 * HEAD_DIM]),
     )
     for start, width, keys, vals in pieces:
@@ -77,7 +87,9 @@
     row_ref[:, :WINDOW] = jnp.broadcast_to(
         low_ref[2 * HEAD_DIM :].astype(jnp.float32), (8, WINDOW)
     )
-    row_ref[:, WINDOW : WINDOW + rows] = jnp.broadcast_to(lab_ref[...], (8, rows))
+    row_ref[:, WINDOW : WINDOW + rows] = jnp.broadcast_to(
+        packed_ref[2 * HEAD_DIM :].astype(jnp.float32), (8, rows)
+    )
     row_ref[:, WINDOW + rows :] = jnp.broadcast_to(
         high_ref[2 * HEAD_DIM :].astype(jnp.float32), (8, WINDOW)
     )
@@ -113,11 +125,14 @@
         return carry
 
     lax.fori_loop(0, rows // WINDOW, step, 0)
+    copies[1].wait()
     for k in range(NY):
         cols = pl.ds(pl.multiple_of(at_ref[NY + k] * span, span), span)
         theirs_ref[k] = jnp.dot(
             att_ref[...], w_ref[:, cols], preferred_element_type=jnp.float32
         ).astype(jnp.bfloat16)
+        cols = pl.ds(pl.multiple_of(at_ref[k] * span, span), span)
+        mine_ref[k] = jnp.dot(att_ref[...], w_ref[:, cols], preferred_element_type=jnp.float32)
 
 
 def vmem_specs(count):
@@ -128,7 +143,7 @@
     return [pl.BlockSpec(memory_space=pltpu.SMEM)] * count
 
 
-def attention(order, sink, queries, keys_t, vals_t, labels, low, high, w_out):
+def attention(order, sink, queries, packed, low, high, w_out):
     rows, cols = queries.shape
     span = w_out.shape[1] // (NY * NC)
     reach = rows + 2 * WINDOW
@@ -136,43 +151,42 @@
     return pl.pallas_call(
         attention_kernel,
         out_shape=[
-            jax.ShapeDtypeStruct((rows, cols), jnp.bfloat16),
             jax.ShapeDtypeStruct((NY, rows, span), jnp.bfloat16),
+            jax.ShapeDtypeStruct((NY, rows, span), jnp.float32),
         ],
-        in_specs=smem_specs(2) + vmem_specs(7),
+        in_specs=smem_specs(2) + [pl.BlockSpec(memory_space=pltpu.HBM)] * 2 + vmem_specs(3),
         out_specs=vmem_specs(2),
         scratch_shapes=[
+            pltpu.VMEM((rows, cols), jnp.bfloat16),
+            pltpu.VMEM(w_out.shape, jnp.bfloat16),
+            pltpu.VMEM((rows, cols), jnp.bfloat16),
             pltpu.VMEM((heads, cols, reach), jnp.bfloat16),
             pltpu.VMEM((heads, reach, cols), jnp.bfloat16),
             pltpu.VMEM((8, reach), jnp.float32),
             pltpu.VMEM((rows, WINDOW), jnp.float32),
+            pltpu.SemaphoreType.DMA((2,)),
         ],
         compiler_params=pltpu.CompilerParams(vmem_limit_bytes=12 * MB),
         cost_estimate=pl.CostEstimate(flops=4 * 10**9, bytes_accessed=4 * MB, transcendentals=0),
         name="attention",
-    )(order, sink, queries, keys_t, vals_t, labels, low, high, w_out)
-
-
-def pair_kernel(at_ref, left_ref, w_ref, got_ref, s0, s1, s2, s3):
-    span = s0.shape[1]
+    )(order, sink, queries, w_out, packed, low, high)
+
+
+def pair_kernel(mine_ref, got_ref, s0, s1, s2, s3):
     for k, out in enumerate((s0, s1, s2, s3)):
-        cols = pl.ds(pl.multiple_of(at_ref[k] * span, span), span)
-        out[...] = (
-            jnp.dot(left_ref[...], w_ref[:, cols], preferred_element_type=jnp.float32)
-            + got_ref[k].astype(jnp.float32)
-        ).astype(jnp.bfloat16)
-
-
-def pair_sums(order, left, w_out, got):
+        out[...] = (mine_ref[k] + got_ref[k].astype(jnp.float32)).astype(jnp.bfloat16)
+
+
+def pair_sums(mine, got):
     return pl.pallas_call(
         pair_kernel,
         out_shape=[jax.ShapeDtypeStruct(got.shape[1:], jnp.bfloat16)] * NY,
-        in_specs=smem_specs(1) + vmem_specs(3),
+        in_specs=vmem_specs(2),
         out_specs=vmem_specs(NY),
         compiler_params=pltpu.CompilerParams(vmem_limit_bytes=8 * MB),
         cost_estimate=pl.CostEstimate(flops=10**9, bytes_accessed=4 * MB, transcendentals=0),
         name="pair_sums",
-    )(order, left, w_out, got)
+    )(mine, got)
 
 
 def norm_kernel(at_ref, p0, p1, p2, p3, rest_ref, gain_ref, out_ref):
@@ -235,7 +249,7 @@
     rows, ff = out_ref.shape
     tail = gate_ref.shape[1]
     width = value_ref.shape[1]
-    chunk = 64
+    chunk = 256
     count = rows // chunk
     row = lax.broadcasted_iota(jnp.int32, (chunk, 128), 0)
 
@@ -337,21 +351,7 @@
         [w_gate_up[:, :tail], first, w_gate_up[:, tail:]], axis=1
     )
     rows_w, width = share.shape
-    gathered = []
-    for k in range(1, NX):
-        gathered.append(send_x(share, k))
-
-    attended, theirs = attention(
-        order, sink_logits, queries, keys_t, vals_t, labels, low, high, w_out
-    )
-    got = swap(theirs)
-
-    gathered = lax.optimization_barrier((*gathered, theirs))[:-1]
-    block = put(jnp.zeros((NX, rows_w, width), share.dtype), share, x)
-    for k, piece in enumerate(gathered):
-        block = put(block, piece, (x - k - 1) % NX)
-    block = block.reshape(NX * rows_w, width)
-    full = put(jnp.zeros((NZ, NX * rows_w, width), share.dtype), block, z)
+    up_rows = lax.all_gather(share, "x", axis=0, tiled=True)
 
     def ring_step(plus, minus):
         plus = send_z(plus, 1)
@@ -361,9 +361,12 @@
     def keep(full, plus, minus, k):
         return put(put(full, plus, (z - k) % NZ), minus, (z + k) % NZ)
 
-    plus1, minus1 = ring_step(block, block)
-
-    pairs = pair_sums(order, attended, w_out, got)
+    plus1, minus1 = ring_step(up_rows, up_rows)
+
+    theirs, mine = attention(order, sink_logits, queries, packed, low, high, w_out)
+    got = swap(theirs)
+
+    pairs = pair_sums(mine, got)
     sent = to_owners(pairs)
 
     down1 = after(w_down_t, pairs[0])
@@ -374,11 +377,7 @@
     plus2, minus2 = ring_step(plus1, minus1)
     third = ring_step(far_plus, far_minus)
     last = send_apart(jnp.where(core == 0, far_plus, far_minus), 2, 0)
-    whole = put(jnp.zeros((NZ,) + w_down_t.shape, w_down_t.dtype), w_down_t, z)
-    whole = keep(whole, *near, 1)
-    whole = keep(whole, far_plus, far_minus, 2)
-    whole = keep(whole, *third, 3)
-    whole = put(whole, last, (z + NZ // 2) % NZ)
+    last_down = last
 
     own_res = lax.dynamic_slice_in_dim(residual, tp * span, span, 1)
     total = own_res.astype(jnp.float32)
@@ -387,30 +386,42 @@
         summed = summed + block.astype(jnp.float32)
     mixed_own = (total + summed).astype(jnp.bfloat16)
 
-    parts = [mixed_own] + to_owners([mixed_own] * NY)
+    came = to_owners([mixed_own] * NY)
+    came = lax.optimization_barrier((*came, plus2, minus2))[: NY - 1]
+    parts = [mixed_own, *came]
     plus3, minus3 = ring_step(plus2, minus2)
-    full = keep(after(full, mixed_own), plus1, minus1, 1)
+    full = put(jnp.zeros((NZ,) + up_rows.shape, share.dtype), after(up_rows, mixed_own), z)
+    full = keep(full, plus1, minus1, 1)
+    whole = jnp.zeros((NZ,) + w_down_t.shape, w_down_t.dtype)
+    whole = put(whole, after(w_down_t, mixed_own), z)
+    whole = keep(whole, *near, 1)
+    whole = keep(whole, far_plus, far_minus, 2)
+    whole = keep(whole, *third, 3)
+    whole = put(whole, last_down, (z + NZ // 2) % NZ)
     whole_plus = send_x(whole, 1)
     whole_minus = send_x(whole, -1)
 
-    rest = swap(jnp.stack(parts))
+    stacked = jnp.stack(parts)
+    rest = swap(stacked)
     last = send_apart(jnp.where(core == 0, plus3, minus3), 1, 0)
-    full = keep(after(full, rest), plus2, minus2, 2)
+    normed = normalised(order, parts, rest, norm_gain[None])
+    full = keep(after(full, normed), plus2, minus2, 2)
     full = keep(full, plus3, minus3, 3)
     full = put(full, last, (z + NZ // 2) % NZ).reshape(model_width, width)
 
+    whole_plus, whole_minus = lax.optimization_barrier((whole_plus, whole_minus, normed))[:2]
     whole_far = send_apart(jnp.where(core == 0, whole_plus, whole_minus), 0, 1)
     full_down = jnp.zeros((NZ, NX, rows_w, ff), w_down_t.dtype)
-    full_down = put(full_down, whole[:, None], 0, x)
+    full_down = put(full_down, after(whole, normed)[:, None], 0, x)
     full_down = put(full_down, whole_plus[:, None], 0, (x - 1) % NX)
     full_down = put(full_down, whole_minus[:, None], 0, (x + 1) % NX)
     full_down = put(full_down, whole_far[:, None], 0, (x + 2) % NX).reshape(model_width, ff)
 
-    normed = normalised(order, parts, rest, norm_gain[None])
     up_value = up(normed, full, tail, width - tail)
     before = lax.ppermute(up_value[-1:, :ff], ("z", "x"), forward)
     behind = lax.ppermute(up_value[:1, :ff], ("z", "x"), backward)
     up_gate = up(normed, full, 0, tail)
+    low, packed, high = lax.optimization_barrier((low, packed, high, pairs[0]))[:3]
     edge = jnp.concatenate([low[-1:, -1:], packed[-1:], high[-1:, :1]], axis=1)[0]
     same = jnp.stack([edge[:-2] == edge[1:-1], edge[2:] == edge[1:-1]], axis=1)
     same = same.astype(jnp.float32)

time: 219 us -> 188 us (0.86)
  the two profiles are of different devices: /device:TPU:103 before, /device:TPU:129 now
where the time goes in v2:
time: 188 us; the launch traced here: 187 us
  starting transfers between devices  64.5 us (34%)
  waiting for transfers between devices  62.7 us (33%)
  Pallas kernels  23.5 us (12%)
  local copies, waits for them, and re-layouts  15.1 us (8%)
  blocking collectives  12.2 us (6%)
  other arithmetic  5.58 us (3%)
  matrix products  2.88 us (2%)
    ppermute x9, waiting for transfers between devices, to_owners(): lax.ppermute(pairs[k], 'y', [(y, (y + k) % NY) for y in range(NY)])  25 us
    ppermute x12, waiting for transfers between devices, send_z(): return lax.ppermute(block, 'z', [(z, (z + k) % NZ) for z in range(NZ)])  19.3 us
    ppermute x12, starting transfers between devices, send_z(): return lax.ppermute(block, 'z', [(z, (z + k) % NZ) for z in range(NZ)])  18.7 us
    ppermute x3, starting transfers between devices, swap(): return lax.ppermute(block, 'core', [(0, 1), (1, 0)])  15.1 us
    ppermute x3, waiting for transfers between devices, send_apart(): return lax.ppermute(block, AXES, pairs)  14.6 us
    ppermute x9, starting transfers between devices, to_owners(): lax.ppermute(pairs[k], 'y', [(y, (y + k) % NY) for y in range(NY)])  12.8 us
    all_gather x1, blocking collectives, per_device(): up_rows = lax.all_gather(share, 'x', axis=0, tiled=True)  12.2 us
    pallas_call x1, Pallas kernels, attention(): pl.pallas_call(attention_kernel, out_shape=[jax.ShapeDtypeStruct((NY, row...  9.34 us
  transfers between devices with their start and end apart: 33, of which 12 were waited for; matrix products, arithmetic and copies ran while one was open for 8% of the time, Pallas kernels for 8%

profile of v2, /device:TPU:129, one launch (start us, length us, event | category | flops | bytes accessed | tf_op | source)
XLA Modules:
  0.0 187.1 jit_solution(18348082704329641399)
XLA Ops:
  1.7 3.1 %collective-permute-start = (bf16[129,128]{1,0:T(8,128)(2,1)S(1)}, bf16[129,128]{1,0:T(8,128)(2,1)S(1)}, u32[]{:S(2)}, u32[]{:S(2)}) collective-permute-start(bf16[129,128]{1,0:T(8,128)(2,1)S(1)} %get-tuple-element.59), channel_id=1, source_target_pairs={{0,8},{8,16},{16,24},{24,32},{32,40},{40,48},{48,56},{56,64},{64,7... | collective-permute-start | bytes 99080 | tf_op jit(solution)/shard_map/ppermute | solution.py:345
  4.8 5.5 %collective-permute-start.1 = (bf16[129,128]{1,0:T(8,128)(2,1)S(1)}, bf16[129,128]{1,0:T(8,128)(2,1)S(1)}, u32[]{:S(2)}, u32[]{:S(2)}) collective-permute-start(bf16[129,128]{1,0:T(8,128)(2,1)S(1)} %get-tuple-element.58), channel_id=1, source_target_pairs={{8,0},{16,8},{24,16},{32,24},{40,32},{48,40},{56,48},{64,56},{72,6... | collective-permute-start | bytes 99080 | tf_op jit(solution)/shard_map/ppermute | solution.py:346
  11.3 1.2 copy-done.1
  14.2 9.3 %attention.1 = (bf16[4,768,256]{2,1,0:T(8,128)(2,1)}, f32[4,768,256]{2,1,0:T(8,128)S(1)}) custom-call(s32[16]{0:T(128)S(1)} %stack.81.at_ref, f32[4]{0:T(128)S(1)} %copy-done.7, bf16[768,256]{1,0:T(8,128)(2,1)S(1)} %copy-done.2, bf16[256,2048]{1,0:T(8,128)(2,1)S(1)} %copy-done.1, bf16[129,768]{1,0:T(8,128)(2,1)S(1)} %pad_maximum_fusion.1.packed_ref, ...), custom_call_target="tpu_custom_call" | custom-call | flops 4000000000 | bytes 4194304 | tf_op jit(solution)/shard_map/attention/pallas_call | solution.py:151
  23.6 1.9 %collective-permute-start.2 = (bf16[4,768,256]{2,1,0:T(8,128)(2,1)}, bf16[4,768,256]{2,1,0:T(8,128)(2,1)}, u32[]{:S(2)}, u32[]{:S(2)}) collective-permute-start(bf16[4,768,256]{2,1,0:T(8,128)(2,1)} %get-tuple-element.26), channel_id=1, source_target_pairs={{0,1},{1,0},{2,3},{3,2},{4,5},{5,4},{6,7},{7,6},{8,9},{9,8},{10,11... | collective-permute-start | bytes 4718600 | tf_op jit(solution)/shard_map/ppermute | solution.py:45
  26.5 12.2 %all_gather.3 = bf16[256,1408]{1,0:T(8,128)(2,1)} all-gather(bf16[64,1408]{1,0:T(8,128)(2,1)S(1)} %concatenate.20), channel_id=1, replica_groups=mesh['z'=8,'x'=4,'y'=4,'core'=2] {'x'}, dimensions={0}, use_global_device_ids=true | all-gather | bytes 901120 | tf_op jit(solution)/shard_map/all_gather | solution.py:354
  38.7 1.3 collective-permute-start.9
  40.0 2.4 %collective-permute-start.11 = (bf16[256,1408]{1,0:T(8,128)(2,1)}, bf16[256,1408]{1,0:T(8,128)(2,1)}, u32[]{:S(2)}, u32[]{:S(2)}) collective-permute-start(bf16[256,1408]{1,0:T(8,128)(2,1)} %all_gather.3), channel_id=1, source_target_pairs={{0,224},{32,0},{64,32},{96,64},{128,96},{160,128},{192,160},{224,1... | collective-permute-start | bytes 2162696 | tf_op jit(solution)/shard_map/ppermute | solution.py:37
  42.5 2.6 %pair_sums.1 = (bf16[768,256]{1,0:T(8,128)(2,1)S(1)}, bf16[768,256]{1,0:T(8,128)(2,1)}, bf16[768,256]{1,0:T(8,128)(2,1)}, bf16[768,256]{1,0:T(8,128)(2,1)}) custom-call(f32[4,768,256]{2,1,0:T(8,128)S(1)} %get-tuple-element.25.mine_ref, bf16[4,768,256]{2,1,0:T(8,128)(2,1)} %collective-permute-done.2.got_ref), custom_call_target="tpu_custom_call" | custom-call | flops 1000000000 | bytes 4194304 | tf_op jit(solution)/shard_map/pair_sums/pallas_call | solution.py:181
  45.1 2.7 %collective-permute-start.5 = (bf16[768,256]{1,0:T(8,128)(2,1)}, bf16[768,256]{1,0:T(8,128)(2,1)S(1)}, u32[]{:S(2)}, u32[]{:S(2)}) collective-permute-start(bf16[768,256]{1,0:T(8,128)(2,1)} %get-tuple-element.30), channel_id=1, source_target_pairs={{0,6},{2,0},{4,2},{6,4},{1,7},{3,1},{5,3},{7,5},{8,14},{10,8},{12,... | collective-permute-start | bytes 1179656 | tf_op jit(solution)/shard_map/ppermute | solution.py:311
  49.6 1.2 slice.56
  50.8 1.2 slice.59
  52.0 1.3 compare_bitcast_fusion.1
  53.2 4.6 %collective-permute-done.9 = bf16[256,1408]{1,0:T(8,128)(2,1)} collective-permute-done((bf16[256,1408]{1,0:T(8,128)(2,1)}, bf16[256,1408]{1,0:T(8,128)(2,1)}, u32[]{:S(2)}, u32[]{:S(2)}) %collective-permute-start.9) | collective-permute-done | bytes 720928 | tf_op jit(solution)/shard_map/ppermute | solution.py:37
  57.8 3.6 %collective-permute-start.22 = (bf16[64,704]{1,0:T(8,128)(2,1)}, bf16[64,704]{1,0:T(8,128)(2,1)S(1)}, u32[]{:S(2)}, u32[]{:S(2)}) collective-permute-start(bf16[64,704]{1,0:T(8,128)(2,1)} %param.23), channel_id=1, source_target_pairs={{0,192},{32,224},{64,0},{96,32},{128,64},{160,96},{192,128},{224,1... | collective-permute-start | bytes 270344 | tf_op jit(solution)/shard_map/ppermute | solution.py:37
  61.6 3.0 %collective-permute-done.21 = bf16[64,704]{1,0:T(8,128)(2,1)} collective-permute-done((bf16[64,704]{1,0:T(8,128)(2,1)}, bf16[64,704]{1,0:T(8,128)(2,1)}, u32[]{:S(2)}, u32[]{:S(2)}) %collective-permute-start.21) | collective-permute-done | bytes 90144 | tf_op jit(solution)/shard_map/ppermute | solution.py:37
  64.6 2.7 %collective-permute-start.12 = (bf16[256,1408]{1,0:T(8,128)(2,1)}, bf16[256,1408]{1,0:T(8,128)(2,1)S(1)}, u32[]{:S(2)}, u32[]{:S(2)}) collective-permute-start(bf16[256,1408]{1,0:T(8,128)(2,1)} %collective-permute-done.11), channel_id=1, source_target_pairs={{0,224},{32,0},{64,32},{96,64},{128,96},{160,128},{192,160},{224,1... | collective-permute-start | bytes 2162696 | tf_op jit(solution)/shard_map/ppermute | solution.py:37
  67.4 2.7 %collective-permute-start.20 = (bf16[64,704]{1,0:T(8,128)(2,1)}, bf16[64,704]{1,0:T(8,128)(2,1)S(1)}, u32[]{:S(2)}, u32[]{:S(2)}) collective-permute-start(bf16[64,704]{1,0:T(8,128)(2,1)} %param.23), channel_id=1, source_target_pairs={{0,224},{32,0},{64,32},{96,64},{128,96},{160,128},{192,160},{224,1... | collective-permute-start | bytes 270344 | tf_op jit(solution)/shard_map/ppermute | solution.py:37
  70.2 1.2 add_convert_fusion.2.p0
  72.4 9.3 %collective-permute-done.19 = bf16[64,704]{1,0:T(8,128)(2,1)S(1)} collective-permute-done((bf16[64,704]{1,0:T(8,128)(2,1)}, bf16[64,704]{1,0:T(8,128)(2,1)S(1)}, u32[]{:S(2)}, u32[]{:S(2)}) %collective-permute-start.19) | collective-permute-done | bytes 90144 | tf_op jit(solution)/shard_map/ppermute | solution.py:37
  81.7 3.3 %collective-permute-start.24 = (bf16[64,704]{1,0:T(8,128)(2,1)S(1)}, bf16[64,704]{1,0:T(8,128)(2,1)S(1)}, u32[]{:S(2)}, u32[]{:S(2)}) collective-permute-start(bf16[64,704]{1,0:T(8,128)(2,1)S(1)} %collective-permute-done.22), channel_id=1, source_target_pairs={{0,224},{32,0},{64,32},{96,64},{128,96},{160,128},{192,160},{224,1... | collective-permute-start | bytes 270344 | tf_op jit(solution)/shard_map/ppermute | solution.py:37
  85.9 2.4 %collective-permute-done.23 = bf16[64,704]{1,0:T(8,128)(2,1)S(1)} collective-permute-done((bf16[64,704]{1,0:T(8,128)(2,1)}, bf16[64,704]{1,0:T(8,128)(2,1)S(1)}, u32[]{:S(2)}, u32[]{:S(2)}) %collective-permute-start.23) | collective-permute-done | bytes 90144 | tf_op jit(solution)/shard_map/ppermute | solution.py:37
  88.3 1.3 collective-permute-start.6
  89.6 2.7 %collective-permute-start.7 = (bf16[768,256]{1,0:T(8,128)(2,1)S(1)}, bf16[768,256]{1,0:T(8,128)(2,1)S(1)}, u32[]{:S(2)}, u32[]{:S(2)}) collective-permute-start(bf16[768,256]{1,0:T(8,128)(2,1)S(1)} %add_convert_fusion.2.p0), channel_id=1, source_target_pairs={{0,4},{2,6},{4,0},{6,2},{1,5},{3,7},{5,1},{7,3},{8,12},{10,14},{12... | collective-permute-start | bytes 1179656 | tf_op jit(solution)/shard_map/ppermute | solution.py:311
  92.3 1.1 collective-permute-start.8
  93.5 2.7 %collective-permute-start.15 = (bf16[256,1408]{1,0:T(8,128)(2,1)S(1)}, bf16[256,1408]{1,0:T(8,128)(2,1)S(1)}, u32[]{:S(2)}, u32[]{:S(2)}) collective-permute-start(bf16[256,1408]{1,0:T(8,128)(2,1)S(1)} %collective-permute-done.12), channel_id=1, source_target_pairs={{0,224},{32,0},{64,32},{96,64},{128,96},{160,128},{192,160},{224,1... | collective-permute-start | bytes 2162696 | tf_op jit(solution)/shard_map/ppermute | solution.py:37
  96.3 6.8 %collective-permute-done.7.p2 = bf16[768,256]{1,0:T(8,128)(2,1)S(1)} collective-permute-done((bf16[768,256]{1,0:T(8,128)(2,1)S(1)}, bf16[768,256]{1,0:T(8,128)(2,1)S(1)}, u32[]{:S(2)}, u32[]{:S(2)}) %collective-permute-start.7) | collective-permute-done | bytes 393248 | tf_op jit(solution)/shard_map/ppermute | solution.py:311
  103.3 8.4 %collective-permute-start.13 = (bf16[4,768,256]{2,1,0:T(8,128)(2,1)S(1)}, bf16[4,768,256]{2,1,0:T(8,128)(2,1)S(1)}, u32[]{:S(2)}, u32[]{:S(2)}) collective-permute-start(bf16[4,768,256]{2,1,0:T(8,128)(2,1)S(1)} %pad_maximum_fusion), channel_id=1, source_target_pairs={{0,1},{1,0},{2,3},{3,2},{4,5},{5,4},{6,7},{7,6},{8,9},{9,8},{10,11... | collective-permute-start | bytes 4718600 | tf_op jit(solution)/shard_map/ppermute | solution.py:45
  112.2 1.2 bitcast_dynamic-update-slice_fusion.11
  113.4 1.2 bitcast_dynamic-update-slice_fusion.10
  114.6 1.2 bitcast_dynamic-update-slice_fusion.9
  116.0 2.6 %normalise.1.left_ref = bf16[768,2048]{1,0:T(8,128)(2,1)S(1)} custom-call(s32[16]{0:T(128)S(1)} %stack.81.at_ref, bf16[768,256]{1,0:T(8,128)(2,1)S(1)} %add_convert_fusion.2.p0, bf16[768,256]{1,0:T(8,128)(2,1)S(1)} %collective-permute-done.6.p1, bf16[768,256]{1,0:T(8,128)(2,1)S(1)} %collective-permute-done.7.p2, ...), custom_call_target="tpu_custom_call" | custom-call | flops 2000000000 | bytes 6291456 | tf_op jit(solution)/shard_map/normalise/pallas_call | solution.py:213
  119.0 7.4 %collective-permute-done.16 = bf16[256,1408]{1,0:T(8,128)(2,1)S(1)} collective-permute-done((bf16[256,1408]{1,0:T(8,128)(2,1)S(1)}, bf16[256,1408]{1,0:T(8,128)(2,1)S(1)}, u32[]{:S(2)}, u32[]{:S(2)}) %collective-permute-start.16) | collective-permute-done | bytes 720928 | tf_op jit(solution)/shard_map/ppermute | solution.py:33
  126.5 3.0 %shard_map.118.value_ref = bf16[768,768]{1,0:T(8,128)(2,1)S(1)} custom-call(bf16[768,2048]{1,0:T(8,128)(2,1)S(1)} %normalise.1.left_ref, bf16[2048,1408]{1,0:T(8,128)(2,1)S(1)} %bitcast.75), custom_call_target="tpu_custom_call" | custom-call | flops 3000000000 | bytes 8388608 | tf_op jit(solution)/shard_map/pallas_call | solution.py:238
  129.6 2.9 %collective-permute-start.17 = (bf16[1,704]{1,0:T(2,128)(2,1)S(1)}, bf16[1,704]{1,0:T(2,128)(2,1)S(1)}, u32[]{:S(2)}, u32[]{:S(2)}) collective-permute-start(bf16[1,704]{1,0:T(2,128)(2,1)S(1)} %get-tuple-element.57), channel_id=1, source_target_pairs={{0,8},{8,16},{16,24},{24,32},{32,40},{40,48},{48,56},{56,64},{64,7... | collective-permute-start | bytes 4232 | tf_op jit(solution)/shard_map/ppermute | solution.py:421
  132.4 6.0 %collective-permute-start.18 = (bf16[1,704]{1,0:T(2,128)(2,1)S(1)}, bf16[1,704]{1,0:T(2,128)(2,1)S(1)}, u32[]{:S(2)}, u32[]{:S(2)}) collective-permute-start(bf16[1,704]{1,0:T(2,128)(2,1)S(1)} %get-tuple-element.56), channel_id=1, source_target_pairs={{8,0},{16,8},{24,16},{32,24},{40,32},{48,40},{56,48},{64,56},{72,6... | collective-permute-start | bytes 4232 | tf_op jit(solution)/shard_map/ppermute | solution.py:422
  138.4 3.0 %shard_map.119.gate_ref = bf16[768,640]{1,0:T(8,128)(2,1)S(1)} custom-call(bf16[768,2048]{1,0:T(8,128)(2,1)S(1)} %normalise.1.left_ref, bf16[2048,1408]{1,0:T(8,128)(2,1)S(1)} %bitcast.76), custom_call_target="tpu_custom_call" | custom-call | flops 3000000000 | bytes 8388608 | tf_op jit(solution)/shard_map/pallas_call | solution.py:238
  142.7 2.9 %hidden_units.1 = bf16[768,704]{1,0:T(8,128)(2,1)S(1)} custom-call(bf16[768,768]{1,0:T(8,128)(2,1)S(1)} %shard_map.118.value_ref, bf16[768,640]{1,0:T(8,128)(2,1)S(1)} %shard_map.119.gate_ref, f32[768,2]{1,0:T(8,128)S(1)} %copy.22.same_ref, bf16[1,704]{1,0:T(2,128)(2,1)S(1)} %collective-permute-done.17.before_ref, ...), custom_call_target="tpu_custom_call" | custom-call | flops 2000000000 | bytes 4194304 | tf_op jit(solution)/shard_map/hidden_units/pallas_call | solution.py:297
  145.6 7.2 %collective-permute-done.28 = bf16[8,64,704]{2,1,0:T(8,128)(2,1)S(1)} collective-permute-done((bf16[8,64,704]{2,1,0:T(8,128)(2,1)S(1)}, bf16[8,64,704]{2,1,0:T(8,128)(2,1)S(1)}, u32[]{:S(2)}, u32[]{:S(2)}) %collective-permute-start.28) | collective-permute-done | bytes 720928 | tf_op jit(solution)/shard_map/ppermute | solution.py:33
  153.1 1.4 convolution_convert_fusion
  154.5 4.8 %collective-permute-start.29 = (bf16[768,1024]{1,0:T(8,128)(2,1)S(1)}, bf16[768,1024]{1,0:T(8,128)(2,1)S(1)}, u32[]{:S(2)}, u32[]{:S(2)}) collective-permute-start(bf16[768,1024]{1,0:T(8,128)(2,1)S(1)} %convolution_convert_fusion), channel_id=1, source_target_pairs={{0,1},{1,0},{2,3},{3,2},{4,5},{5,4},{6,7},{7,6},{8,9},{9,8},{10,11... | collective-permute-start | bytes 4718600 | tf_op jit(solution)/shard_map/ppermute | solution.py:45
  159.3 3.0 %collective-permute-done.29 = bf16[768,1024]{1,0:T(8,128)(2,1)S(1)} collective-permute-done((bf16[768,1024]{1,0:T(8,128)(2,1)S(1)}, bf16[768,1024]{1,0:T(8,128)(2,1)S(1)}, u32[]{:S(2)}, u32[]{:S(2)}) %collective-permute-start.29) | collective-permute-done | bytes 1572896 | tf_op jit(solution)/shard_map/ppermute | solution.py:45
  162.4 1.4 add_convert_fusion
  163.9 1.2 collective-permute-start.32
  165.1 2.0 %collective-permute-start.31 = (bf16[768,256]{1,0:T(8,128)(2,1)S(1)}, bf16[768,256]{1,0:T(8,128)(2,1)S(1)}, u32[]{:S(2)}, u32[]{:S(2)}) collective-permute-start(bf16[768,256]{1,0:T(8,128)(2,1)S(1)} %get-tuple-element.55), channel_id=1, source_target_pairs={{0,4},{2,6},{4,0},{6,2},{1,5},{3,7},{5,1},{7,3},{8,12},{10,14},{12... | collective-permute-start | bytes 1179656 | tf_op jit(solution)/shard_map/ppermute | solution.py:311
  167.8 6.5 %collective-permute-done.32 = bf16[768,256]{1,0:T(8,128)(2,1)S(1)} collective-permute-done((bf16[768,256]{1,0:T(8,128)(2,1)S(1)}, bf16[768,256]{1,0:T(8,128)(2,1)S(1)}, u32[]{:S(2)}, u32[]{:S(2)}) %collective-permute-start.32) | collective-permute-done | bytes 393248 | tf_op jit(solution)/shard_map/ppermute | solution.py:311
  174.3 2.4 %collective-permute-done.31 = bf16[768,256]{1,0:T(8,128)(2,1)S(1)} collective-permute-done((bf16[768,256]{1,0:T(8,128)(2,1)S(1)}, bf16[768,256]{1,0:T(8,128)(2,1)S(1)}, u32[]{:S(2)}, u32[]{:S(2)}) %collective-permute-start.31) | collective-permute-done | bytes 393248 | tf_op jit(solution)/shard_map/ppermute | solution.py:311
  176.7 9.4 %collective-permute-done.30 = bf16[768,256]{1,0:T(8,128)(2,1)S(1)} collective-permute-done((bf16[768,256]{1,0:T(8,128)(2,1)S(1)}, bf16[768,256]{1,0:T(8,128)(2,1)S(1)}, u32[]{:S(2)}, u32[]{:S(2)}) %collective-permute-start.30) | collective-permute-done | bytes 393248 | tf_op jit(solution)/shard_map/ppermute | solution.py:311
  (91 shorter events, 14.2 us)
Async XLA Ops:
  1.7 21.9 %copy-start = (bf16[129,768]{1,0:T(8,128)(2,1)}, bf16[129,768]{1,0:T(8,128)(2,1)S(1)}, u32[]{:S(2)}) copy-start(bf16[129,768]{1,0:T(8,128)(2,1)S(1)} %pad_maximum_fusion.1.packed_ref) | copy-start | bytes 594436
  1.7 8.8 %collective-permute-start = (bf16[129,128]{1,0:T(8,128)(2,1)S(1)}, bf16[129,128]{1,0:T(8,128)(2,1)S(1)}, u32[]{:S(2)}, u32[]{:S(2)}) collective-permute-start(bf16[129,128]{1,0:T(8,128)(2,1)S(1)} %get-tuple-element.59), channel_id=1, source_target_pairs={{0,8},{8,16},{16,24},{24,32},{32,40},{40,48},{48,56},{56,64},{64,7... | collective-permute-start | bytes 99080 | tf_op jit(solution)/shard_map/ppermute | solution.py:345
  4.8 6.5 %collective-permute-start.1 = (bf16[129,128]{1,0:T(8,128)(2,1)S(1)}, bf16[129,128]{1,0:T(8,128)(2,1)S(1)}, u32[]{:S(2)}, u32[]{:S(2)}) collective-permute-start(bf16[129,128]{1,0:T(8,128)(2,1)S(1)} %get-tuple-element.58), channel_id=1, source_target_pairs={{8,0},{16,8},{24,16},{32,24},{40,32},{48,40},{56,48},{64,56},{72,6... | collective-permute-start | bytes 99080 | tf_op jit(solution)/shard_map/ppermute | solution.py:346
  10.5 13.1 %copy-start.3 = (bf16[129,128]{1,0:T(8,128)(2,1)}, bf16[129,128]{1,0:T(8,128)(2,1)S(1)}, u32[]{:S(2)}) copy-start(bf16[129,128]{1,0:T(8,128)(2,1)S(1)} %collective-permute-done.low_ref) | copy-start | bytes 99076
  11.3 1.2 copy-start.1
  12.5 1.0 copy-start.2
  13.5 0.7 copy-start.7
  14.2 9.4 %copy-start.4 = (bf16[129,128]{1,0:T(8,128)(2,1)}, bf16[129,128]{1,0:T(8,128)(2,1)S(1)}, u32[]{:S(2)}) copy-start(bf16[129,128]{1,0:T(8,128)(2,1)S(1)} %collective-permute-done.1.high_ref) | copy-start | bytes 99076
  14.2 11.3 %slice-start = ((bf16[64,704]{1,0:T(8,128)(2,1)}), bf16[64,640]{1,0:T(8,128)(2,1)S(1)}, s32[]{:S(2)}) async-start(bf16[64,704]{1,0:T(8,128)(2,1)} %param.21), calls=%async_computation | async-start | bytes 163840 | tf_op jit(solution)/shard_map/slice | solution.py:351
  14.2 11.3 %slice-start.1 = ((bf16[64,704]{1,0:T(8,128)(2,1)}), bf16[64,64]{1,0:T(8,128)(2,1)S(1)}, s32[]{:S(2)}) async-start(bf16[64,704]{1,0:T(8,128)(2,1)} %param.21), calls=%async_computation.1 | async-start | bytes 32768 | tf_op jit(solution)/shard_map/slice | solution.py:351
  23.6 18.9 %collective-permute-start.2 = (bf16[4,768,256]{2,1,0:T(8,128)(2,1)}, bf16[4,768,256]{2,1,0:T(8,128)(2,1)}, u32[]{:S(2)}, u32[]{:S(2)}) collective-permute-start(bf16[4,768,256]{2,1,0:T(8,128)(2,1)} %get-tuple-element.26), channel_id=1, source_target_pairs={{0,1},{1,0},{2,3},{3,2},{4,5},{5,4},{6,7},{7,6},{8,9},{9,8},{10,11... | collective-permute-start | bytes 4718600 | tf_op jit(solution)/shard_map/ppermute | solution.py:45
  38.7 19.1 %collective-permute-start.9 = (bf16[256,1408]{1,0:T(8,128)(2,1)}, bf16[256,1408]{1,0:T(8,128)(2,1)}, u32[]{:S(2)}, u32[]{:S(2)}) collective-permute-start(bf16[256,1408]{1,0:T(8,128)(2,1)} %all_gather.3), channel_id=1, source_target_pairs={{0,32},{32,64},{64,96},{96,128},{128,160},{160,192},{192,224},{224... | collective-permute-start | bytes 2162696 | tf_op jit(solution)/shard_map/ppermute | solution.py:37
  40.0 17.8 %collective-permute-start.11 = (bf16[256,1408]{1,0:T(8,128)(2,1)}, bf16[256,1408]{1,0:T(8,128)(2,1)}, u32[]{:S(2)}, u32[]{:S(2)}) collective-permute-start(bf16[256,1408]{1,0:T(8,128)(2,1)} %all_gather.3), channel_id=1, source_target_pairs={{0,224},{32,0},{64,32},{96,64},{128,96},{160,128},{192,160},{224,1... | collective-permute-start | bytes 2162696 | tf_op jit(solution)/shard_map/ppermute | solution.py:37
  45.1 22.2 %collective-permute-start.5 = (bf16[768,256]{1,0:T(8,128)(2,1)}, bf16[768,256]{1,0:T(8,128)(2,1)S(1)}, u32[]{:S(2)}, u32[]{:S(2)}) collective-permute-start(bf16[768,256]{1,0:T(8,128)(2,1)} %get-tuple-element.30), channel_id=1, source_target_pairs={{0,6},{2,0},{4,2},{6,4},{1,7},{3,1},{5,3},{7,5},{8,14},{10,8},{12,... | collective-permute-start | bytes 1179656 | tf_op jit(solution)/shard_map/ppermute | solution.py:311
  47.8 19.6 %collective-permute-start.4 = (bf16[768,256]{1,0:T(8,128)(2,1)}, bf16[768,256]{1,0:T(8,128)(2,1)S(1)}, u32[]{:S(2)}, u32[]{:S(2)}) collective-permute-start(bf16[768,256]{1,0:T(8,128)(2,1)} %get-tuple-element.29), channel_id=1, source_target_pairs={{0,4},{2,6},{4,0},{6,2},{1,5},{3,7},{5,1},{7,3},{8,12},{10,14},{12... | collective-permute-start | bytes 1179656 | tf_op jit(solution)/shard_map/ppermute | solution.py:311
  48.2 21.9 %collective-permute-start.3 = (bf16[768,256]{1,0:T(8,128)(2,1)}, bf16[768,256]{1,0:T(8,128)(2,1)S(1)}, u32[]{:S(2)}, u32[]{:S(2)}) collective-permute-start(bf16[768,256]{1,0:T(8,128)(2,1)} %get-tuple-element.28), channel_id=1, source_target_pairs={{0,2},{2,4},{4,6},{6,0},{1,3},{3,5},{5,7},{7,1},{8,10},{10,12},{12... | collective-permute-start | bytes 1179656 | tf_op jit(solution)/shard_map/ppermute | solution.py:311
  57.8 6.8 %collective-permute-start.21 = (bf16[64,704]{1,0:T(8,128)(2,1)}, bf16[64,704]{1,0:T(8,128)(2,1)}, u32[]{:S(2)}, u32[]{:S(2)}) collective-permute-start(bf16[64,704]{1,0:T(8,128)(2,1)} %param.23), channel_id=1, source_target_pairs={{0,64},{32,96},{64,128},{96,160},{128,192},{160,224},{192,0},{224,... | collective-permute-start | bytes 270344 | tf_op jit(solution)/shard_map/ppermute | solution.py:37
  57.8 6.8 %collective-permute-start.22 = (bf16[64,704]{1,0:T(8,128)(2,1)}, bf16[64,704]{1,0:T(8,128)(2,1)S(1)}, u32[]{:S(2)}, u32[]{:S(2)}) collective-permute-start(bf16[64,704]{1,0:T(8,128)(2,1)} %param.23), channel_id=1, source_target_pairs={{0,192},{32,224},{64,0},{96,32},{128,64},{160,96},{192,128},{224,1... | collective-permute-start | bytes 270344 | tf_op jit(solution)/shard_map/ppermute | solution.py:37
  64.6 25.0 %collective-permute-start.10 = (bf16[256,1408]{1,0:T(8,128)(2,1)}, bf16[256,1408]{1,0:T(8,128)(2,1)S(1)}, u32[]{:S(2)}, u32[]{:S(2)}) collective-permute-start(bf16[256,1408]{1,0:T(8,128)(2,1)} %collective-permute-done.9), channel_id=1, source_target_pairs={{0,32},{32,64},{64,96},{96,128},{128,160},{160,192},{192,224},{224... | collective-permute-start | bytes 2162696 | tf_op jit(solution)/shard_map/ppermute | solution.py:37
  64.6 28.8 %collective-permute-start.12 = (bf16[256,1408]{1,0:T(8,128)(2,1)}, bf16[256,1408]{1,0:T(8,128)(2,1)S(1)}, u32[]{:S(2)}, u32[]{:S(2)}) collective-permute-start(bf16[256,1408]{1,0:T(8,128)(2,1)} %collective-permute-done.11), channel_id=1, source_target_pairs={{0,224},{32,0},{64,32},{96,64},{128,96},{160,128},{192,160},{224,1... | collective-permute-start | bytes 2162696 | tf_op jit(solution)/shard_map/ppermute | solution.py:37
  67.3 14.3 %collective-permute-start.19 = (bf16[64,704]{1,0:T(8,128)(2,1)}, bf16[64,704]{1,0:T(8,128)(2,1)S(1)}, u32[]{:S(2)}, u32[]{:S(2)}) collective-permute-start(bf16[64,704]{1,0:T(8,128)(2,1)} %param.23), channel_id=1, source_target_pairs={{0,32},{32,64},{64,96},{96,128},{128,160},{160,192},{192,224},{224... | collective-permute-start | bytes 270344 | tf_op jit(solution)/shard_map/ppermute | solution.py:37
  67.4 14.3 %collective-permute-start.20 = (bf16[64,704]{1,0:T(8,128)(2,1)}, bf16[64,704]{1,0:T(8,128)(2,1)S(1)}, u32[]{:S(2)}, u32[]{:S(2)}) collective-permute-start(bf16[64,704]{1,0:T(8,128)(2,1)} %param.23), channel_id=1, source_target_pairs={{0,224},{32,0},{64,32},{96,64},{128,96},{160,128},{192,160},{224,1... | collective-permute-start | bytes 270344 | tf_op jit(solution)/shard_map/ppermute | solution.py:37
  70.1 23.4 %collective-permute-start.25 = (bf16[64,704]{1,0:T(8,128)(2,1)S(1)}, bf16[64,704]{1,0:T(8,128)(2,1)S(1)}, u32[]{:S(2)}, u32[]{:S(2)}) collective-permute-start(bf16[64,704]{1,0:T(8,128)(2,1)S(1)} %broadcast_select_fusion.2), channel_id=1, source_target_pairs={{0,64},{1,193},{2,66},{3,195},{4,68},{5,197},{6,70},{7,199},{8,72}... | collective-permute-start | bytes 270344 | tf_op jit(solution)/shard_map/ppermute | solution.py:33
  81.7 6.6 %collective-permute-start.23 = (bf16[64,704]{1,0:T(8,128)(2,1)}, bf16[64,704]{1,0:T(8,128)(2,1)S(1)}, u32[]{:S(2)}, u32[]{:S(2)}) collective-permute-start(bf16[64,704]{1,0:T(8,128)(2,1)} %collective-permute-done.21), channel_id=1, source_target_pairs={{0,32},{32,64},{64,96},{96,128},{128,160},{160,192},{192,224},{224... | collective-permute-start | bytes 270344 | tf_op jit(solution)/shard_map/ppermute | solution.py:37
  81.7 10.6 %collective-permute-start.24 = (bf16[64,704]{1,0:T(8,128)(2,1)S(1)}, bf16[64,704]{1,0:T(8,128)(2,1)S(1)}, u32[]{:S(2)}, u32[]{:S(2)}) collective-permute-start(bf16[64,704]{1,0:T(8,128)(2,1)S(1)} %collective-permute-done.22), channel_id=1, source_target_pairs={{0,224},{32,0},{64,32},{96,64},{128,96},{160,128},{192,160},{224,1... | collective-permute-start | bytes 270344 | tf_op jit(solution)/shard_map/ppermute | solution.py:37
  88.3 8.0 %collective-permute-start.6 = (bf16[768,256]{1,0:T(8,128)(2,1)S(1)}, bf16[768,256]{1,0:T(8,128)(2,1)S(1)}, u32[]{:S(2)}, u32[]{:S(2)}) collective-permute-start(bf16[768,256]{1,0:T(8,128)(2,1)S(1)} %add_convert_fusion.2.p0), channel_id=1, source_target_pairs={{0,2},{2,4},{4,6},{6,0},{1,3},{3,5},{5,7},{7,1},{8,10},{10,12},{12... | collective-permute-start | bytes 1179656 | tf_op jit(solution)/shard_map/ppermute | solution.py:311
  89.6 13.5 %collective-permute-start.7 = (bf16[768,256]{1,0:T(8,128)(2,1)S(1)}, bf16[768,256]{1,0:T(8,128)(2,1)S(1)}, u32[]{:S(2)}, u32[]{:S(2)}) collective-permute-start(bf16[768,256]{1,0:T(8,128)(2,1)S(1)} %add_convert_fusion.2.p0), channel_id=1, source_target_pairs={{0,4},{2,6},{4,0},{6,2},{1,5},{3,7},{5,1},{7,3},{8,12},{10,14},{12... | collective-permute-start | bytes 1179656 | tf_op jit(solution)/shard_map/ppermute | solution.py:311
  92.3 10.8 %collective-permute-start.8 = (bf16[768,256]{1,0:T(8,128)(2,1)S(1)}, bf16[768,256]{1,0:T(8,128)(2,1)S(1)}, u32[]{:S(2)}, u32[]{:S(2)}) collective-permute-start(bf16[768,256]{1,0:T(8,128)(2,1)S(1)} %add_convert_fusion.2.p0), channel_id=1, source_target_pairs={{0,6},{2,0},{4,2},{6,4},{1,7},{3,1},{5,3},{7,5},{8,14},{10,8},{12,... | collective-permute-start | bytes 1179656 | tf_op jit(solution)/shard_map/ppermute | solution.py:311
  93.4 22.4 %collective-permute-start.14 = (bf16[256,1408]{1,0:T(8,128)(2,1)S(1)}, bf16[256,1408]{1,0:T(8,128)(2,1)S(1)}, u32[]{:S(2)}, u32[]{:S(2)}) collective-permute-start(bf16[256,1408]{1,0:T(8,128)(2,1)S(1)} %collective-permute-done.10), channel_id=1, source_target_pairs={{0,32},{32,64},{64,96},{96,128},{128,160},{160,192},{192,224},{224... | collective-permute-start | bytes 2162696 | tf_op jit(solution)/shard_map/ppermute | solution.py:37
  93.5 22.3 %collective-permute-start.15 = (bf16[256,1408]{1,0:T(8,128)(2,1)S(1)}, bf16[256,1408]{1,0:T(8,128)(2,1)S(1)}, u32[]{:S(2)}, u32[]{:S(2)}) collective-permute-start(bf16[256,1408]{1,0:T(8,128)(2,1)S(1)} %collective-permute-done.12), channel_id=1, source_target_pairs={{0,224},{32,0},{64,32},{96,64},{128,96},{160,128},{192,160},{224,1... | collective-permute-start | bytes 2162696 | tf_op jit(solution)/shard_map/ppermute | solution.py:37
  96.2 45.2 %collective-permute-start.26 = (bf16[8,64,704]{2,1,0:T(8,128)(2,1)S(1)}, bf16[8,64,704]{2,1,0:T(8,128)(2,1)S(1)}, u32[]{:S(2)}, u32[]{:S(2)}) collective-permute-start(bf16[8,64,704]{2,1,0:T(8,128)(2,1)S(1)} %bitcast_dynamic-update-slice_fusion.12), channel_id=1, source_target_pairs={{0,8},{8,16},{16,24},{24,0},{1,9},{9,17},{17,25},{25,1},{2,10},{10... | collective-permute-start | bytes 2162696 | tf_op jit(solution)/shard_map/ppermute | solution.py:41
  103.1 38.4 %collective-permute-start.27 = (bf16[8,64,704]{2,1,0:T(8,128)(2,1)S(1)}, bf16[8,64,704]{2,1,0:T(8,128)(2,1)S(1)}, u32[]{:S(2)}, u32[]{:S(2)}) collective-permute-start(bf16[8,64,704]{2,1,0:T(8,128)(2,1)S(1)} %bitcast_dynamic-update-slice_fusion.12), channel_id=1, source_target_pairs={{0,24},{8,0},{16,8},{24,16},{1,25},{9,1},{17,9},{25,17},{2,26},{10... | collective-permute-start | bytes 2162696 | tf_op jit(solution)/shard_map/ppermute | solution.py:41
  103.3 12.7 %collective-permute-start.13 = (bf16[4,768,256]{2,1,0:T(8,128)(2,1)S(1)}, bf16[4,768,256]{2,1,0:T(8,128)(2,1)S(1)}, u32[]{:S(2)}, u32[]{:S(2)}) collective-permute-start(bf16[4,768,256]{2,1,0:T(8,128)(2,1)S(1)} %pad_maximum_fusion), channel_id=1, source_target_pairs={{0,1},{1,0},{2,3},{3,2},{4,5},{5,4},{6,7},{7,6},{8,9},{9,8},{10,11... | collective-permute-start | bytes 4718600 | tf_op jit(solution)/shard_map/ppermute | solution.py:45
  112.2 3.8 %copy-start.5 = (f32[2048]{0:T(1024)S(1)}, f32[2048]{0:T(1024)}, u32[]{:S(2)}) copy-start(f32[2048]{0:T(1024)} %param.19) | copy-start | bytes 24580
  115.9 10.5 %collective-permute-start.16 = (bf16[256,1408]{1,0:T(8,128)(2,1)S(1)}, bf16[256,1408]{1,0:T(8,128)(2,1)S(1)}, u32[]{:S(2)}, u32[]{:S(2)}) collective-permute-start(bf16[256,1408]{1,0:T(8,128)(2,1)S(1)} %broadcast_select_fusion.1), channel_id=1, source_target_pairs={{0,32},{1,225},{2,34},{3,227},{4,36},{5,229},{6,38},{7,231},{8,40}... | collective-permute-start | bytes 2162696 | tf_op jit(solution)/shard_map/ppermute | solution.py:33
  129.6 12.7 %collective-permute-start.17 = (bf16[1,704]{1,0:T(2,128)(2,1)S(1)}, bf16[1,704]{1,0:T(2,128)(2,1)S(1)}, u32[]{:S(2)}, u32[]{:S(2)}) collective-permute-start(bf16[1,704]{1,0:T(2,128)(2,1)S(1)} %get-tuple-element.57), channel_id=1, source_target_pairs={{0,8},{8,16},{16,24},{24,32},{32,40},{40,48},{48,56},{56,64},{64,7... | collective-permute-start | bytes 4232 | tf_op jit(solution)/shard_map/ppermute | solution.py:421
  132.4 9.8 %collective-permute-start.18 = (bf16[1,704]{1,0:T(2,128)(2,1)S(1)}, bf16[1,704]{1,0:T(2,128)(2,1)S(1)}, u32[]{:S(2)}, u32[]{:S(2)}) collective-permute-start(bf16[1,704]{1,0:T(2,128)(2,1)S(1)} %get-tuple-element.56), channel_id=1, source_target_pairs={{8,0},{16,8},{24,16},{32,24},{40,32},{48,40},{56,48},{64,56},{72,6... | collective-permute-start | bytes 4232 | tf_op jit(solution)/shard_map/ppermute | solution.py:422
  141.5 11.2 %collective-permute-start.28 = (bf16[8,64,704]{2,1,0:T(8,128)(2,1)S(1)}, bf16[8,64,704]{2,1,0:T(8,128)(2,1)S(1)}, u32[]{:S(2)}, u32[]{:S(2)}) collective-permute-start(bf16[8,64,704]{2,1,0:T(8,128)(2,1)S(1)} %broadcast_select_fusion), channel_id=1, source_target_pairs={{0,8},{1,25},{2,10},{3,27},{4,12},{5,29},{6,14},{7,31},{8,16},{9,1... | collective-permute-start | bytes 2162696 | tf_op jit(solution)/shard_map/ppermute | solution.py:33
  142.0 0.7 copy-start.6
  154.5 7.8 %collective-permute-start.29 = (bf16[768,1024]{1,0:T(8,128)(2,1)S(1)}, bf16[768,1024]{1,0:T(8,128)(2,1)S(1)}, u32[]{:S(2)}, u32[]{:S(2)}) collective-permute-start(bf16[768,1024]{1,0:T(8,128)(2,1)S(1)} %convolution_convert_fusion), channel_id=1, source_target_pairs={{0,1},{1,0},{2,3},{3,2},{4,5},{5,4},{6,7},{7,6},{8,9},{9,8},{10,11... | collective-permute-start | bytes 4718600 | tf_op jit(solution)/shard_map/ppermute | solution.py:45
  163.9 10.4 %collective-permute-start.32 = (bf16[768,256]{1,0:T(8,128)(2,1)S(1)}, bf16[768,256]{1,0:T(8,128)(2,1)S(1)}, u32[]{:S(2)}, u32[]{:S(2)}) collective-permute-start(bf16[768,256]{1,0:T(8,128)(2,1)S(1)} %get-tuple-element.54), channel_id=1, source_target_pairs={{0,6},{2,0},{4,2},{6,4},{1,7},{3,1},{5,3},{7,5},{8,14},{10,8},{12,... | collective-permute-start | bytes 1179656 | tf_op jit(solution)/shard_map/ppermute | solution.py:311
  165.1 11.6 %collective-permute-start.31 = (bf16[768,256]{1,0:T(8,128)(2,1)S(1)}, bf16[768,256]{1,0:T(8,128)(2,1)S(1)}, u32[]{:S(2)}, u32[]{:S(2)}) collective-permute-start(bf16[768,256]{1,0:T(8,128)(2,1)S(1)} %get-tuple-element.55), channel_id=1, source_target_pairs={{0,4},{2,6},{4,0},{6,2},{1,5},{3,7},{5,1},{7,3},{8,12},{10,14},{12... | collective-permute-start | bytes 1179656 | tf_op jit(solution)/shard_map/ppermute | solution.py:311
  167.0 19.0 %collective-permute-start.30 = (bf16[768,256]{1,0:T(8,128)(2,1)S(1)}, bf16[768,256]{1,0:T(8,128)(2,1)S(1)}, u32[]{:S(2)}, u32[]{:S(2)}) collective-permute-start(bf16[768,256]{1,0:T(8,128)(2,1)S(1)} %get-tuple-element.53), channel_id=1, source_target_pairs={{0,2},{2,4},{4,6},{6,0},{1,3},{3,5},{5,7},{7,1},{8,10},{10,12},{12... | collective-permute-start | bytes 1179656 | tf_op jit(solution)/shard_map/ppermute | solution.py:311

commit v3 on v2

--- a/solution.py
+++ b/solution.py
@@ -56,24 +56,15 @@
 
 
 def attention_kernel(
-    at_ref, sink_ref, q_hbm, w_hbm, packed_ref, low_ref, high_ref,
-    theirs_ref, mine_ref,
-    q_ref, w_ref, att_ref, kx_ref, vx_ref, row_ref, col_ref, sems,
+    at_ref, sink_ref, q_ref, w_ref, packed_ref, low_ref, high_ref,
+    theirs_ref, mine_ref, same_ref,
+    att_ref, kx_ref, vx_ref, row_ref, col_ref,
 ):
-    copies = [
-        pltpu.make_async_copy(source, target, sems.at[i])
-        for i, (source, target) in enumerate(
-            ((q_hbm, q_ref), (w_hbm, w_ref))
-        )
-    ]
-    for copy in copies:
-        copy.start()
     rows = q_ref.shape[0]
     heads = q_ref.shape[1] // HEAD_DIM
     span = theirs_ref.shape[2]
     kx_ref[...] = jnp.zeros_like(kx_ref)
     vx_ref[...] = jnp.zeros_like(vx_ref)
-    copies[0].wait()
     pieces = (
         (0, WINDOW, low_ref[:HEAD_DIM], low_ref[HEAD_DIM : 2 * HEAD_DIM]),
         (WINDOW, rows, packed_ref[:HEAD_DIM], packed_ref[HEAD_DIM : 2 * HEAD_DIM]),
@@ -98,6 +89,15 @@
         col_ref[n * WINDOW : (n + 1) * WINDOW, :] = jnp.broadcast_to(
             part[:1], (WINDOW, WINDOW)
         ).T
+
+    label = col_ref[...]
+    at_row = lax.broadcasted_iota(jnp.int32, (rows, WINDOW), 0)
+    at_lane = lax.broadcasted_iota(jnp.int32, (rows, WINDOW), 1)
+    first, last = row_ref[:1, WINDOW - 1 : WINDOW], row_ref[:1, WINDOW + rows : WINDOW + rows + 1]
+    prior = jnp.where(at_row == 0, first, pltpu.roll(label, 1, 0))
+    following = jnp.where(at_row == rows - 1, last, pltpu.roll(label, rows - 1, 0))
+    other = jnp.where(at_lane == 0, prior, following)
+    same_ref[...] = jnp.where(other == label, 1.0, 0.0)
 
     def step(n, carry):
         base = pl.multiple_of(n * WINDOW, WINDOW)
@@ -125,14 +125,15 @@
         return carry
 
     lax.fori_loop(0, rows // WINDOW, step, 0)
-    copies[1].wait()
     for k in range(NY):
         cols = pl.ds(pl.multiple_of(at_ref[NY + k] * span, span), span)
         theirs_ref[k] = jnp.dot(
             att_ref[...], w_ref[:, cols], preferred_element_type=jnp.float32
         ).astype(jnp.bfloat16)
         cols = pl.ds(pl.multiple_of(at_ref[k] * span, span), span)
-        mine_ref[k] = jnp.dot(att_ref[...], w_ref[:, cols], preferred_element_type=jnp.float32)
+        mine_ref[k] = jnp.dot(
+            att_ref[...], w_ref[:, cols], preferred_element_type=jnp.float32
+        ).astype(jnp.bfloat16)
 
 
 def vmem_specs(count):
@@ -152,19 +153,17 @@
         attention_kernel,
         out_shape=[
             jax.ShapeDtypeStruct((NY, rows, span), jnp.bfloat16),
-            jax.ShapeDtypeStruct((NY, rows, span), jnp.float32),
+            jax.ShapeDtypeStruct((NY, rows, span), jnp.bfloat16),
+            jax.ShapeDtypeStruct((rows, WINDOW), jnp.float32),
         ],
-        in_specs=smem_specs(2) + [pl.BlockSpec(memory_space=pltpu.HBM)] * 2 + vmem_specs(3),
-        out_specs=vmem_specs(2),
+        in_specs=smem_specs(2) + vmem_specs(5),
+        out_specs=vmem_specs(3),
         scratch_shapes=[
-            pltpu.VMEM((rows, cols), jnp.bfloat16),
-            pltpu.VMEM(w_out.shape, jnp.bfloat16),
             pltpu.VMEM((rows, cols), jnp.bfloat16),
             pltpu.VMEM((heads, cols, reach), jnp.bfloat16),
             pltpu.VMEM((heads, reach, cols), jnp.bfloat16),
             pltpu.VMEM((8, reach), jnp.float32),
             pltpu.VMEM((rows, WINDOW), jnp.float32),
-            pltpu.SemaphoreType.DMA((2,)),
         ],
         compiler_params=pltpu.CompilerParams(vmem_limit_bytes=12 * MB),
         cost_estimate=pl.CostEstimate(flops=4 * 10**9, bytes_accessed=4 * MB, transcendentals=0),
@@ -174,7 +173,9 @@
 
 def pair_kernel(mine_ref, got_ref, s0, s1, s2, s3):
     for k, out in enumerate((s0, s1, s2, s3)):
-        out[...] = (mine_ref[k] + got_ref[k].astype(jnp.float32)).astype(jnp.bfloat16)
+        out[...] = (
+            mine_ref[k].astype(jnp.float32) + got_ref[k].astype(jnp.float32)
+        ).astype(jnp.bfloat16)
 
 
 def pair_sums(mine, got):
@@ -363,7 +364,7 @@
 
     plus1, minus1 = ring_step(up_rows, up_rows)
 
-    theirs, mine = attention(order, sink_logits, queries, packed, low, high, w_out)
+    theirs, mine, same = attention(order, sink_logits, queries, packed, low, high, w_out)
     got = swap(theirs)
 
     pairs = pair_sums(mine, got)
@@ -393,7 +394,7 @@
     full = put(jnp.zeros((NZ,) + up_rows.shape, share.dtype), after(up_rows, mixed_own), z)
     full = keep(full, plus1, minus1, 1)
     whole = jnp.zeros((NZ,) + w_down_t.shape, w_down_t.dtype)
-    whole = put(whole, after(w_down_t, mixed_own), z)
+    whole = put(whole, after(w_down_t, mixed_own, plus2, minus2), z)
     whole = keep(whole, *near, 1)
     whole = keep(whole, far_plus, far_minus, 2)
     whole = keep(whole, *third, 3)
@@ -415,16 +416,13 @@
     full_down = put(full_down, after(whole, normed)[:, None], 0, x)
     full_down = put(full_down, whole_plus[:, None], 0, (x - 1) % NX)
     full_down = put(full_down, whole_minus[:, None], 0, (x + 1) % NX)
+    normed = after(normed, full_down)
     full_down = put(full_down, whole_far[:, None], 0, (x + 2) % NX).reshape(model_width, ff)
 
     up_value = up(normed, full, tail, width - tail)
     before = lax.ppermute(up_value[-1:, :ff], ("z", "x"), forward)
     behind = lax.ppermute(up_value[:1, :ff], ("z", "x"), backward)
     up_gate = up(normed, full, 0, tail)
-    low, packed, high = lax.optimization_barrier((low, packed, high, pairs[0]))[:3]
-    edge = jnp.concatenate([low[-1:, -1:], packed[-1:], high[-1:, :1]], axis=1)[0]
-    same = jnp.stack([edge[:-2] == edge[1:-1], edge[2:] == edge[1:-1]], axis=1)
-    same = same.astype(jnp.float32)
     hidden = hidden_units(up_value, up_gate, same, before, behind, conv_taps)
 
     def down(who):

time: 188 us -> 186 us (0.989)
  the two profiles are of different devices: /device:TPU:129 before, /device:TPU:2 now
where the time goes in v3:
time: 186 us; the launch traced here: 183 us
  starting transfers between devices  66.4 us (36%)
  waiting for transfers between devices  59.2 us (32%)
  Pallas kernels  19.7 us (11%)
  blocking collectives  16.9 us (9%)
  local copies, waits for them, and re-layouts  12.3 us (7%)
  other arithmetic  4.64 us (2%)
  matrix products  2.89 us (2%)
    ppermute x12, waiting for transfers between devices, send_z(): return lax.ppermute(block, 'z', [(z, (z + k) % NZ) for z in range(NZ)])  27.8 us
    ppermute x12, starting transfers between devices, send_z(): return lax.ppermute(block, 'z', [(z, (z + k) % NZ) for z in range(NZ)])  23.9 us
    ppermute x9, waiting for transfers between devices, to_owners(): lax.ppermute(pairs[k], 'y', [(y, (y + k) % NY) for y in range(NY)])  21.9 us
    ppermute x9, starting transfers between devices, to_owners(): lax.ppermute(pairs[k], 'y', [(y, (y + k) % NY) for y in range(NY)])  17.2 us
    all_gather x1, blocking collectives, per_device(): up_rows = lax.all_gather(share, 'x', axis=0, tiled=True)  16.9 us
    ppermute x3, starting transfers between devices, send_apart(): return lax.ppermute(block, AXES, pairs)  9.11 us
    pallas_call x1, Pallas kernels, attention(): pl.pallas_call(attention_kernel, out_shape=[jax.ShapeDtypeStruct((NY, row...  7.83 us
    pallas_call x2, Pallas kernels, up(): pl.pallas_call(functools.partial(up_kernel, start), out_shape=jax.ShapeDt...  6.03 us
  transfers between devices with their start and end apart: 33, of which 15 were waited for; matrix products, arithmetic and copies ran while one was open for 6% of the time, Pallas kernels for 6%

profile of v3, /device:TPU:2, one launch (start us, length us, event | category | flops | bytes accessed | tf_op | source)
XLA Modules:
  0.0 182.6 jit_solution(17806382073201674761)
XLA Ops:
  1.7 3.4 %collective-permute-start = (bf16[129,128]{1,0:T(8,128)(2,1)S(1)}, bf16[129,128]{1,0:T(8,128)(2,1)S(1)}, u32[]{:S(2)}, u32[]{:S(2)}) collective-permute-start(bf16[129,128]{1,0:T(8,128)(2,1)S(1)} %get-tuple-element.57), channel_id=1, source_target_pairs={{0,8},{8,16},{16,24},{24,32},{32,40},{40,48},{48,56},{56,64},{64,7... | collective-permute-start | bytes 99080 | tf_op jit(solution)/shard_map/ppermute | solution.py:346
  5.1 2.4 %collective-permute-start.1 = (bf16[129,128]{1,0:T(8,128)(2,1)S(1)}, bf16[129,128]{1,0:T(8,128)(2,1)S(1)}, u32[]{:S(2)}, u32[]{:S(2)}) collective-permute-start(bf16[129,128]{1,0:T(8,128)(2,1)S(1)} %get-tuple-element.56), channel_id=1, source_target_pairs={{8,0},{16,8},{24,16},{32,24},{40,32},{48,40},{56,48},{64,56},{72,6... | collective-permute-start | bytes 99080 | tf_op jit(solution)/shard_map/ppermute | solution.py:347
  9.3 1.0 concatenate.13
  10.9 1.2 copy-done
  12.1 1.0 copy-done.1
  13.8 7.8 %attention.1 = (bf16[4,768,256]{2,1,0:T(8,128)(2,1)S(1)}, bf16[4,768,256]{2,1,0:T(8,128)(2,1)S(1)}, f32[768,128]{1,0:T(8,128)S(1)}) custom-call(s32[16]{0:T(128)S(1)} %stack.76.at_ref, f32[4]{0:T(128)S(1)} %copy-done.4, bf16[768,256]{1,0:T(8,128)(2,1)S(1)} %copy-done.1, bf16[256,2048]{1,0:T(8,128)(2,1)S(1)} %copy-done, ...), custom_call_target="tpu_custom_call" | custom-call | flops 4000000000 | bytes 4194304 | tf_op jit(solution)/shard_map/attention/pallas_call | solution.py:152
  21.7 16.9 %all_gather.3 = bf16[256,1408]{1,0:T(8,128)(2,1)S(1)} all-gather(bf16[64,1408]{1,0:T(8,128)(2,1)S(1)} %concatenate.13), channel_id=1, replica_groups=mesh['z'=8,'x'=4,'y'=4,'core'=2] {'x'}, dimensions={0}, use_global_device_ids=true | all-gather | bytes 901120 | tf_op jit(solution)/shard_map/all_gather | solution.py:355
  38.6 1.9 %collective-permute-start.9 = (bf16[256,1408]{1,0:T(8,128)(2,1)S(1)}, bf16[256,1408]{1,0:T(8,128)(2,1)S(1)}, u32[]{:S(2)}, u32[]{:S(2)}) collective-permute-start(bf16[256,1408]{1,0:T(8,128)(2,1)S(1)} %all_gather.3), channel_id=1, source_target_pairs={{0,32},{32,64},{64,96},{96,128},{128,160},{160,192},{192,224},{224... | collective-permute-start | bytes 2162696 | tf_op jit(solution)/shard_map/ppermute | solution.py:37
  40.5 1.3 collective-permute-start.11
  41.8 13.9 %collective-permute-done.9 = bf16[256,1408]{1,0:T(8,128)(2,1)S(1)} collective-permute-done((bf16[256,1408]{1,0:T(8,128)(2,1)S(1)}, bf16[256,1408]{1,0:T(8,128)(2,1)S(1)}, u32[]{:S(2)}, u32[]{:S(2)}) %collective-permute-start.9) | collective-permute-done | bytes 720928 | tf_op jit(solution)/shard_map/ppermute | solution.py:37
  56.7 2.3 %collective-permute-start.12 = (bf16[256,1408]{1,0:T(8,128)(2,1)}, bf16[256,1408]{1,0:T(8,128)(2,1)}, u32[]{:S(2)}, u32[]{:S(2)}) collective-permute-start(bf16[256,1408]{1,0:T(8,128)(2,1)} %collective-permute-done.11), channel_id=1, source_target_pairs={{0,224},{32,0},{64,32},{96,64},{128,96},{160,128},{192,160},{224,1... | collective-permute-start | bytes 2162696 | tf_op jit(solution)/shard_map/ppermute | solution.py:37
  59.4 3.5 %collective-permute-start.16 = (bf16[64,704]{1,0:T(8,128)(2,1)}, bf16[64,704]{1,0:T(8,128)(2,1)S(1)}, u32[]{:S(2)}, u32[]{:S(2)}) collective-permute-start(bf16[64,704]{1,0:T(8,128)(2,1)} %param.23), channel_id=1, source_target_pairs={{0,64},{32,96},{64,128},{96,160},{128,192},{160,224},{192,0},{224,... | collective-permute-start | bytes 270344 | tf_op jit(solution)/shard_map/ppermute | solution.py:37
  62.9 1.6 collective-permute-start.3
  64.5 2.9 %collective-permute-start.4 = (bf16[768,256]{1,0:T(8,128)(2,1)S(1)}, bf16[768,256]{1,0:T(8,128)(2,1)}, u32[]{:S(2)}, u32[]{:S(2)}) collective-permute-start(bf16[768,256]{1,0:T(8,128)(2,1)S(1)} %get-tuple-element.28), channel_id=1, source_target_pairs={{0,4},{2,6},{4,0},{6,2},{1,5},{3,7},{5,1},{7,3},{8,12},{10,14},{12... | collective-permute-start | bytes 1179656 | tf_op jit(solution)/shard_map/ppermute | solution.py:312
  67.4 7.3 %collective-permute-done.10 = bf16[256,1408]{1,0:T(8,128)(2,1)S(1)} collective-permute-done((bf16[256,1408]{1,0:T(8,128)(2,1)S(1)}, bf16[256,1408]{1,0:T(8,128)(2,1)S(1)}, u32[]{:S(2)}, u32[]{:S(2)}) %collective-permute-start.10) | collective-permute-done | bytes 720928 | tf_op jit(solution)/shard_map/ppermute | solution.py:37
  74.6 3.0 %collective-permute-start.5 = (bf16[768,256]{1,0:T(8,128)(2,1)S(1)}, bf16[768,256]{1,0:T(8,128)(2,1)}, u32[]{:S(2)}, u32[]{:S(2)}) collective-permute-start(bf16[768,256]{1,0:T(8,128)(2,1)S(1)} %get-tuple-element.29), channel_id=1, source_target_pairs={{0,6},{2,0},{4,2},{6,4},{1,7},{3,1},{5,3},{7,5},{8,14},{10,8},{12,... | collective-permute-start | bytes 1179656 | tf_op jit(solution)/shard_map/ppermute | solution.py:312
  77.7 2.9 %collective-permute-start.17 = (bf16[64,704]{1,0:T(8,128)(2,1)}, bf16[64,704]{1,0:T(8,128)(2,1)}, u32[]{:S(2)}, u32[]{:S(2)}) collective-permute-start(bf16[64,704]{1,0:T(8,128)(2,1)} %param.23), channel_id=1, source_target_pairs={{0,192},{32,224},{64,0},{96,32},{128,64},{160,96},{192,128},{224,1... | collective-permute-start | bytes 270344 | tf_op jit(solution)/shard_map/ppermute | solution.py:37
  80.5 3.8 %collective-permute-done.17 = bf16[64,704]{1,0:T(8,128)(2,1)} collective-permute-done((bf16[64,704]{1,0:T(8,128)(2,1)}, bf16[64,704]{1,0:T(8,128)(2,1)}, u32[]{:S(2)}, u32[]{:S(2)}) %collective-permute-start.17) | collective-permute-done | bytes 90144 | tf_op jit(solution)/shard_map/ppermute | solution.py:37
  84.4 2.3 %collective-permute-start.23 = (bf16[256,1408]{1,0:T(8,128)(2,1)S(1)}, bf16[256,1408]{1,0:T(8,128)(2,1)S(1)}, u32[]{:S(2)}, u32[]{:S(2)}) collective-permute-start(bf16[256,1408]{1,0:T(8,128)(2,1)S(1)} %collective-permute-done.10), channel_id=1, source_target_pairs={{0,32},{32,64},{64,96},{96,128},{128,160},{160,192},{192,224},{224... | collective-permute-start | bytes 2162696 | tf_op jit(solution)/shard_map/ppermute | solution.py:37
  86.7 2.5 %collective-permute-start.14 = (bf16[64,704]{1,0:T(8,128)(2,1)}, bf16[64,704]{1,0:T(8,128)(2,1)S(1)}, u32[]{:S(2)}, u32[]{:S(2)}) collective-permute-start(bf16[64,704]{1,0:T(8,128)(2,1)} %param.23), channel_id=1, source_target_pairs={{0,32},{32,64},{64,96},{96,128},{128,160},{160,192},{192,224},{224... | collective-permute-start | bytes 270344 | tf_op jit(solution)/shard_map/ppermute | solution.py:37
  89.3 1.0 collective-permute-start.15
  90.3 5.0 %collective-permute-start.20 = (bf16[64,704]{1,0:T(8,128)(2,1)S(1)}, bf16[64,704]{1,0:T(8,128)(2,1)S(1)}, u32[]{:S(2)}, u32[]{:S(2)}) collective-permute-start(bf16[64,704]{1,0:T(8,128)(2,1)S(1)} %broadcast_select_fusion.2), channel_id=1, source_target_pairs={{0,64},{1,193},{2,66},{3,195},{4,68},{5,197},{6,70},{7,199},{8,72}... | collective-permute-start | bytes 270344 | tf_op jit(solution)/shard_map/ppermute | solution.py:33
  95.2 1.6 add_convert_fusion.2.p0
  98.4 2.6 %collective-permute-done.14 = bf16[64,704]{1,0:T(8,128)(2,1)S(1)} collective-permute-done((bf16[64,704]{1,0:T(8,128)(2,1)}, bf16[64,704]{1,0:T(8,128)(2,1)S(1)}, u32[]{:S(2)}, u32[]{:S(2)}) %collective-permute-start.14) | collective-permute-done | bytes 90144 | tf_op jit(solution)/shard_map/ppermute | solution.py:37
  101.0 1.7 collective-permute-start.19
  102.7 1.5 collective-permute-start.6
  105.2 3.1 %collective-permute-start.7 = (bf16[768,256]{1,0:T(8,128)(2,1)S(1)}, bf16[768,256]{1,0:T(8,128)(2,1)S(1)}, u32[]{:S(2)}, u32[]{:S(2)}) collective-permute-start(bf16[768,256]{1,0:T(8,128)(2,1)S(1)} %add_convert_fusion.2.p0), channel_id=1, source_target_pairs={{0,4},{2,6},{4,0},{6,2},{1,5},{3,7},{5,1},{7,3},{8,12},{10,14},{12... | collective-permute-start | bytes 1179656 | tf_op jit(solution)/shard_map/ppermute | solution.py:312
  108.4 1.7 collective-permute-start.8
  110.1 2.8 %collective-permute-start.24 = (bf16[256,1408]{1,0:T(8,128)(2,1)}, bf16[256,1408]{1,0:T(8,128)(2,1)S(1)}, u32[]{:S(2)}, u32[]{:S(2)}) collective-permute-start(bf16[256,1408]{1,0:T(8,128)(2,1)} %collective-permute-done.12), channel_id=1, source_target_pairs={{0,224},{32,0},{64,32},{96,64},{128,96},{160,128},{192,160},{224,1... | collective-permute-start | bytes 2162696 | tf_op jit(solution)/shard_map/ppermute | solution.py:37
  114.1 3.4 %collective-permute-done.7.p2 = bf16[768,256]{1,0:T(8,128)(2,1)S(1)} collective-permute-done((bf16[768,256]{1,0:T(8,128)(2,1)S(1)}, bf16[768,256]{1,0:T(8,128)(2,1)S(1)}, u32[]{:S(2)}, u32[]{:S(2)}) %collective-permute-start.7) | collective-permute-done | bytes 393248 | tf_op jit(solution)/shard_map/ppermute | solution.py:312
  117.5 1.7 collective-permute-start.22
  120.7 1.2 bitcast_dynamic-update-slice_fusion.9
  123.0 2.6 %normalise.1.left_ref = bf16[768,2048]{1,0:T(8,128)(2,1)S(1)} custom-call(s32[16]{0:T(128)S(1)} %stack.76.at_ref, bf16[768,256]{1,0:T(8,128)(2,1)S(1)} %add_convert_fusion.2.p0, bf16[768,256]{1,0:T(8,128)(2,1)S(1)} %collective-permute-done.6.p1, bf16[768,256]{1,0:T(8,128)(2,1)S(1)} %collective-permute-done.7.p2, ...), custom_call_target="tpu_custom_call" | custom-call | flops 2000000000 | bytes 6291456 | tf_op jit(solution)/shard_map/normalise/pallas_call | solution.py:214
  125.5 3.7 %collective-permute-done.21 = bf16[8,64,704]{2,1,0:T(8,128)(2,1)S(1)} collective-permute-done((bf16[8,64,704]{2,1,0:T(8,128)(2,1)S(1)}, bf16[8,64,704]{2,1,0:T(8,128)(2,1)S(1)}, u32[]{:S(2)}, u32[]{:S(2)}) %collective-permute-start.21) | collective-permute-done | bytes 720928 | tf_op jit(solution)/shard_map/ppermute | solution.py:41
  129.2 1.1 collective-permute-done.22
  130.4 3.6 %collective-permute-start.28 = (bf16[8,64,704]{2,1,0:T(8,128)(2,1)S(1)}, bf16[8,64,704]{2,1,0:T(8,128)(2,1)S(1)}, u32[]{:S(2)}, u32[]{:S(2)}) collective-permute-start(bf16[8,64,704]{2,1,0:T(8,128)(2,1)S(1)} %broadcast_select_fusion), channel_id=1, source_target_pairs={{0,8},{1,25},{2,10},{3,27},{4,12},{5,29},{6,14},{7,31},{8,16},{9,1... | collective-permute-start | bytes 2162696 | tf_op jit(solution)/shard_map/ppermute | solution.py:33
  134.6 1.2 bitcast_dynamic-update-slice_fusion.7
  136.2 3.0 %shard_map.118.value_ref = bf16[768,768]{1,0:T(8,128)(2,1)S(1)} custom-call(bf16[768,2048]{1,0:T(8,128)(2,1)S(1)} %normalise.1.left_ref, bf16[2048,1408]{1,0:T(8,128)(2,1)S(1)} %bitcast.71), custom_call_target="tpu_custom_call" | custom-call | flops 3000000000 | bytes 8388608 | tf_op jit(solution)/shard_map/pallas_call | solution.py:239
  139.2 5.7 %collective-permute-start.26 = (bf16[1,704]{1,0:T(2,128)(2,1)S(1)}, bf16[1,704]{1,0:T(2,128)(2,1)S(1)}, u32[]{:S(2)}, u32[]{:S(2)}) collective-permute-start(bf16[1,704]{1,0:T(2,128)(2,1)S(1)} %get-tuple-element.55), channel_id=1, source_target_pairs={{0,8},{8,16},{16,24},{24,32},{32,40},{40,48},{48,56},{56,64},{64,7... | collective-permute-start | bytes 4232 | tf_op jit(solution)/shard_map/ppermute | solution.py:423
  144.9 1.9 %collective-permute-start.27 = (bf16[1,704]{1,0:T(2,128)(2,1)S(1)}, bf16[1,704]{1,0:T(2,128)(2,1)S(1)}, u32[]{:S(2)}, u32[]{:S(2)}) collective-permute-start(bf16[1,704]{1,0:T(2,128)(2,1)S(1)} %get-tuple-element.54), channel_id=1, source_target_pairs={{8,0},{16,8},{24,16},{32,24},{40,32},{48,40},{56,48},{64,56},{72,6... | collective-permute-start | bytes 4232 | tf_op jit(solution)/shard_map/ppermute | solution.py:424
  146.8 3.0 %shard_map.119.gate_ref = bf16[768,640]{1,0:T(8,128)(2,1)S(1)} custom-call(bf16[768,2048]{1,0:T(8,128)(2,1)S(1)} %normalise.1.left_ref, bf16[2048,1408]{1,0:T(8,128)(2,1)S(1)} %bitcast.72), custom_call_target="tpu_custom_call" | custom-call | flops 3000000000 | bytes 8388608 | tf_op jit(solution)/shard_map/pallas_call | solution.py:239
  150.4 2.9 %hidden_units.1 = bf16[768,704]{1,0:T(8,128)(2,1)S(1)} custom-call(bf16[768,768]{1,0:T(8,128)(2,1)S(1)} %shard_map.118.value_ref, bf16[768,640]{1,0:T(8,128)(2,1)S(1)} %shard_map.119.gate_ref, f32[768,128]{1,0:T(8,128)S(1)} %get-tuple-element.42.same_ref, bf16[1,704]{1,0:T(2,128)(2,1)S(1)} %collective-permute-done.26.before_ref, ...), custom_call_target="tpu_custom_call" | custom-call | flops 2000000000 | bytes 4194304 | tf_op jit(solution)/shard_map/hidden_units/pallas_call | solution.py:298
  153.6 1.4 convolution_convert_fusion
  155.1 3.4 %collective-permute-done.29 = bf16[768,1024]{1,0:T(8,128)(2,1)S(1)} collective-permute-done((bf16[768,1024]{1,0:T(8,128)(2,1)S(1)}, bf16[768,1024]{1,0:T(8,128)(2,1)S(1)}, u32[]{:S(2)}, u32[]{:S(2)}) %collective-permute-start.29) | collective-permute-done | bytes 1572896 | tf_op jit(solution)/shard_map/ppermute | solution.py:45
  158.5 1.5 add_convert_fusion
  160.3 3.1 %collective-permute-start.32 = (bf16[768,256]{1,0:T(8,128)(2,1)S(1)}, bf16[768,256]{1,0:T(8,128)(2,1)S(1)}, u32[]{:S(2)}, u32[]{:S(2)}) collective-permute-start(bf16[768,256]{1,0:T(8,128)(2,1)S(1)} %get-tuple-element.52), channel_id=1, source_target_pairs={{0,6},{2,0},{4,2},{6,4},{1,7},{3,1},{5,3},{7,5},{8,14},{10,8},{12,... | collective-permute-start | bytes 1179656 | tf_op jit(solution)/shard_map/ppermute | solution.py:312
  163.4 17.6 %collective-permute-done.30 = bf16[768,256]{1,0:T(8,128)(2,1)S(1)} collective-permute-done((bf16[768,256]{1,0:T(8,128)(2,1)S(1)}, bf16[768,256]{1,0:T(8,128)(2,1)S(1)}, u32[]{:S(2)}, u32[]{:S(2)}) %collective-permute-start.30) | collective-permute-done | bytes 393248 | tf_op jit(solution)/shard_map/ppermute | solution.py:312
  181.6 1.0 add_convert_fusion.1
  (81 shorter events, 15.0 us)
Async XLA Ops:
  1.7 8.7 %collective-permute-start = (bf16[129,128]{1,0:T(8,128)(2,1)S(1)}, bf16[129,128]{1,0:T(8,128)(2,1)S(1)}, u32[]{:S(2)}, u32[]{:S(2)}) collective-permute-start(bf16[129,128]{1,0:T(8,128)(2,1)S(1)} %get-tuple-element.57), channel_id=1, source_target_pairs={{0,8},{8,16},{16,24},{24,32},{32,40},{40,48},{48,56},{56,64},{64,7... | collective-permute-start | bytes 99080 | tf_op jit(solution)/shard_map/ppermute | solution.py:346
  5.1 5.8 %collective-permute-start.1 = (bf16[129,128]{1,0:T(8,128)(2,1)S(1)}, bf16[129,128]{1,0:T(8,128)(2,1)S(1)}, u32[]{:S(2)}, u32[]{:S(2)}) collective-permute-start(bf16[129,128]{1,0:T(8,128)(2,1)S(1)} %get-tuple-element.56), channel_id=1, source_target_pairs={{8,0},{16,8},{24,16},{32,24},{40,32},{48,40},{56,48},{64,56},{72,6... | collective-permute-start | bytes 99080 | tf_op jit(solution)/shard_map/ppermute | solution.py:347
  10.9 1.2 copy-start
  12.1 1.0 copy-start.1
  13.1 0.7 copy-start.4
  21.6 37.4 %collective-permute-start.2 = (bf16[4,768,256]{2,1,0:T(8,128)(2,1)S(1)}, bf16[4,768,256]{2,1,0:T(8,128)(2,1)S(1)}, u32[]{:S(2)}, u32[]{:S(2)}) collective-permute-start(bf16[4,768,256]{2,1,0:T(8,128)(2,1)S(1)} %get-tuple-element.25), channel_id=1, source_target_pairs={{0,1},{1,0},{2,3},{3,2},{4,5},{5,4},{6,7},{7,6},{8,9},{9,8},{10,11... | collective-permute-start | bytes 4718600 | tf_op jit(solution)/shard_map/ppermute | solution.py:45
  38.6 17.2 %collective-permute-start.9 = (bf16[256,1408]{1,0:T(8,128)(2,1)S(1)}, bf16[256,1408]{1,0:T(8,128)(2,1)S(1)}, u32[]{:S(2)}, u32[]{:S(2)}) collective-permute-start(bf16[256,1408]{1,0:T(8,128)(2,1)S(1)} %all_gather.3), channel_id=1, source_target_pairs={{0,32},{32,64},{64,96},{96,128},{128,160},{160,192},{192,224},{224... | collective-permute-start | bytes 2162696 | tf_op jit(solution)/shard_map/ppermute | solution.py:37
  40.5 16.2 %collective-permute-start.11 = (bf16[256,1408]{1,0:T(8,128)(2,1)S(1)}, bf16[256,1408]{1,0:T(8,128)(2,1)}, u32[]{:S(2)}, u32[]{:S(2)}) collective-permute-start(bf16[256,1408]{1,0:T(8,128)(2,1)S(1)} %all_gather.3), channel_id=1, source_target_pairs={{0,224},{32,0},{64,32},{96,64},{128,96},{160,128},{192,160},{224,1... | collective-permute-start | bytes 2162696 | tf_op jit(solution)/shard_map/ppermute | solution.py:37
  55.8 21.9 %copy-start.5 = (bf16[256,1408]{1,0:T(8,128)(2,1)}, bf16[256,1408]{1,0:T(8,128)(2,1)S(1)}, u32[]{:S(2)}) copy-start(bf16[256,1408]{1,0:T(8,128)(2,1)S(1)} %collective-permute-done.9) | copy-start | bytes 2162692
  55.8 18.9 %collective-permute-start.10 = (bf16[256,1408]{1,0:T(8,128)(2,1)S(1)}, bf16[256,1408]{1,0:T(8,128)(2,1)S(1)}, u32[]{:S(2)}, u32[]{:S(2)}) collective-permute-start(bf16[256,1408]{1,0:T(8,128)(2,1)S(1)} %collective-permute-done.9), channel_id=1, source_target_pairs={{0,32},{32,64},{64,96},{96,128},{128,160},{160,192},{192,224},{224... | collective-permute-start | bytes 2162696 | tf_op jit(solution)/shard_map/ppermute | solution.py:37
  56.7 40.1 %collective-permute-start.12 = (bf16[256,1408]{1,0:T(8,128)(2,1)}, bf16[256,1408]{1,0:T(8,128)(2,1)}, u32[]{:S(2)}, u32[]{:S(2)}) collective-permute-start(bf16[256,1408]{1,0:T(8,128)(2,1)} %collective-permute-done.11), channel_id=1, source_target_pairs={{0,224},{32,0},{64,32},{96,64},{128,96},{160,128},{192,160},{224,1... | collective-permute-start | bytes 2162696 | tf_op jit(solution)/shard_map/ppermute | solution.py:37
  59.4 18.3 %collective-permute-start.16 = (bf16[64,704]{1,0:T(8,128)(2,1)}, bf16[64,704]{1,0:T(8,128)(2,1)S(1)}, u32[]{:S(2)}, u32[]{:S(2)}) collective-permute-start(bf16[64,704]{1,0:T(8,128)(2,1)} %param.23), channel_id=1, source_target_pairs={{0,64},{32,96},{64,128},{96,160},{128,192},{160,224},{192,0},{224,... | collective-permute-start | bytes 270344 | tf_op jit(solution)/shard_map/ppermute | solution.py:37
  62.9 23.9 %collective-permute-start.3 = (bf16[768,256]{1,0:T(8,128)(2,1)S(1)}, bf16[768,256]{1,0:T(8,128)(2,1)}, u32[]{:S(2)}, u32[]{:S(2)}) collective-permute-start(bf16[768,256]{1,0:T(8,128)(2,1)S(1)} %get-tuple-element.27), channel_id=1, source_target_pairs={{0,2},{2,4},{4,6},{6,0},{1,3},{3,5},{5,7},{7,1},{8,10},{10,12},{12... | collective-permute-start | bytes 1179656 | tf_op jit(solution)/shard_map/ppermute | solution.py:312
  64.5 24.8 %collective-permute-start.4 = (bf16[768,256]{1,0:T(8,128)(2,1)S(1)}, bf16[768,256]{1,0:T(8,128)(2,1)}, u32[]{:S(2)}, u32[]{:S(2)}) collective-permute-start(bf16[768,256]{1,0:T(8,128)(2,1)S(1)} %get-tuple-element.28), channel_id=1, source_target_pairs={{0,4},{2,6},{4,0},{6,2},{1,5},{3,7},{5,1},{7,3},{8,12},{10,14},{12... | collective-permute-start | bytes 1179656 | tf_op jit(solution)/shard_map/ppermute | solution.py:312
  74.6 15.6 %collective-permute-start.5 = (bf16[768,256]{1,0:T(8,128)(2,1)S(1)}, bf16[768,256]{1,0:T(8,128)(2,1)}, u32[]{:S(2)}, u32[]{:S(2)}) collective-permute-start(bf16[768,256]{1,0:T(8,128)(2,1)S(1)} %get-tuple-element.29), channel_id=1, source_target_pairs={{0,6},{2,0},{4,2},{6,4},{1,7},{3,1},{5,3},{7,5},{8,14},{10,8},{12,... | collective-permute-start | bytes 1179656 | tf_op jit(solution)/shard_map/ppermute | solution.py:312
  77.7 6.7 %collective-permute-start.17 = (bf16[64,704]{1,0:T(8,128)(2,1)}, bf16[64,704]{1,0:T(8,128)(2,1)}, u32[]{:S(2)}, u32[]{:S(2)}) collective-permute-start(bf16[64,704]{1,0:T(8,128)(2,1)} %param.23), channel_id=1, source_target_pairs={{0,192},{32,224},{64,0},{96,32},{128,64},{160,96},{192,128},{224,1... | collective-permute-start | bytes 270344 | tf_op jit(solution)/shard_map/ppermute | solution.py:37
  84.4 37.5 %collective-permute-start.23 = (bf16[256,1408]{1,0:T(8,128)(2,1)S(1)}, bf16[256,1408]{1,0:T(8,128)(2,1)S(1)}, u32[]{:S(2)}, u32[]{:S(2)}) collective-permute-start(bf16[256,1408]{1,0:T(8,128)(2,1)S(1)} %collective-permute-done.10), channel_id=1, source_target_pairs={{0,32},{32,64},{64,96},{96,128},{128,160},{160,192},{192,224},{224... | collective-permute-start | bytes 2162696 | tf_op jit(solution)/shard_map/ppermute | solution.py:37
  86.7 14.2 %collective-permute-start.14 = (bf16[64,704]{1,0:T(8,128)(2,1)}, bf16[64,704]{1,0:T(8,128)(2,1)S(1)}, u32[]{:S(2)}, u32[]{:S(2)}) collective-permute-start(bf16[64,704]{1,0:T(8,128)(2,1)} %param.23), channel_id=1, source_target_pairs={{0,32},{32,64},{64,96},{96,128},{128,160},{160,192},{192,224},{224... | collective-permute-start | bytes 270344 | tf_op jit(solution)/shard_map/ppermute | solution.py:37
  89.3 13.5 %collective-permute-start.15 = (bf16[64,704]{1,0:T(8,128)(2,1)}, bf16[64,704]{1,0:T(8,128)(2,1)S(1)}, u32[]{:S(2)}, u32[]{:S(2)}) collective-permute-start(bf16[64,704]{1,0:T(8,128)(2,1)} %param.23), channel_id=1, source_target_pairs={{0,224},{32,0},{64,32},{96,64},{128,96},{160,128},{192,160},{224,1... | collective-permute-start | bytes 270344 | tf_op jit(solution)/shard_map/ppermute | solution.py:37
  90.3 19.9 %collective-permute-start.20 = (bf16[64,704]{1,0:T(8,128)(2,1)S(1)}, bf16[64,704]{1,0:T(8,128)(2,1)S(1)}, u32[]{:S(2)}, u32[]{:S(2)}) collective-permute-start(bf16[64,704]{1,0:T(8,128)(2,1)S(1)} %broadcast_select_fusion.2), channel_id=1, source_target_pairs={{0,64},{1,193},{2,66},{3,195},{4,68},{5,197},{6,70},{7,199},{8,72}... | collective-permute-start | bytes 270344 | tf_op jit(solution)/shard_map/ppermute | solution.py:33
  96.8 8.4 %collective-permute-start.18 = (bf16[64,704]{1,0:T(8,128)(2,1)S(1)}, bf16[64,704]{1,0:T(8,128)(2,1)S(1)}, u32[]{:S(2)}, u32[]{:S(2)}) collective-permute-start(bf16[64,704]{1,0:T(8,128)(2,1)S(1)} %collective-permute-done.16), channel_id=1, source_target_pairs={{0,32},{32,64},{64,96},{96,128},{128,160},{160,192},{192,224},{224... | collective-permute-start | bytes 270344 | tf_op jit(solution)/shard_map/ppermute | solution.py:37
  101.0 7.4 %collective-permute-start.19 = (bf16[64,704]{1,0:T(8,128)(2,1)}, bf16[64,704]{1,0:T(8,128)(2,1)S(1)}, u32[]{:S(2)}, u32[]{:S(2)}) collective-permute-start(bf16[64,704]{1,0:T(8,128)(2,1)} %collective-permute-done.17), channel_id=1, source_target_pairs={{0,224},{32,0},{64,32},{96,64},{128,96},{160,128},{192,160},{224,1... | collective-permute-start | bytes 270344 | tf_op jit(solution)/shard_map/ppermute | solution.py:37
  102.7 10.6 %collective-permute-start.6 = (bf16[768,256]{1,0:T(8,128)(2,1)S(1)}, bf16[768,256]{1,0:T(8,128)(2,1)S(1)}, u32[]{:S(2)}, u32[]{:S(2)}) collective-permute-start(bf16[768,256]{1,0:T(8,128)(2,1)S(1)} %add_convert_fusion.2.p0), channel_id=1, source_target_pairs={{0,2},{2,4},{4,6},{6,0},{1,3},{3,5},{5,7},{7,1},{8,10},{10,12},{12... | collective-permute-start | bytes 1179656 | tf_op jit(solution)/shard_map/ppermute | solution.py:312
  105.2 12.3 %collective-permute-start.7 = (bf16[768,256]{1,0:T(8,128)(2,1)S(1)}, bf16[768,256]{1,0:T(8,128)(2,1)S(1)}, u32[]{:S(2)}, u32[]{:S(2)}) collective-permute-start(bf16[768,256]{1,0:T(8,128)(2,1)S(1)} %add_convert_fusion.2.p0), channel_id=1, source_target_pairs={{0,4},{2,6},{4,0},{6,2},{1,5},{3,7},{5,1},{7,3},{8,12},{10,14},{12... | collective-permute-start | bytes 1179656 | tf_op jit(solution)/shard_map/ppermute | solution.py:312
  108.4 10.9 %collective-permute-start.8 = (bf16[768,256]{1,0:T(8,128)(2,1)S(1)}, bf16[768,256]{1,0:T(8,128)(2,1)S(1)}, u32[]{:S(2)}, u32[]{:S(2)}) collective-permute-start(bf16[768,256]{1,0:T(8,128)(2,1)S(1)} %add_convert_fusion.2.p0), channel_id=1, source_target_pairs={{0,6},{2,0},{4,2},{6,4},{1,7},{3,1},{5,3},{7,5},{8,14},{10,8},{12,... | collective-permute-start | bytes 1179656 | tf_op jit(solution)/shard_map/ppermute | solution.py:312
  110.1 11.9 %collective-permute-start.24 = (bf16[256,1408]{1,0:T(8,128)(2,1)}, bf16[256,1408]{1,0:T(8,128)(2,1)S(1)}, u32[]{:S(2)}, u32[]{:S(2)}) collective-permute-start(bf16[256,1408]{1,0:T(8,128)(2,1)} %collective-permute-done.12), channel_id=1, source_target_pairs={{0,224},{32,0},{64,32},{96,64},{128,96},{160,128},{192,160},{224,1... | collective-permute-start | bytes 2162696 | tf_op jit(solution)/shard_map/ppermute | solution.py:37
  113.3 15.9 %collective-permute-start.21 = (bf16[8,64,704]{2,1,0:T(8,128)(2,1)S(1)}, bf16[8,64,704]{2,1,0:T(8,128)(2,1)S(1)}, u32[]{:S(2)}, u32[]{:S(2)}) collective-permute-start(bf16[8,64,704]{2,1,0:T(8,128)(2,1)S(1)} %bitcast_dynamic-update-slice_fusion.12), channel_id=1, source_target_pairs={{0,8},{8,16},{16,24},{24,0},{1,9},{9,17},{17,25},{25,1},{2,10},{10... | collective-permute-start | bytes 2162696 | tf_op jit(solution)/shard_map/ppermute | solution.py:41
  117.5 12.8 %collective-permute-start.22 = (bf16[8,64,704]{2,1,0:T(8,128)(2,1)S(1)}, bf16[8,64,704]{2,1,0:T(8,128)(2,1)S(1)}, u32[]{:S(2)}, u32[]{:S(2)}) collective-permute-start(bf16[8,64,704]{2,1,0:T(8,128)(2,1)S(1)} %bitcast_dynamic-update-slice_fusion.12), channel_id=1, source_target_pairs={{0,24},{8,0},{16,8},{24,16},{1,25},{9,1},{17,9},{25,17},{2,26},{10... | collective-permute-start | bytes 2162696 | tf_op jit(solution)/shard_map/ppermute | solution.py:41
  119.4 1.1 copy-start.6
  119.5 3.5 %collective-permute-start.13 = (bf16[4,768,256]{2,1,0:T(8,128)(2,1)S(1)}, bf16[4,768,256]{2,1,0:T(8,128)(2,1)S(1)}, u32[]{:S(2)}, u32[]{:S(2)}) collective-permute-start(bf16[4,768,256]{2,1,0:T(8,128)(2,1)S(1)} %pad_maximum_fusion), channel_id=1, source_target_pairs={{0,1},{1,0},{2,3},{3,2},{4,5},{5,4},{6,7},{7,6},{8,9},{9,8},{10,11... | collective-permute-start | bytes 4718600 | tf_op jit(solution)/shard_map/ppermute | solution.py:45
  120.0 3.0 %copy-start.2 = (f32[2048]{0:T(1024)S(1)}, f32[2048]{0:T(1024)}, u32[]{:S(2)}) copy-start(f32[2048]{0:T(1024)} %param.19) | copy-start | bytes 24580
  122.2 13.9 %collective-permute-start.25 = (bf16[256,1408]{1,0:T(8,128)(2,1)S(1)}, bf16[256,1408]{1,0:T(8,128)(2,1)S(1)}, u32[]{:S(2)}, u32[]{:S(2)}) collective-permute-start(bf16[256,1408]{1,0:T(8,128)(2,1)S(1)} %broadcast_select_fusion.1), channel_id=1, source_target_pairs={{0,32},{1,225},{2,34},{3,227},{4,36},{5,229},{6,38},{7,231},{8,40}... | collective-permute-start | bytes 2162696 | tf_op jit(solution)/shard_map/ppermute | solution.py:33
  130.4 22.9 %collective-permute-start.28 = (bf16[8,64,704]{2,1,0:T(8,128)(2,1)S(1)}, bf16[8,64,704]{2,1,0:T(8,128)(2,1)S(1)}, u32[]{:S(2)}, u32[]{:S(2)}) collective-permute-start(bf16[8,64,704]{2,1,0:T(8,128)(2,1)S(1)} %broadcast_select_fusion), channel_id=1, source_target_pairs={{0,8},{1,25},{2,10},{3,27},{4,12},{5,29},{6,14},{7,31},{8,16},{9,1... | collective-permute-start | bytes 2162696 | tf_op jit(solution)/shard_map/ppermute | solution.py:33
  139.2 10.6 %collective-permute-start.26 = (bf16[1,704]{1,0:T(2,128)(2,1)S(1)}, bf16[1,704]{1,0:T(2,128)(2,1)S(1)}, u32[]{:S(2)}, u32[]{:S(2)}) collective-permute-start(bf16[1,704]{1,0:T(2,128)(2,1)S(1)} %get-tuple-element.55), channel_id=1, source_target_pairs={{0,8},{8,16},{16,24},{24,32},{32,40},{40,48},{48,56},{56,64},{64,7... | collective-permute-start | bytes 4232 | tf_op jit(solution)/shard_map/ppermute | solution.py:423
  144.9 5.5 %copy-start.3 = (bf16[3,704]{1,0:T(4,128)(2,1)S(1)}, bf16[3,704]{1,0:T(4,128)(2,1)}, u32[]{:S(2)}) copy-start(bf16[3,704]{1,0:T(4,128)(2,1)} %taps_ref.1) | copy-start | bytes 12676
  144.9 5.5 %collective-permute-start.27 = (bf16[1,704]{1,0:T(2,128)(2,1)S(1)}, bf16[1,704]{1,0:T(2,128)(2,1)S(1)}, u32[]{:S(2)}, u32[]{:S(2)}) collective-permute-start(bf16[1,704]{1,0:T(2,128)(2,1)S(1)} %get-tuple-element.54), channel_id=1, source_target_pairs={{8,0},{16,8},{24,16},{32,24},{40,32},{48,40},{56,48},{64,56},{72,6... | collective-permute-start | bytes 4232 | tf_op jit(solution)/shard_map/ppermute | solution.py:424
  155.0 3.5 %collective-permute-start.29 = (bf16[768,1024]{1,0:T(8,128)(2,1)S(1)}, bf16[768,1024]{1,0:T(8,128)(2,1)S(1)}, u32[]{:S(2)}, u32[]{:S(2)}) collective-permute-start(bf16[768,1024]{1,0:T(8,128)(2,1)S(1)} %convolution_convert_fusion), channel_id=1, source_target_pairs={{0,1},{1,0},{2,3},{3,2},{4,5},{5,4},{6,7},{7,6},{8,9},{9,8},{10,11... | collective-permute-start | bytes 4718600 | tf_op jit(solution)/shard_map/ppermute | solution.py:45
  160.1 20.9 %collective-permute-start.30 = (bf16[768,256]{1,0:T(8,128)(2,1)S(1)}, bf16[768,256]{1,0:T(8,128)(2,1)S(1)}, u32[]{:S(2)}, u32[]{:S(2)}) collective-permute-start(bf16[768,256]{1,0:T(8,128)(2,1)S(1)} %get-tuple-element.51), channel_id=1, source_target_pairs={{0,2},{2,4},{4,6},{6,0},{1,3},{3,5},{5,7},{7,1},{8,10},{10,12},{12... | collective-permute-start | bytes 1179656 | tf_op jit(solution)/shard_map/ppermute | solution.py:312
  160.2 20.8 %collective-permute-start.31 = (bf16[768,256]{1,0:T(8,128)(2,1)S(1)}, bf16[768,256]{1,0:T(8,128)(2,1)S(1)}, u32[]{:S(2)}, u32[]{:S(2)}) collective-permute-start(bf16[768,256]{1,0:T(8,128)(2,1)S(1)} %get-tuple-element.53), channel_id=1, source_target_pairs={{0,4},{2,6},{4,0},{6,2},{1,5},{3,7},{5,1},{7,3},{8,12},{10,14},{12... | collective-permute-start | bytes 1179656 | tf_op jit(solution)/shard_map/ppermute | solution.py:312
  160.3 21.3 %collective-permute-start.32 = (bf16[768,256]{1,0:T(8,128)(2,1)S(1)}, bf16[768,256]{1,0:T(8,128)(2,1)S(1)}, u32[]{:S(2)}, u32[]{:S(2)}) collective-permute-start(bf16[768,256]{1,0:T(8,128)(2,1)S(1)} %get-tuple-element.52), channel_id=1, source_target_pairs={{0,6},{2,0},{4,2},{6,4},{1,7},{3,1},{5,3},{7,5},{8,14},{10,8},{12,... | collective-permute-start | bytes 1179656 | tf_op jit(solution)/shard_map/ppermute | solution.py:312

commit v4 on v3

--- a/solution.py
+++ b/solution.py
@@ -352,7 +352,9 @@
         [w_gate_up[:, :tail], first, w_gate_up[:, tail:]], axis=1
     )
     rows_w, width = share.shape
-    up_rows = lax.all_gather(share, "x", axis=0, tiled=True)
+    gathered = []
+    for k in range(1, NX):
+        gathered.append(send_x(share, k))
 
     def ring_step(plus, minus):
         plus = send_z(plus, 1)
@@ -362,10 +364,15 @@
     def keep(full, plus, minus, k):
         return put(put(full, plus, (z - k) % NZ), minus, (z + k) % NZ)
 
-    plus1, minus1 = ring_step(up_rows, up_rows)
-
     theirs, mine, same = attention(order, sink_logits, queries, packed, low, high, w_out)
     got = swap(theirs)
+
+    gathered = lax.optimization_barrier((*gathered, theirs))[:-1]
+    up_rows = put(jnp.zeros((NX, rows_w, width), share.dtype), share, x)
+    for k, piece in enumerate(gathered):
+        up_rows = put(up_rows, piece, (x - k - 1) % NX)
+    up_rows = up_rows.reshape(NX * rows_w, width)
+    plus1, minus1 = ring_step(up_rows, up_rows)
 
     pairs = pair_sums(mine, got)
     sent = to_owners(pairs)
@@ -376,16 +383,15 @@
     far_minus = send_z(down1, -2)
 
     plus2, minus2 = ring_step(plus1, minus1)
-    third = ring_step(far_plus, far_minus)
-    last = send_apart(jnp.where(core == 0, far_plus, far_minus), 2, 0)
-    last_down = last
-
     own_res = lax.dynamic_slice_in_dim(residual, tp * span, span, 1)
-    total = own_res.astype(jnp.float32)
     summed = pairs[0].astype(jnp.float32)
     for block in sent:
         summed = summed + block.astype(jnp.float32)
-    mixed_own = (total + summed).astype(jnp.bfloat16)
+    mixed_own = (own_res.astype(jnp.float32) + summed).astype(jnp.bfloat16)
+
+    far_plus, far_minus = lax.optimization_barrier((far_plus, far_minus, mixed_own))[:2]
+    third = ring_step(far_plus, far_minus)
+    last_down = send_apart(jnp.where(core == 0, far_plus, far_minus), 2, 0)
 
     came = to_owners([mixed_own] * NY)
     came = lax.optimization_barrier((*came, plus2, minus2))[: NY - 1]

time: 186 us -> 184 us (0.989); the launches traced: 183 us -> 183 us
  waiting for transfers between devices: 59.2 us -> 87.8 us
  blocking collectives: 16.9 us -> 0 us
  starting transfers between devices: 66.4 us -> 55.9 us
    ppermute x9, waiting for transfers between devices: 21.9 us -> 44 us  [to_owners(): lax.ppermute(pairs[k], 'y', [(y, (y + k) % NY) for y in range(NY)])]
    all_gather x1 -> x0, blocking collectives: 16.9 us -> none  [per_device(): up_rows = lax.all_gather(share, 'x', axis=0, tiled=True)]
    ppermute x2 -> x5, waiting for transfers between devices: 4.77 us -> 14.1 us  [send_x(): return lax.ppermute(block, 'x', [(x, (x + k) % NX) for x in range(NX)])]
    ppermute x12, starting transfers between devices: 23.9 us -> 16.5 us  [send_z(): return lax.ppermute(block, 'z', [(z, (z + k) % NZ) for z in range(NZ)])]
    ppermute x12, waiting for transfers between devices: 27.8 us -> 20.5 us  [send_z(): return lax.ppermute(block, 'z', [(z, (z + k) % NZ) for z in range(NZ)])]
    ppermute x3, starting transfers between devices: 9.11 us -> 4.94 us  [send_apart(): return lax.ppermute(block, AXES, pairs)]
    ppermute x2 -> x5, starting transfers between devices: 2.53 us -> 6.34 us  [send_x(): return lax.ppermute(block, 'x', [(x, (x + k) % NX) for x in range(NX)])]
    ppermute x1, starting transfers between devices: 5.65 us -> 2.12 us  [per_device(): before = lax.ppermute(up_value[-1:, :ff], ('z', 'x'), forward)]
  transfers between devices with their start and end apart: 33 -> 36, of which waited for: 15 -> 14; matrix products, arithmetic and copies ran while one was open for 6% -> 4% of each run, Pallas kernels for 6% -> 11%
where the time goes in v4:
time: 184 us; the launch traced here: 183 us
  waiting for transfers between devices  87.8 us (48%)
  starting transfers between devices  55.9 us (30%)
  Pallas kernels  19.6 us (11%)
  local copies, waits for them, and re-layouts  11.4 us (6%)
  other arithmetic  4.69 us (3%)
  matrix products  2.85 us (2%)
    ppermute x9, waiting for transfers between devices, to_owners(): lax.ppermute(pairs[k], 'y', [(y, (y + k) % NY) for y in range(NY)])  44 us
    ppermute x12, waiting for transfers between devices, send_z(): return lax.ppermute(block, 'z', [(z, (z + k) % NZ) for z in range(NZ)])  20.5 us
    ppermute x12, starting transfers between devices, send_z(): return lax.ppermute(block, 'z', [(z, (z + k) % NZ) for z in range(NZ)])  16.5 us
    ppermute x9, starting transfers between devices, to_owners(): lax.ppermute(pairs[k], 'y', [(y, (y + k) % NY) for y in range(NY)])  16.2 us
    ppermute x5, waiting for transfers between devices, send_x(): return lax.ppermute(block, 'x', [(x, (x + k) % NX) for x in range(NX)])  14.1 us
    pallas_call x1, Pallas kernels, attention(): pl.pallas_call(attention_kernel, out_shape=[jax.ShapeDtypeStruct((NY, row...  7.75 us
    ppermute x5, starting transfers between devices, send_x(): return lax.ppermute(block, 'x', [(x, (x + k) % NX) for x in range(NX)])  6.34 us
    pallas_call x2, Pallas kernels, up(): pl.pallas_call(functools.partial(up_kernel, start), out_shape=jax.ShapeDt...  6.02 us
  transfers between devices with their start and end apart: 36, of which 14 were waited for; matrix products, arithmetic and copies ran while one was open for 4% of the time, Pallas kernels for 11%

profile of v4, /device:TPU:2, one launch (start us, length us, event | category | flops | bytes accessed | tf_op | source)
XLA Modules:
  0.0 182.9 jit_solution(4023677972965991019)
XLA Ops:
  4.3 2.2 %collective-permute-start.10 = (bf16[64,1408]{1,0:T(8,128)(2,1)S(1)}, bf16[64,1408]{1,0:T(8,128)(2,1)S(1)}, u32[]{:S(2)}, u32[]{:S(2)}) collective-permute-start(bf16[64,1408]{1,0:T(8,128)(2,1)S(1)} %concatenate.13), channel_id=1, source_target_pairs={{0,16},{8,24},{16,0},{24,8},{1,17},{9,25},{17,1},{25,9},{2,18},{10... | collective-permute-start | bytes 540680 | tf_op jit(solution)/shard_map/ppermute | solution.py:41
  6.5 1.4 collective-permute-start.11
  8.5 3.5 %collective-permute-start = (bf16[129,128]{1,0:T(8,128)(2,1)S(1)}, bf16[129,128]{1,0:T(8,128)(2,1)S(1)}, u32[]{:S(2)}, u32[]{:S(2)}) collective-permute-start(bf16[129,128]{1,0:T(8,128)(2,1)S(1)} %get-tuple-element.67), channel_id=1, source_target_pairs={{0,8},{8,16},{16,24},{24,32},{32,40},{40,48},{48,56},{56,64},{64,7... | collective-permute-start | bytes 99080 | tf_op jit(solution)/shard_map/ppermute | solution.py:346
  12.0 2.4 %collective-permute-start.1 = (bf16[129,128]{1,0:T(8,128)(2,1)S(1)}, bf16[129,128]{1,0:T(8,128)(2,1)S(1)}, u32[]{:S(2)}, u32[]{:S(2)}) collective-permute-start(bf16[129,128]{1,0:T(8,128)(2,1)S(1)} %get-tuple-element.66), channel_id=1, source_target_pairs={{8,0},{16,8},{24,16},{32,24},{40,32},{48,40},{56,48},{64,56},{72,6... | collective-permute-start | bytes 99080 | tf_op jit(solution)/shard_map/ppermute | solution.py:347
  14.7 2.1 %collective-permute-done.low_ref = bf16[129,128]{1,0:T(8,128)(2,1)S(1)} collective-permute-done((bf16[129,128]{1,0:T(8,128)(2,1)S(1)}, bf16[129,128]{1,0:T(8,128)(2,1)S(1)}, u32[]{:S(2)}, u32[]{:S(2)}) %collective-permute-start) | collective-permute-done | bytes 33056 | tf_op jit(solution)/shard_map/ppermute | solution.py:346
  16.8 1.0 collective-permute-done.1.high_ref
  17.8 1.2 copy-done
  20.7 7.8 %attention.1 = (bf16[4,768,256]{2,1,0:T(8,128)(2,1)S(1)}, bf16[4,768,256]{2,1,0:T(8,128)(2,1)S(1)}, f32[768,128]{1,0:T(8,128)S(1)}) custom-call(s32[16]{0:T(128)S(1)} %stack.76.at_ref, f32[4]{0:T(128)S(1)} %copy-done.4, bf16[768,256]{1,0:T(8,128)(2,1)S(1)} %copy-done.1, bf16[256,2048]{1,0:T(8,128)(2,1)S(1)} %copy-done, ...), custom_call_target="tpu_custom_call" | custom-call | flops 4000000000 | bytes 4194304 | tf_op jit(solution)/shard_map/attention/pallas_call | solution.py:152
  28.7 1.6 collective-permute-start.12
  30.3 4.0 %collective-permute-start.14 = (bf16[256,1408]{1,0:T(8,128)(2,1)S(1)}, bf16[256,1408]{1,0:T(8,128)(2,1)}, u32[]{:S(2)}, u32[]{:S(2)}) collective-permute-start(bf16[256,1408]{1,0:T(8,128)(2,1)S(1)} %bitcast.89), channel_id=1, source_target_pairs={{0,224},{32,0},{64,32},{96,64},{128,96},{160,128},{192,160},{224,1... | collective-permute-start | bytes 2162696 | tf_op jit(solution)/shard_map/ppermute | solution.py:37
  34.3 16.8 %collective-permute-done.12 = bf16[256,1408]{1,0:T(8,128)(2,1)} collective-permute-done((bf16[256,1408]{1,0:T(8,128)(2,1)S(1)}, bf16[256,1408]{1,0:T(8,128)(2,1)}, u32[]{:S(2)}, u32[]{:S(2)}) %collective-permute-start.12) | collective-permute-done | bytes 720928 | tf_op jit(solution)/shard_map/ppermute | solution.py:37
  51.1 3.2 %collective-permute-start.15 = (bf16[256,1408]{1,0:T(8,128)(2,1)}, bf16[256,1408]{1,0:T(8,128)(2,1)}, u32[]{:S(2)}, u32[]{:S(2)}) collective-permute-start(bf16[256,1408]{1,0:T(8,128)(2,1)} %collective-permute-done.14), channel_id=1, source_target_pairs={{0,224},{32,0},{64,32},{96,64},{128,96},{160,128},{192,160},{224,1... | collective-permute-start | bytes 2162696 | tf_op jit(solution)/shard_map/ppermute | solution.py:37
  54.7 1.6 collective-permute-start.3
  56.4 2.9 %collective-permute-start.4 = (bf16[768,256]{1,0:T(8,128)(2,1)S(1)}, bf16[768,256]{1,0:T(8,128)(2,1)}, u32[]{:S(2)}, u32[]{:S(2)}) collective-permute-start(bf16[768,256]{1,0:T(8,128)(2,1)S(1)} %get-tuple-element.33), channel_id=1, source_target_pairs={{0,4},{2,6},{4,0},{6,2},{1,5},{3,7},{5,1},{7,3},{8,12},{10,14},{12... | collective-permute-start | bytes 1179656 | tf_op jit(solution)/shard_map/ppermute | solution.py:312
  59.3 1.4 collective-permute-start.5
  60.6 6.3 %collective-permute-done.3 = bf16[768,256]{1,0:T(8,128)(2,1)} collective-permute-done((bf16[768,256]{1,0:T(8,128)(2,1)S(1)}, bf16[768,256]{1,0:T(8,128)(2,1)}, u32[]{:S(2)}, u32[]{:S(2)}) %collective-permute-start.3) | collective-permute-done | bytes 393248 | tf_op jit(solution)/shard_map/ppermute | solution.py:312
  67.0 9.2 %collective-permute-done.4 = bf16[768,256]{1,0:T(8,128)(2,1)} collective-permute-done((bf16[768,256]{1,0:T(8,128)(2,1)S(1)}, bf16[768,256]{1,0:T(8,128)(2,1)}, u32[]{:S(2)}, u32[]{:S(2)}) %collective-permute-start.4) | collective-permute-done | bytes 393248 | tf_op jit(solution)/shard_map/ppermute | solution.py:312
  76.8 1.1 collective-permute-start.17
  77.9 1.6 add_convert_fusion.2.p0
  79.5 2.3 %collective-permute-start.18 = (bf16[64,704]{1,0:T(8,128)(2,1)S(1)}, bf16[64,704]{1,0:T(8,128)(2,1)S(1)}, u32[]{:S(2)}, u32[]{:S(2)}) collective-permute-start(bf16[64,704]{1,0:T(8,128)(2,1)S(1)} %copy-done.5), channel_id=1, source_target_pairs={{0,224},{32,0},{64,32},{96,64},{128,96},{160,128},{192,160},{224,1... | collective-permute-start | bytes 270344 | tf_op jit(solution)/shard_map/ppermute | solution.py:37
  81.8 3.2 %collective-permute-start.27 = (bf16[256,1408]{1,0:T(8,128)(2,1)}, bf16[256,1408]{1,0:T(8,128)(2,1)S(1)}, u32[]{:S(2)}, u32[]{:S(2)}) collective-permute-start(bf16[256,1408]{1,0:T(8,128)(2,1)} %collective-permute-done.15), channel_id=1, source_target_pairs={{0,224},{32,0},{64,32},{96,64},{128,96},{160,128},{192,160},{224,1... | collective-permute-start | bytes 2162696 | tf_op jit(solution)/shard_map/ppermute | solution.py:37
  85.7 3.7 %collective-permute-start.7 = (bf16[768,256]{1,0:T(8,128)(2,1)S(1)}, bf16[768,256]{1,0:T(8,128)(2,1)S(1)}, u32[]{:S(2)}, u32[]{:S(2)}) collective-permute-start(bf16[768,256]{1,0:T(8,128)(2,1)S(1)} %add_convert_fusion.2.p0), channel_id=1, source_target_pairs={{0,4},{2,6},{4,0},{6,2},{1,5},{3,7},{5,1},{7,3},{8,12},{10,14},{12... | collective-permute-start | bytes 1179656 | tf_op jit(solution)/shard_map/ppermute | solution.py:312
  89.5 2.7 %collective-permute-start.8 = (bf16[768,256]{1,0:T(8,128)(2,1)S(1)}, bf16[768,256]{1,0:T(8,128)(2,1)S(1)}, u32[]{:S(2)}, u32[]{:S(2)}) collective-permute-start(bf16[768,256]{1,0:T(8,128)(2,1)S(1)} %add_convert_fusion.2.p0), channel_id=1, source_target_pairs={{0,6},{2,0},{4,2},{6,4},{1,7},{3,1},{5,3},{7,5},{8,14},{10,8},{12,... | collective-permute-start | bytes 1179656 | tf_op jit(solution)/shard_map/ppermute | solution.py:312
  92.7 1.2 bitcast_dynamic-update-slice_fusion.10
  93.9 2.9 %collective-permute-done.6.p1 = bf16[768,256]{1,0:T(8,128)(2,1)S(1)} collective-permute-done((bf16[768,256]{1,0:T(8,128)(2,1)S(1)}, bf16[768,256]{1,0:T(8,128)(2,1)S(1)}, u32[]{:S(2)}, u32[]{:S(2)}) %collective-permute-start.6) | collective-permute-done | bytes 393248 | tf_op jit(solution)/shard_map/ppermute | solution.py:312
  96.8 7.4 %collective-permute-done.7.p2 = bf16[768,256]{1,0:T(8,128)(2,1)S(1)} collective-permute-done((bf16[768,256]{1,0:T(8,128)(2,1)S(1)}, bf16[768,256]{1,0:T(8,128)(2,1)S(1)}, u32[]{:S(2)}, u32[]{:S(2)}) %collective-permute-start.7) | collective-permute-done | bytes 393248 | tf_op jit(solution)/shard_map/ppermute | solution.py:312
  105.2 3.7 %collective-permute-done.22 = bf16[64,704]{1,0:T(8,128)(2,1)S(1)} collective-permute-done((bf16[64,704]{1,0:T(8,128)(2,1)S(1)}, bf16[64,704]{1,0:T(8,128)(2,1)S(1)}, u32[]{:S(2)}, u32[]{:S(2)}) %collective-permute-start.22) | collective-permute-done | bytes 90144 | tf_op jit(solution)/shard_map/ppermute | solution.py:37
  108.9 2.7 %collective-permute-done.23 = bf16[64,704]{1,0:T(8,128)(2,1)S(1)} collective-permute-done((bf16[64,704]{1,0:T(8,128)(2,1)S(1)}, bf16[64,704]{1,0:T(8,128)(2,1)S(1)}, u32[]{:S(2)}, u32[]{:S(2)}) %collective-permute-start.23) | collective-permute-done | bytes 90144 | tf_op jit(solution)/shard_map/ppermute | solution.py:33
  111.6 2.1 %collective-permute-start.24 = (bf16[8,64,704]{2,1,0:T(8,128)(2,1)S(1)}, bf16[8,64,704]{2,1,0:T(8,128)(2,1)S(1)}, u32[]{:S(2)}, u32[]{:S(2)}) collective-permute-start(bf16[8,64,704]{2,1,0:T(8,128)(2,1)S(1)} %bitcast_dynamic-update-slice_fusion.16), channel_id=1, source_target_pairs={{0,8},{8,16},{16,24},{24,0},{1,9},{9,17},{17,25},{25,1},{2,10},{10... | collective-permute-start | bytes 2162696 | tf_op jit(solution)/shard_map/ppermute | solution.py:41
  113.7 1.2 bitcast_dynamic-update-slice_fusion.9
  115.0 2.7 %collective-permute-start.28 = (bf16[256,1408]{1,0:T(8,128)(2,1)S(1)}, bf16[256,1408]{1,0:T(8,128)(2,1)S(1)}, u32[]{:S(2)}, u32[]{:S(2)}) collective-permute-start(bf16[256,1408]{1,0:T(8,128)(2,1)S(1)} %broadcast_select_fusion.1), channel_id=1, source_target_pairs={{0,32},{1,225},{2,34},{3,227},{4,36},{5,229},{6,38},{7,231},{8,40}... | collective-permute-start | bytes 2162696 | tf_op jit(solution)/shard_map/ppermute | solution.py:33
  117.8 2.6 %normalise.1.left_ref = bf16[768,2048]{1,0:T(8,128)(2,1)S(1)} custom-call(s32[16]{0:T(128)S(1)} %stack.76.at_ref, bf16[768,256]{1,0:T(8,128)(2,1)S(1)} %add_convert_fusion.2.p0, bf16[768,256]{1,0:T(8,128)(2,1)S(1)} %collective-permute-done.6.p1, bf16[768,256]{1,0:T(8,128)(2,1)S(1)} %collective-permute-done.7.p2, ...), custom_call_target="tpu_custom_call" | custom-call | flops 2000000000 | bytes 6291456 | tf_op jit(solution)/shard_map/normalise/pallas_call | solution.py:214
  120.4 6.5 %collective-permute-done.24 = bf16[8,64,704]{2,1,0:T(8,128)(2,1)S(1)} collective-permute-done((bf16[8,64,704]{2,1,0:T(8,128)(2,1)S(1)}, bf16[8,64,704]{2,1,0:T(8,128)(2,1)S(1)}, u32[]{:S(2)}, u32[]{:S(2)}) %collective-permute-start.24) | collective-permute-done | bytes 720928 | tf_op jit(solution)/shard_map/ppermute | solution.py:41
  126.9 7.5 %collective-permute-done.25 = bf16[8,64,704]{2,1,0:T(8,128)(2,1)S(1)} collective-permute-done((bf16[8,64,704]{2,1,0:T(8,128)(2,1)S(1)}, bf16[8,64,704]{2,1,0:T(8,128)(2,1)S(1)}, u32[]{:S(2)}, u32[]{:S(2)}) %collective-permute-start.25) | collective-permute-done | bytes 720928 | tf_op jit(solution)/shard_map/ppermute | solution.py:41
  134.5 2.0 %collective-permute-start.31 = (bf16[8,64,704]{2,1,0:T(8,128)(2,1)S(1)}, bf16[8,64,704]{2,1,0:T(8,128)(2,1)S(1)}, u32[]{:S(2)}, u32[]{:S(2)}) collective-permute-start(bf16[8,64,704]{2,1,0:T(8,128)(2,1)S(1)} %broadcast_select_fusion), channel_id=1, source_target_pairs={{0,8},{1,25},{2,10},{3,27},{4,12},{5,29},{6,14},{7,31},{8,16},{9,1... | collective-permute-start | bytes 2162696 | tf_op jit(solution)/shard_map/ppermute | solution.py:33
  137.1 1.2 bitcast_dynamic-update-slice_fusion.7
  138.7 3.0 %shard_map.118.value_ref = bf16[768,768]{1,0:T(8,128)(2,1)S(1)} custom-call(bf16[768,2048]{1,0:T(8,128)(2,1)S(1)} %normalise.1.left_ref, bf16[2048,1408]{1,0:T(8,128)(2,1)S(1)} %bitcast.80), custom_call_target="tpu_custom_call" | custom-call | flops 3000000000 | bytes 8388608 | tf_op jit(solution)/shard_map/pallas_call | solution.py:239
  141.8 2.1 %collective-permute-start.29 = (bf16[1,704]{1,0:T(2,128)(2,1)S(1)}, bf16[1,704]{1,0:T(2,128)(2,1)S(1)}, u32[]{:S(2)}, u32[]{:S(2)}) collective-permute-start(bf16[1,704]{1,0:T(2,128)(2,1)S(1)} %get-tuple-element.65), channel_id=1, source_target_pairs={{0,8},{8,16},{16,24},{24,32},{32,40},{40,48},{48,56},{56,64},{64,7... | collective-permute-start | bytes 4232 | tf_op jit(solution)/shard_map/ppermute | solution.py:429
  143.9 3.7 %collective-permute-start.30 = (bf16[1,704]{1,0:T(2,128)(2,1)S(1)}, bf16[1,704]{1,0:T(2,128)(2,1)S(1)}, u32[]{:S(2)}, u32[]{:S(2)}) collective-permute-start(bf16[1,704]{1,0:T(2,128)(2,1)S(1)} %get-tuple-element.64), channel_id=1, source_target_pairs={{8,0},{16,8},{24,16},{32,24},{40,32},{48,40},{56,48},{64,56},{72,6... | collective-permute-start | bytes 4232 | tf_op jit(solution)/shard_map/ppermute | solution.py:430
  147.6 3.0 %shard_map.119.gate_ref = bf16[768,640]{1,0:T(8,128)(2,1)S(1)} custom-call(bf16[768,2048]{1,0:T(8,128)(2,1)S(1)} %normalise.1.left_ref, bf16[2048,1408]{1,0:T(8,128)(2,1)S(1)} %bitcast.81), custom_call_target="tpu_custom_call" | custom-call | flops 3000000000 | bytes 8388608 | tf_op jit(solution)/shard_map/pallas_call | solution.py:239
  150.7 2.9 %hidden_units.1 = bf16[768,704]{1,0:T(8,128)(2,1)S(1)} custom-call(bf16[768,768]{1,0:T(8,128)(2,1)S(1)} %shard_map.118.value_ref, bf16[768,640]{1,0:T(8,128)(2,1)S(1)} %shard_map.119.gate_ref, f32[768,128]{1,0:T(8,128)S(1)} %get-tuple-element.52.same_ref, bf16[1,704]{1,0:T(2,128)(2,1)S(1)} %collective-permute-done.29.before_ref, ...), custom_call_target="tpu_custom_call" | custom-call | flops 2000000000 | bytes 4194304 | tf_op jit(solution)/shard_map/hidden_units/pallas_call | solution.py:298
  153.9 1.4 convolution_convert_fusion
  155.4 3.4 %collective-permute-done.32 = bf16[768,1024]{1,0:T(8,128)(2,1)S(1)} collective-permute-done((bf16[768,1024]{1,0:T(8,128)(2,1)S(1)}, bf16[768,1024]{1,0:T(8,128)(2,1)S(1)}, u32[]{:S(2)}, u32[]{:S(2)}) %collective-permute-start.32) | collective-permute-done | bytes 1572896 | tf_op jit(solution)/shard_map/ppermute | solution.py:45
  158.8 1.4 add_convert_fusion
  160.4 1.2 collective-permute-start.34
  161.7 2.0 %collective-permute-start.35 = (bf16[768,256]{1,0:T(8,128)(2,1)S(1)}, bf16[768,256]{1,0:T(8,128)(2,1)S(1)}, u32[]{:S(2)}, u32[]{:S(2)}) collective-permute-start(bf16[768,256]{1,0:T(8,128)(2,1)S(1)} %get-tuple-element.62), channel_id=1, source_target_pairs={{0,6},{2,0},{4,2},{6,4},{1,7},{3,1},{5,3},{7,5},{8,14},{10,8},{12,... | collective-permute-start | bytes 1179656 | tf_op jit(solution)/shard_map/ppermute | solution.py:312
  163.7 17.6 %collective-permute-done.33 = bf16[768,256]{1,0:T(8,128)(2,1)S(1)} collective-permute-done((bf16[768,256]{1,0:T(8,128)(2,1)S(1)}, bf16[768,256]{1,0:T(8,128)(2,1)S(1)}, u32[]{:S(2)}, u32[]{:S(2)}) %collective-permute-start.33) | collective-permute-done | bytes 393248 | tf_op jit(solution)/shard_map/ppermute | solution.py:312
  181.8 1.0 add_convert_fusion.1
  (89 shorter events, 12.5 us)
Async XLA Ops:
  4.3 24.3 %collective-permute-start.10 = (bf16[64,1408]{1,0:T(8,128)(2,1)S(1)}, bf16[64,1408]{1,0:T(8,128)(2,1)S(1)}, u32[]{:S(2)}, u32[]{:S(2)}) collective-permute-start(bf16[64,1408]{1,0:T(8,128)(2,1)S(1)} %concatenate.13), channel_id=1, source_target_pairs={{0,16},{8,24},{16,0},{24,8},{1,17},{9,25},{17,1},{25,9},{2,18},{10... | collective-permute-start | bytes 540680 | tf_op jit(solution)/shard_map/ppermute | solution.py:41
  6.5 22.1 %collective-permute-start.11 = (bf16[64,1408]{1,0:T(8,128)(2,1)S(1)}, bf16[64,1408]{1,0:T(8,128)(2,1)S(1)}, u32[]{:S(2)}, u32[]{:S(2)}) collective-permute-start(bf16[64,1408]{1,0:T(8,128)(2,1)S(1)} %concatenate.13), channel_id=1, source_target_pairs={{0,24},{8,0},{16,8},{24,16},{1,25},{9,1},{17,9},{25,17},{2,26},{10... | collective-permute-start | bytes 540680 | tf_op jit(solution)/shard_map/ppermute | solution.py:41
  7.9 20.7 %collective-permute-start.9 = (bf16[64,1408]{1,0:T(8,128)(2,1)S(1)}, bf16[64,1408]{1,0:T(8,128)(2,1)S(1)}, u32[]{:S(2)}, u32[]{:S(2)}) collective-permute-start(bf16[64,1408]{1,0:T(8,128)(2,1)S(1)} %concatenate.13), channel_id=1, source_target_pairs={{0,8},{8,16},{16,24},{24,0},{1,9},{9,17},{17,25},{25,1},{2,10},{10... | collective-permute-start | bytes 540680 | tf_op jit(solution)/shard_map/ppermute | solution.py:41
  8.5 8.3 %collective-permute-start = (bf16[129,128]{1,0:T(8,128)(2,1)S(1)}, bf16[129,128]{1,0:T(8,128)(2,1)S(1)}, u32[]{:S(2)}, u32[]{:S(2)}) collective-permute-start(bf16[129,128]{1,0:T(8,128)(2,1)S(1)} %get-tuple-element.67), channel_id=1, source_target_pairs={{0,8},{8,16},{16,24},{24,32},{32,40},{40,48},{48,56},{56,64},{64,7... | collective-permute-start | bytes 99080 | tf_op jit(solution)/shard_map/ppermute | solution.py:346
  12.0 5.8 %collective-permute-start.1 = (bf16[129,128]{1,0:T(8,128)(2,1)S(1)}, bf16[129,128]{1,0:T(8,128)(2,1)S(1)}, u32[]{:S(2)}, u32[]{:S(2)}) collective-permute-start(bf16[129,128]{1,0:T(8,128)(2,1)S(1)} %get-tuple-element.66), channel_id=1, source_target_pairs={{8,0},{16,8},{24,16},{32,24},{40,32},{48,40},{56,48},{64,56},{72,6... | collective-permute-start | bytes 99080 | tf_op jit(solution)/shard_map/ppermute | solution.py:347
  17.8 1.2 copy-start
  19.1 1.0 copy-start.1
  20.0 0.7 copy-start.4
  28.5 38.5 %copy-start.5 = (bf16[64,704]{1,0:T(8,128)(2,1)S(1)}, bf16[64,704]{1,0:T(8,128)(2,1)}, u32[]{:S(2)}) copy-start(bf16[64,704]{1,0:T(8,128)(2,1)} %param.23) | copy-start | bytes 270340
  28.5 25.9 %collective-permute-start.2 = (bf16[4,768,256]{2,1,0:T(8,128)(2,1)S(1)}, bf16[4,768,256]{2,1,0:T(8,128)(2,1)S(1)}, u32[]{:S(2)}, u32[]{:S(2)}) collective-permute-start(bf16[4,768,256]{2,1,0:T(8,128)(2,1)S(1)} %get-tuple-element.30), channel_id=1, source_target_pairs={{0,1},{1,0},{2,3},{3,2},{4,5},{5,4},{6,7},{7,6},{8,9},{9,8},{10,11... | collective-permute-start | bytes 4718600 | tf_op jit(solution)/shard_map/ppermute | solution.py:45
  28.7 22.4 %collective-permute-start.12 = (bf16[256,1408]{1,0:T(8,128)(2,1)S(1)}, bf16[256,1408]{1,0:T(8,128)(2,1)}, u32[]{:S(2)}, u32[]{:S(2)}) collective-permute-start(bf16[256,1408]{1,0:T(8,128)(2,1)S(1)} %bitcast.88), channel_id=1, source_target_pairs={{0,32},{32,64},{64,96},{96,128},{128,160},{160,192},{192,224},{224... | collective-permute-start | bytes 2162696 | tf_op jit(solution)/shard_map/ppermute | solution.py:37
  30.3 20.8 %collective-permute-start.14 = (bf16[256,1408]{1,0:T(8,128)(2,1)S(1)}, bf16[256,1408]{1,0:T(8,128)(2,1)}, u32[]{:S(2)}, u32[]{:S(2)}) collective-permute-start(bf16[256,1408]{1,0:T(8,128)(2,1)S(1)} %bitcast.89), channel_id=1, source_target_pairs={{0,224},{32,0},{64,32},{96,64},{128,96},{160,128},{192,160},{224,1... | collective-permute-start | bytes 2162696 | tf_op jit(solution)/shard_map/ppermute | solution.py:37
  51.1 28.4 %collective-permute-start.13 = (bf16[256,1408]{1,0:T(8,128)(2,1)}, bf16[256,1408]{1,0:T(8,128)(2,1)S(1)}, u32[]{:S(2)}, u32[]{:S(2)}) collective-permute-start(bf16[256,1408]{1,0:T(8,128)(2,1)} %collective-permute-done.12), channel_id=1, source_target_pairs={{0,32},{32,64},{64,96},{96,128},{128,160},{160,192},{192,224},{224... | collective-permute-start | bytes 2162696 | tf_op jit(solution)/shard_map/ppermute | solution.py:37
  51.1 30.7 %collective-permute-start.15 = (bf16[256,1408]{1,0:T(8,128)(2,1)}, bf16[256,1408]{1,0:T(8,128)(2,1)}, u32[]{:S(2)}, u32[]{:S(2)}) collective-permute-start(bf16[256,1408]{1,0:T(8,128)(2,1)} %collective-permute-done.14), channel_id=1, source_target_pairs={{0,224},{32,0},{64,32},{96,64},{128,96},{160,128},{192,160},{224,1... | collective-permute-start | bytes 2162696 | tf_op jit(solution)/shard_map/ppermute | solution.py:37
  54.7 12.3 %collective-permute-start.3 = (bf16[768,256]{1,0:T(8,128)(2,1)S(1)}, bf16[768,256]{1,0:T(8,128)(2,1)}, u32[]{:S(2)}, u32[]{:S(2)}) collective-permute-start(bf16[768,256]{1,0:T(8,128)(2,1)S(1)} %get-tuple-element.32), channel_id=1, source_target_pairs={{0,2},{2,4},{4,6},{6,0},{1,3},{3,5},{5,7},{7,1},{8,10},{10,12},{12... | collective-permute-start | bytes 1179656 | tf_op jit(solution)/shard_map/ppermute | solution.py:312
  56.4 19.8 %collective-permute-start.4 = (bf16[768,256]{1,0:T(8,128)(2,1)S(1)}, bf16[768,256]{1,0:T(8,128)(2,1)}, u32[]{:S(2)}, u32[]{:S(2)}) collective-permute-start(bf16[768,256]{1,0:T(8,128)(2,1)S(1)} %get-tuple-element.33), channel_id=1, source_target_pairs={{0,4},{2,6},{4,0},{6,2},{1,5},{3,7},{5,1},{7,3},{8,12},{10,14},{12... | collective-permute-start | bytes 1179656 | tf_op jit(solution)/shard_map/ppermute | solution.py:312
  59.3 17.6 %collective-permute-start.5 = (bf16[768,256]{1,0:T(8,128)(2,1)S(1)}, bf16[768,256]{1,0:T(8,128)(2,1)}, u32[]{:S(2)}, u32[]{:S(2)}) collective-permute-start(bf16[768,256]{1,0:T(8,128)(2,1)S(1)} %get-tuple-element.34), channel_id=1, source_target_pairs={{0,6},{2,0},{4,2},{6,4},{1,7},{3,1},{5,3},{7,5},{8,14},{10,8},{12,... | collective-permute-start | bytes 1179656 | tf_op jit(solution)/shard_map/ppermute | solution.py:312
  67.0 14.8 %collective-permute-start.19 = (bf16[64,704]{1,0:T(8,128)(2,1)S(1)}, bf16[64,704]{1,0:T(8,128)(2,1)S(1)}, u32[]{:S(2)}, u32[]{:S(2)}) collective-permute-start(bf16[64,704]{1,0:T(8,128)(2,1)S(1)} %copy-done.5), channel_id=1, source_target_pairs={{0,64},{32,96},{64,128},{96,160},{128,192},{160,224},{192,0},{224,... | collective-permute-start | bytes 270344 | tf_op jit(solution)/shard_map/ppermute | solution.py:37
  76.1 8.9 %collective-permute-start.20 = (bf16[64,704]{1,0:T(8,128)(2,1)S(1)}, bf16[64,704]{1,0:T(8,128)(2,1)S(1)}, u32[]{:S(2)}, u32[]{:S(2)}) collective-permute-start(bf16[64,704]{1,0:T(8,128)(2,1)S(1)} %copy-done.5), channel_id=1, source_target_pairs={{0,192},{32,224},{64,0},{96,32},{128,64},{160,96},{192,128},{224,1... | collective-permute-start | bytes 270344 | tf_op jit(solution)/shard_map/ppermute | solution.py:37
  76.8 8.8 %collective-permute-start.17 = (bf16[64,704]{1,0:T(8,128)(2,1)S(1)}, bf16[64,704]{1,0:T(8,128)(2,1)S(1)}, u32[]{:S(2)}, u32[]{:S(2)}) collective-permute-start(bf16[64,704]{1,0:T(8,128)(2,1)S(1)} %copy-done.5), channel_id=1, source_target_pairs={{0,32},{32,64},{64,96},{96,128},{128,160},{160,192},{192,224},{224... | collective-permute-start | bytes 270344 | tf_op jit(solution)/shard_map/ppermute | solution.py:37
  79.5 9.9 %collective-permute-start.18 = (bf16[64,704]{1,0:T(8,128)(2,1)S(1)}, bf16[64,704]{1,0:T(8,128)(2,1)S(1)}, u32[]{:S(2)}, u32[]{:S(2)}) collective-permute-start(bf16[64,704]{1,0:T(8,128)(2,1)S(1)} %copy-done.5), channel_id=1, source_target_pairs={{0,224},{32,0},{64,32},{96,64},{128,96},{160,128},{192,160},{224,1... | collective-permute-start | bytes 270344 | tf_op jit(solution)/shard_map/ppermute | solution.py:37
  81.8 33.2 %collective-permute-start.26 = (bf16[256,1408]{1,0:T(8,128)(2,1)S(1)}, bf16[256,1408]{1,0:T(8,128)(2,1)S(1)}, u32[]{:S(2)}, u32[]{:S(2)}) collective-permute-start(bf16[256,1408]{1,0:T(8,128)(2,1)S(1)} %collective-permute-done.13), channel_id=1, source_target_pairs={{0,32},{32,64},{64,96},{96,128},{128,160},{160,192},{192,224},{224... | collective-permute-start | bytes 2162696 | tf_op jit(solution)/shard_map/ppermute | solution.py:37
  81.8 33.2 %collective-permute-start.27 = (bf16[256,1408]{1,0:T(8,128)(2,1)}, bf16[256,1408]{1,0:T(8,128)(2,1)S(1)}, u32[]{:S(2)}, u32[]{:S(2)}) collective-permute-start(bf16[256,1408]{1,0:T(8,128)(2,1)} %collective-permute-done.15), channel_id=1, source_target_pairs={{0,224},{32,0},{64,32},{96,64},{128,96},{160,128},{192,160},{224,1... | collective-permute-start | bytes 2162696 | tf_op jit(solution)/shard_map/ppermute | solution.py:37
  85.0 11.8 %collective-permute-start.6 = (bf16[768,256]{1,0:T(8,128)(2,1)S(1)}, bf16[768,256]{1,0:T(8,128)(2,1)S(1)}, u32[]{:S(2)}, u32[]{:S(2)}) collective-permute-start(bf16[768,256]{1,0:T(8,128)(2,1)S(1)} %add_convert_fusion.2.p0), channel_id=1, source_target_pairs={{0,2},{2,4},{4,6},{6,0},{1,3},{3,5},{5,7},{7,1},{8,10},{10,12},{12... | collective-permute-start | bytes 1179656 | tf_op jit(solution)/shard_map/ppermute | solution.py:312
  85.7 18.6 %collective-permute-start.7 = (bf16[768,256]{1,0:T(8,128)(2,1)S(1)}, bf16[768,256]{1,0:T(8,128)(2,1)S(1)}, u32[]{:S(2)}, u32[]{:S(2)}) collective-permute-start(bf16[768,256]{1,0:T(8,128)(2,1)S(1)} %add_convert_fusion.2.p0), channel_id=1, source_target_pairs={{0,4},{2,6},{4,0},{6,2},{1,5},{3,7},{5,1},{7,3},{8,12},{10,14},{12... | collective-permute-start | bytes 1179656 | tf_op jit(solution)/shard_map/ppermute | solution.py:312
  89.5 15.2 %collective-permute-start.8 = (bf16[768,256]{1,0:T(8,128)(2,1)S(1)}, bf16[768,256]{1,0:T(8,128)(2,1)S(1)}, u32[]{:S(2)}, u32[]{:S(2)}) collective-permute-start(bf16[768,256]{1,0:T(8,128)(2,1)S(1)} %add_convert_fusion.2.p0), channel_id=1, source_target_pairs={{0,6},{2,0},{4,2},{6,4},{1,7},{3,1},{5,3},{7,5},{8,14},{10,8},{12,... | collective-permute-start | bytes 1179656 | tf_op jit(solution)/shard_map/ppermute | solution.py:312
  96.8 8.3 %collective-permute-start.21 = (bf16[64,704]{1,0:T(8,128)(2,1)S(1)}, bf16[64,704]{1,0:T(8,128)(2,1)S(1)}, u32[]{:S(2)}, u32[]{:S(2)}) collective-permute-start(bf16[64,704]{1,0:T(8,128)(2,1)S(1)} %collective-permute-done.19), channel_id=1, source_target_pairs={{0,32},{32,64},{64,96},{96,128},{128,160},{160,192},{192,224},{224... | collective-permute-start | bytes 270344 | tf_op jit(solution)/shard_map/ppermute | solution.py:37
  104.3 4.6 %collective-permute-start.22 = (bf16[64,704]{1,0:T(8,128)(2,1)S(1)}, bf16[64,704]{1,0:T(8,128)(2,1)S(1)}, u32[]{:S(2)}, u32[]{:S(2)}) collective-permute-start(bf16[64,704]{1,0:T(8,128)(2,1)S(1)} %collective-permute-done.20), channel_id=1, source_target_pairs={{0,224},{32,0},{64,32},{96,64},{128,96},{160,128},{192,160},{224,1... | collective-permute-start | bytes 270344 | tf_op jit(solution)/shard_map/ppermute | solution.py:37
  104.6 7.0 %collective-permute-start.23 = (bf16[64,704]{1,0:T(8,128)(2,1)S(1)}, bf16[64,704]{1,0:T(8,128)(2,1)S(1)}, u32[]{:S(2)}, u32[]{:S(2)}) collective-permute-start(bf16[64,704]{1,0:T(8,128)(2,1)S(1)} %broadcast_select_fusion.2), channel_id=1, source_target_pairs={{0,64},{1,193},{2,66},{3,195},{4,68},{5,197},{6,70},{7,199},{8,72}... | collective-permute-start | bytes 270344 | tf_op jit(solution)/shard_map/ppermute | solution.py:33
  104.9 12.9 %copy-start.2 = (f32[2048]{0:T(1024)S(1)}, f32[2048]{0:T(1024)}, u32[]{:S(2)}) copy-start(f32[2048]{0:T(1024)} %param.19) | copy-start | bytes 24580
  105.1 12.7 %collective-permute-start.16 = (bf16[4,768,256]{2,1,0:T(8,128)(2,1)S(1)}, bf16[4,768,256]{2,1,0:T(8,128)(2,1)S(1)}, u32[]{:S(2)}, u32[]{:S(2)}) collective-permute-start(bf16[4,768,256]{2,1,0:T(8,128)(2,1)S(1)} %pad_maximum_fusion), channel_id=1, source_target_pairs={{0,1},{1,0},{2,3},{3,2},{4,5},{5,4},{6,7},{7,6},{8,9},{9,8},{10,11... | collective-permute-start | bytes 4718600 | tf_op jit(solution)/shard_map/ppermute | solution.py:45
  111.6 15.3 %collective-permute-start.24 = (bf16[8,64,704]{2,1,0:T(8,128)(2,1)S(1)}, bf16[8,64,704]{2,1,0:T(8,128)(2,1)S(1)}, u32[]{:S(2)}, u32[]{:S(2)}) collective-permute-start(bf16[8,64,704]{2,1,0:T(8,128)(2,1)S(1)} %bitcast_dynamic-update-slice_fusion.16), channel_id=1, source_target_pairs={{0,8},{8,16},{16,24},{24,0},{1,9},{9,17},{17,25},{25,1},{2,10},{10... | collective-permute-start | bytes 2162696 | tf_op jit(solution)/shard_map/ppermute | solution.py:41
  113.7 20.7 %collective-permute-start.25 = (bf16[8,64,704]{2,1,0:T(8,128)(2,1)S(1)}, bf16[8,64,704]{2,1,0:T(8,128)(2,1)S(1)}, u32[]{:S(2)}, u32[]{:S(2)}) collective-permute-start(bf16[8,64,704]{2,1,0:T(8,128)(2,1)S(1)} %bitcast_dynamic-update-slice_fusion.16), channel_id=1, source_target_pairs={{0,24},{8,0},{16,8},{24,16},{1,25},{9,1},{17,9},{25,17},{2,26},{10... | collective-permute-start | bytes 2162696 | tf_op jit(solution)/shard_map/ppermute | solution.py:41
  115.0 23.6 %collective-permute-start.28 = (bf16[256,1408]{1,0:T(8,128)(2,1)S(1)}, bf16[256,1408]{1,0:T(8,128)(2,1)S(1)}, u32[]{:S(2)}, u32[]{:S(2)}) collective-permute-start(bf16[256,1408]{1,0:T(8,128)(2,1)S(1)} %broadcast_select_fusion.1), channel_id=1, source_target_pairs={{0,32},{1,225},{2,34},{3,227},{4,36},{5,229},{6,38},{7,231},{8,40}... | collective-permute-start | bytes 2162696 | tf_op jit(solution)/shard_map/ppermute | solution.py:33
  134.5 19.0 %collective-permute-start.31 = (bf16[8,64,704]{2,1,0:T(8,128)(2,1)S(1)}, bf16[8,64,704]{2,1,0:T(8,128)(2,1)S(1)}, u32[]{:S(2)}, u32[]{:S(2)}) collective-permute-start(bf16[8,64,704]{2,1,0:T(8,128)(2,1)S(1)} %broadcast_select_fusion), channel_id=1, source_target_pairs={{0,8},{1,25},{2,10},{3,27},{4,12},{5,29},{6,14},{7,31},{8,16},{9,1... | collective-permute-start | bytes 2162696 | tf_op jit(solution)/shard_map/ppermute | solution.py:33
  141.8 8.9 %collective-permute-start.29 = (bf16[1,704]{1,0:T(2,128)(2,1)S(1)}, bf16[1,704]{1,0:T(2,128)(2,1)S(1)}, u32[]{:S(2)}, u32[]{:S(2)}) collective-permute-start(bf16[1,704]{1,0:T(2,128)(2,1)S(1)} %get-tuple-element.65), channel_id=1, source_target_pairs={{0,8},{8,16},{16,24},{24,32},{32,40},{40,48},{48,56},{56,64},{64,7... | collective-permute-start | bytes 4232 | tf_op jit(solution)/shard_map/ppermute | solution.py:429
  143.9 6.8 %copy-start.3 = (bf16[3,704]{1,0:T(4,128)(2,1)S(1)}, bf16[3,704]{1,0:T(4,128)(2,1)}, u32[]{:S(2)}) copy-start(bf16[3,704]{1,0:T(4,128)(2,1)} %taps_ref.1) | copy-start | bytes 12676
  143.9 6.8 %collective-permute-start.30 = (bf16[1,704]{1,0:T(2,128)(2,1)S(1)}, bf16[1,704]{1,0:T(2,128)(2,1)S(1)}, u32[]{:S(2)}, u32[]{:S(2)}) collective-permute-start(bf16[1,704]{1,0:T(2,128)(2,1)S(1)} %get-tuple-element.64), channel_id=1, source_target_pairs={{8,0},{16,8},{24,16},{32,24},{40,32},{48,40},{56,48},{64,56},{72,6... | collective-permute-start | bytes 4232 | tf_op jit(solution)/shard_map/ppermute | solution.py:430
  155.3 3.5 %collective-permute-start.32 = (bf16[768,1024]{1,0:T(8,128)(2,1)S(1)}, bf16[768,1024]{1,0:T(8,128)(2,1)S(1)}, u32[]{:S(2)}, u32[]{:S(2)}) collective-permute-start(bf16[768,1024]{1,0:T(8,128)(2,1)S(1)} %convolution_convert_fusion), channel_id=1, source_target_pairs={{0,1},{1,0},{2,3},{3,2},{4,5},{5,4},{6,7},{7,6},{8,9},{9,8},{10,11... | collective-permute-start | bytes 4718600 | tf_op jit(solution)/shard_map/ppermute | solution.py:45
  160.4 20.9 %collective-permute-start.33 = (bf16[768,256]{1,0:T(8,128)(2,1)S(1)}, bf16[768,256]{1,0:T(8,128)(2,1)S(1)}, u32[]{:S(2)}, u32[]{:S(2)}) collective-permute-start(bf16[768,256]{1,0:T(8,128)(2,1)S(1)} %get-tuple-element.61), channel_id=1, source_target_pairs={{0,2},{2,4},{4,6},{6,0},{1,3},{3,5},{5,7},{7,1},{8,10},{10,12},{12... | collective-permute-start | bytes 1179656 | tf_op jit(solution)/shard_map/ppermute | solution.py:312
  160.4 20.8 %collective-permute-start.34 = (bf16[768,256]{1,0:T(8,128)(2,1)S(1)}, bf16[768,256]{1,0:T(8,128)(2,1)S(1)}, u32[]{:S(2)}, u32[]{:S(2)}) collective-permute-start(bf16[768,256]{1,0:T(8,128)(2,1)S(1)} %get-tuple-element.63), channel_id=1, source_target_pairs={{0,4},{2,6},{4,0},{6,2},{1,5},{3,7},{5,1},{7,3},{8,12},{10,14},{12... | collective-permute-start | bytes 1179656 | tf_op jit(solution)/shard_map/ppermute | solution.py:312
  161.7 20.2 %collective-permute-start.35 = (bf16[768,256]{1,0:T(8,128)(2,1)S(1)}, bf16[768,256]{1,0:T(8,128)(2,1)S(1)}, u32[]{:S(2)}, u32[]{:S(2)}) collective-permute-start(bf16[768,256]{1,0:T(8,128)(2,1)S(1)} %get-tuple-element.62), channel_id=1, source_target_pairs={{0,6},{2,0},{4,2},{6,4},{1,7},{3,1},{5,3},{7,5},{8,14},{10,8},{12,... | collective-permute-start | bytes 1179656 | tf_op jit(solution)/shard_map/ppermute | solution.py:312

commit v5 on v4

--- a/solution.py
+++ b/solution.py
@@ -414,12 +414,14 @@
     normed = normalised(order, parts, rest, norm_gain[None])
     full = keep(after(full, normed), plus2, minus2, 2)
     full = keep(full, plus3, minus3, 3)
-    full = put(full, last, (z + NZ // 2) % NZ).reshape(model_width, width)
-
-    whole_plus, whole_minus = lax.optimization_barrier((whole_plus, whole_minus, normed))[:2]
-    whole_far = send_apart(jnp.where(core == 0, whole_plus, whole_minus), 0, 1)
+
     full_down = jnp.zeros((NZ, NX, rows_w, ff), w_down_t.dtype)
     full_down = put(full_down, after(whole, normed)[:, None], 0, x)
+    full, full_down, whole_plus, whole_minus = lax.optimization_barrier(
+        (full, full_down, whole_plus, whole_minus)
+    )
+    full = put(full, last, (z + NZ // 2) % NZ).reshape(model_width, width)
+    whole_far = send_apart(jnp.where(core == 0, whole_plus, whole_minus), 0, 1)
     full_down = put(full_down, whole_plus[:, None], 0, (x - 1) % NX)
     full_down = put(full_down, whole_minus[:, None], 0, (x + 1) % NX)
     normed = after(normed, full_down)
@@ -445,8 +447,10 @@
             hidden, weights, (((1,), (1,)), ((), ())), preferred_element_type=jnp.float32
         )
 
-    got = swap(down(1 - core).astype(jnp.bfloat16))
-    pair = (down(core) + got.astype(jnp.float32)).astype(jnp.bfloat16)
+    theirs = down(1 - core).astype(jnp.bfloat16)
+    got = swap(theirs)
+    mine = after(down(core).astype(jnp.bfloat16), theirs)
+    pair = (mine.astype(jnp.float32) + got.astype(jnp.float32)).astype(jnp.bfloat16)
     pairs = [pair[:, k * span : (k + 1) * span] for k in range(NY)]
     ffn_cols = pairs[0].astype(jnp.float32)
     for block in to_owners(pairs):

time: 184 us -> 188 us (1.022)
  waiting for transfers between devices: 87.8 us -> 90.1 us
    ppermute x9, starting transfers between devices: 16.2 us -> 12.2 us  [to_owners(): lax.ppermute(pairs[k], 'y', [(y, (y + k) % NY) for y in range(NY)])]
    ppermute x3, waiting for transfers between devices: 2.72 us -> 6.14 us  [send_apart(): return lax.ppermute(block, AXES, pairs)]
    ppermute x12, starting transfers between devices: 16.5 us -> 19.2 us  [send_z(): return lax.ppermute(block, 'z', [(z, (z + k) % NZ) for z in range(NZ)])]
    ppermute x5, starting transfers between devices: 6.34 us -> 9.02 us  [send_x(): return lax.ppermute(block, 'x', [(x, (x + k) % NX) for x in range(NX)])]
    ppermute x9, waiting for transfers between devices: 44 us -> 46.6 us  [to_owners(): lax.ppermute(pairs[k], 'y', [(y, (y + k) % NY) for y in range(NY)])]
    ppermute x3, starting transfers between devices: 4.94 us -> 2.83 us  [send_apart(): return lax.ppermute(block, AXES, pairs)]
    ppermute x1, waiting for transfers between devices: 2.11 us -> 0.01 us  [per_device(): low = lax.ppermute(packed[:, -WINDOW:], ('z', 'x'), forward)]
    ppermute x1, waiting for transfers between devices: 1 us -> 3.1 us  [per_device(): high = lax.ppermute(packed[:, :WINDOW], ('z', 'x'), backward)]
  transfers between devices with their start and end apart: 36 -> 36, of which waited for: 14 -> 13; matrix products, arithmetic and copies ran while one was open for 4% -> 5% of each run, Pallas kernels for 11% -> 11%
where the time goes in v5:
time: 188 us; the launch traced here: 185 us
  waiting for transfers between devices  90.1 us (48%)
  starting transfers between devices  55.2 us (29%)
  Pallas kernels  19.6 us (10%)
  local copies, waits for them, and re-layouts  11.3 us (6%)
  other arithmetic  5.38 us (3%)
  matrix products  2.85 us (2%)
    ppermute x9, waiting for transfers between devices, to_owners(): lax.ppermute(pairs[k], 'y', [(y, (y + k) % NY) for y in range(NY)])  46.6 us
    ppermute x12, starting transfers between devices, send_z(): return lax.ppermute(block, 'z', [(z, (z + k) % NZ) for z in range(NZ)])  19.2 us
    ppermute x12, waiting for transfers between devices, send_z(): return lax.ppermute(block, 'z', [(z, (z + k) % NZ) for z in range(NZ)])  19.1 us
    ppermute x5, waiting for transfers between devices, send_x(): return lax.ppermute(block, 'x', [(x, (x + k) % NX) for x in range(NX)])  13.2 us
    ppermute x9, starting transfers between devices, to_owners(): lax.ppermute(pairs[k], 'y', [(y, (y + k) % NY) for y in range(NY)])  12.2 us
    ppermute x5, starting transfers between devices, send_x(): return lax.ppermute(block, 'x', [(x, (x + k) % NX) for x in range(NX)])  9.02 us
    pallas_call x1, Pallas kernels, attention(): pl.pallas_call(attention_kernel, out_shape=[jax.ShapeDtypeStruct((NY, row...  7.75 us
    ppermute x3, waiting for transfers between devices, send_apart(): return lax.ppermute(block, AXES, pairs)  6.14 us
  transfers between devices with their start and end apart: 36, of which 13 were waited for; matrix products, arithmetic and copies ran while one was open for 5% of the time, Pallas kernels for 11%

profile of v5, /device:TPU:2, one launch (start us, length us, event | category | flops | bytes accessed | tf_op | source)
XLA Modules:
  0.0 185.2 jit_solution(14986289989125501133)
XLA Ops:
  2.3 1.0 pad_maximum_fusion.1.packed_ref
  3.3 1.0 concatenate.13
  4.3 1.6 collective-permute-start.9
  5.8 2.8 %collective-permute-start.10 = (bf16[64,1408]{1,0:T(8,128)(2,1)S(1)}, bf16[64,1408]{1,0:T(8,128)(2,1)S(1)}, u32[]{:S(2)}, u32[]{:S(2)}) collective-permute-start(bf16[64,1408]{1,0:T(8,128)(2,1)S(1)} %concatenate.13), channel_id=1, source_target_pairs={{0,16},{8,24},{16,0},{24,8},{1,17},{9,25},{17,1},{25,9},{2,18},{10... | collective-permute-start | bytes 540680 | tf_op jit(solution)/shard_map/ppermute | solution.py:41
  9.1 3.5 %collective-permute-start = (bf16[129,128]{1,0:T(8,128)(2,1)S(1)}, bf16[129,128]{1,0:T(8,128)(2,1)S(1)}, u32[]{:S(2)}, u32[]{:S(2)}) collective-permute-start(bf16[129,128]{1,0:T(8,128)(2,1)S(1)} %get-tuple-element.73), channel_id=1, source_target_pairs={{0,8},{8,16},{16,24},{24,32},{32,40},{40,48},{48,56},{56,64},{64,7... | collective-permute-start | bytes 99080 | tf_op jit(solution)/shard_map/ppermute | solution.py:346
  12.6 2.4 %collective-permute-start.1 = (bf16[129,128]{1,0:T(8,128)(2,1)S(1)}, bf16[129,128]{1,0:T(8,128)(2,1)S(1)}, u32[]{:S(2)}, u32[]{:S(2)}) collective-permute-start(bf16[129,128]{1,0:T(8,128)(2,1)S(1)} %get-tuple-element.72), channel_id=1, source_target_pairs={{8,0},{16,8},{24,16},{32,24},{40,32},{48,40},{56,48},{64,56},{72,6... | collective-permute-start | bytes 99080 | tf_op jit(solution)/shard_map/ppermute | solution.py:347
  15.3 3.1 %collective-permute-done.1.high_ref = bf16[129,128]{1,0:T(8,128)(2,1)S(1)} collective-permute-done((bf16[129,128]{1,0:T(8,128)(2,1)S(1)}, bf16[129,128]{1,0:T(8,128)(2,1)S(1)}, u32[]{:S(2)}, u32[]{:S(2)}) %collective-permute-start.1) | collective-permute-done | bytes 33056 | tf_op jit(solution)/shard_map/ppermute | solution.py:347
  18.4 1.2 copy-done
  19.6 1.0 copy-done.1
  21.3 7.8 %attention.1 = (bf16[4,768,256]{2,1,0:T(8,128)(2,1)S(1)}, bf16[4,768,256]{2,1,0:T(8,128)(2,1)S(1)}, f32[768,128]{1,0:T(8,128)S(1)}) custom-call(s32[16]{0:T(128)S(1)} %stack.76.at_ref, f32[4]{0:T(128)S(1)} %copy-done.4, bf16[768,256]{1,0:T(8,128)(2,1)S(1)} %copy-done.1, bf16[256,2048]{1,0:T(8,128)(2,1)S(1)} %copy-done, ...), custom_call_target="tpu_custom_call" | custom-call | flops 4000000000 | bytes 4194304 | tf_op jit(solution)/shard_map/attention/pallas_call | solution.py:152
  30.2 4.0 %collective-permute-start.14 = (bf16[256,1408]{1,0:T(8,128)(2,1)S(1)}, bf16[256,1408]{1,0:T(8,128)(2,1)}, u32[]{:S(2)}, u32[]{:S(2)}) collective-permute-start(bf16[256,1408]{1,0:T(8,128)(2,1)S(1)} %bitcast.89), channel_id=1, source_target_pairs={{0,224},{32,0},{64,32},{96,64},{128,96},{160,128},{192,160},{224,1... | collective-permute-start | bytes 2162696 | tf_op jit(solution)/shard_map/ppermute | solution.py:37
  34.2 16.8 %collective-permute-done.12 = bf16[256,1408]{1,0:T(8,128)(2,1)} collective-permute-done((bf16[256,1408]{1,0:T(8,128)(2,1)S(1)}, bf16[256,1408]{1,0:T(8,128)(2,1)}, u32[]{:S(2)}, u32[]{:S(2)}) %collective-permute-start.12) | collective-permute-done | bytes 720928 | tf_op jit(solution)/shard_map/ppermute | solution.py:37
  51.0 3.2 %collective-permute-start.15 = (bf16[256,1408]{1,0:T(8,128)(2,1)}, bf16[256,1408]{1,0:T(8,128)(2,1)}, u32[]{:S(2)}, u32[]{:S(2)}) collective-permute-start(bf16[256,1408]{1,0:T(8,128)(2,1)} %collective-permute-done.14), channel_id=1, source_target_pairs={{0,224},{32,0},{64,32},{96,64},{128,96},{160,128},{192,160},{224,1... | collective-permute-start | bytes 2162696 | tf_op jit(solution)/shard_map/ppermute | solution.py:37
  54.6 3.1 %collective-permute-start.5 = (bf16[768,256]{1,0:T(8,128)(2,1)S(1)}, bf16[768,256]{1,0:T(8,128)(2,1)}, u32[]{:S(2)}, u32[]{:S(2)}) collective-permute-start(bf16[768,256]{1,0:T(8,128)(2,1)S(1)} %get-tuple-element.37), channel_id=1, source_target_pairs={{0,6},{2,0},{4,2},{6,4},{1,7},{3,1},{5,3},{7,5},{8,14},{10,8},{12,... | collective-permute-start | bytes 1179656 | tf_op jit(solution)/shard_map/ppermute | solution.py:312
  58.3 1.0 collective-permute-start.3
  59.3 14.7 %collective-permute-done.5 = bf16[768,256]{1,0:T(8,128)(2,1)} collective-permute-done((bf16[768,256]{1,0:T(8,128)(2,1)S(1)}, bf16[768,256]{1,0:T(8,128)(2,1)}, u32[]{:S(2)}, u32[]{:S(2)}) %collective-permute-start.5) | collective-permute-done | bytes 393248 | tf_op jit(solution)/shard_map/ppermute | solution.py:312
  74.0 2.2 %collective-permute-start.21 = (bf16[64,704]{1,0:T(8,128)(2,1)S(1)}, bf16[64,704]{1,0:T(8,128)(2,1)S(1)}, u32[]{:S(2)}, u32[]{:S(2)}) collective-permute-start(bf16[64,704]{1,0:T(8,128)(2,1)S(1)} %copy-done.5), channel_id=1, source_target_pairs={{0,64},{32,96},{64,128},{96,160},{128,192},{160,224},{192,0},{224,... | collective-permute-start | bytes 270344 | tf_op jit(solution)/shard_map/ppermute | solution.py:37
  76.2 1.6 collective-permute-done.3
  78.5 1.6 add_convert_fusion.2.p0
  80.1 1.7 collective-permute-start.20
  82.2 2.9 %collective-permute-start.18 = (bf16[256,1408]{1,0:T(8,128)(2,1)}, bf16[256,1408]{1,0:T(8,128)(2,1)S(1)}, u32[]{:S(2)}, u32[]{:S(2)}) collective-permute-start(bf16[256,1408]{1,0:T(8,128)(2,1)} %collective-permute-done.15), channel_id=1, source_target_pairs={{0,224},{32,0},{64,32},{96,64},{128,96},{160,128},{192,160},{224,1... | collective-permute-start | bytes 2162696 | tf_op jit(solution)/shard_map/ppermute | solution.py:37
  85.9 1.2 bitcast_dynamic-update-slice_fusion.10
  87.2 5.1 %collective-permute-start.7 = (bf16[768,256]{1,0:T(8,128)(2,1)S(1)}, bf16[768,256]{1,0:T(8,128)(2,1)S(1)}, u32[]{:S(2)}, u32[]{:S(2)}) collective-permute-start(bf16[768,256]{1,0:T(8,128)(2,1)S(1)} %add_convert_fusion.2.p0), channel_id=1, source_target_pairs={{0,4},{2,6},{4,0},{6,2},{1,5},{3,7},{5,1},{7,3},{8,12},{10,14},{12... | collective-permute-start | bytes 1179656 | tf_op jit(solution)/shard_map/ppermute | solution.py:312
  92.4 1.2 bitcast_dynamic-update-slice_fusion.9
  93.6 10.9 %collective-permute-done.6.p1 = bf16[768,256]{1,0:T(8,128)(2,1)S(1)} collective-permute-done((bf16[768,256]{1,0:T(8,128)(2,1)S(1)}, bf16[768,256]{1,0:T(8,128)(2,1)S(1)}, u32[]{:S(2)}, u32[]{:S(2)}) %collective-permute-start.6) | collective-permute-done | bytes 393248 | tf_op jit(solution)/shard_map/ppermute | solution.py:312
  104.6 3.2 %collective-permute-start.24 = (bf16[64,704]{1,0:T(8,128)(2,1)S(1)}, bf16[64,704]{1,0:T(8,128)(2,1)S(1)}, u32[]{:S(2)}, u32[]{:S(2)}) collective-permute-start(bf16[64,704]{1,0:T(8,128)(2,1)S(1)} %collective-permute-done.22), channel_id=1, source_target_pairs={{0,224},{32,0},{64,32},{96,64},{128,96},{160,128},{192,160},{224,1... | collective-permute-start | bytes 270344 | tf_op jit(solution)/shard_map/ppermute | solution.py:37
  108.2 2.2 %collective-permute-done.23 = bf16[64,704]{1,0:T(8,128)(2,1)S(1)} collective-permute-done((bf16[64,704]{1,0:T(8,128)(2,1)S(1)}, bf16[64,704]{1,0:T(8,128)(2,1)S(1)}, u32[]{:S(2)}, u32[]{:S(2)}) %collective-permute-start.23) | collective-permute-done | bytes 90144 | tf_op jit(solution)/shard_map/ppermute | solution.py:37
  111.0 6.1 %collective-permute-done.25 = bf16[64,704]{1,0:T(8,128)(2,1)S(1)} collective-permute-done((bf16[64,704]{1,0:T(8,128)(2,1)S(1)}, bf16[64,704]{1,0:T(8,128)(2,1)S(1)}, u32[]{:S(2)}, u32[]{:S(2)}) %collective-permute-start.25) | collective-permute-done | bytes 90144 | tf_op jit(solution)/shard_map/ppermute | solution.py:33
  117.1 2.1 %collective-permute-start.26 = (bf16[8,64,704]{2,1,0:T(8,128)(2,1)S(1)}, bf16[8,64,704]{2,1,0:T(8,128)(2,1)S(1)}, u32[]{:S(2)}, u32[]{:S(2)}) collective-permute-start(bf16[8,64,704]{2,1,0:T(8,128)(2,1)S(1)} %bitcast_dynamic-update-slice_fusion.16), channel_id=1, source_target_pairs={{0,8},{8,16},{16,24},{24,0},{1,9},{9,17},{17,25},{25,1},{2,10},{10... | collective-permute-start | bytes 2162696 | tf_op jit(solution)/shard_map/ppermute | solution.py:41
  119.3 2.1 %collective-permute-start.27 = (bf16[8,64,704]{2,1,0:T(8,128)(2,1)S(1)}, bf16[8,64,704]{2,1,0:T(8,128)(2,1)S(1)}, u32[]{:S(2)}, u32[]{:S(2)}) collective-permute-start(bf16[8,64,704]{2,1,0:T(8,128)(2,1)S(1)} %bitcast_dynamic-update-slice_fusion.16), channel_id=1, source_target_pairs={{0,24},{8,0},{16,8},{24,16},{1,25},{9,1},{17,9},{25,17},{2,26},{10... | collective-permute-start | bytes 2162696 | tf_op jit(solution)/shard_map/ppermute | solution.py:41
  121.7 2.6 %normalise.1.left_ref = bf16[768,2048]{1,0:T(8,128)(2,1)S(1)} custom-call(s32[16]{0:T(128)S(1)} %stack.76.at_ref, bf16[768,256]{1,0:T(8,128)(2,1)S(1)} %add_convert_fusion.2.p0, bf16[768,256]{1,0:T(8,128)(2,1)S(1)} %collective-permute-done.6.p1, bf16[768,256]{1,0:T(8,128)(2,1)S(1)} %collective-permute-done.7.p2, ...), custom_call_target="tpu_custom_call" | custom-call | flops 2000000000 | bytes 6291456 | tf_op jit(solution)/shard_map/normalise/pallas_call | solution.py:214
  124.4 1.2 bitcast_dynamic-update-slice_fusion.7
  126.3 9.2 %collective-permute-done.26 = bf16[8,64,704]{2,1,0:T(8,128)(2,1)S(1)} collective-permute-done((bf16[8,64,704]{2,1,0:T(8,128)(2,1)S(1)}, bf16[8,64,704]{2,1,0:T(8,128)(2,1)S(1)}, u32[]{:S(2)}, u32[]{:S(2)}) %collective-permute-start.26) | collective-permute-done | bytes 720928 | tf_op jit(solution)/shard_map/ppermute | solution.py:41
  135.5 4.1 %collective-permute-done.27 = bf16[8,64,704]{2,1,0:T(8,128)(2,1)S(1)} collective-permute-done((bf16[8,64,704]{2,1,0:T(8,128)(2,1)S(1)}, bf16[8,64,704]{2,1,0:T(8,128)(2,1)S(1)}, u32[]{:S(2)}, u32[]{:S(2)}) %collective-permute-start.27) | collective-permute-done | bytes 720928 | tf_op jit(solution)/shard_map/ppermute | solution.py:41
  139.8 2.0 %collective-permute-start.31 = (bf16[8,64,704]{2,1,0:T(8,128)(2,1)S(1)}, bf16[8,64,704]{2,1,0:T(8,128)(2,1)S(1)}, u32[]{:S(2)}, u32[]{:S(2)}) collective-permute-start(bf16[8,64,704]{2,1,0:T(8,128)(2,1)S(1)} %broadcast_select_fusion), channel_id=1, source_target_pairs={{0,8},{1,25},{2,10},{3,27},{4,12},{5,29},{6,14},{7,31},{8,16},{9,1... | collective-permute-start | bytes 2162696 | tf_op jit(solution)/shard_map/ppermute | solution.py:33
  141.8 3.0 %shard_map.118.value_ref = bf16[768,768]{1,0:T(8,128)(2,1)S(1)} custom-call(bf16[768,2048]{1,0:T(8,128)(2,1)S(1)} %normalise.1.left_ref, bf16[2048,1408]{1,0:T(8,128)(2,1)S(1)} %bitcast.80), custom_call_target="tpu_custom_call" | custom-call | flops 3000000000 | bytes 8388608 | tf_op jit(solution)/shard_map/pallas_call | solution.py:239
  144.9 2.1 %collective-permute-start.29 = (bf16[1,704]{1,0:T(2,128)(2,1)S(1)}, bf16[1,704]{1,0:T(2,128)(2,1)S(1)}, u32[]{:S(2)}, u32[]{:S(2)}) collective-permute-start(bf16[1,704]{1,0:T(2,128)(2,1)S(1)} %get-tuple-element.71), channel_id=1, source_target_pairs={{0,8},{8,16},{16,24},{24,32},{32,40},{40,48},{48,56},{56,64},{64,7... | collective-permute-start | bytes 4232 | tf_op jit(solution)/shard_map/ppermute | solution.py:431
  147.0 3.7 %collective-permute-start.30 = (bf16[1,704]{1,0:T(2,128)(2,1)S(1)}, bf16[1,704]{1,0:T(2,128)(2,1)S(1)}, u32[]{:S(2)}, u32[]{:S(2)}) collective-permute-start(bf16[1,704]{1,0:T(2,128)(2,1)S(1)} %get-tuple-element.70), channel_id=1, source_target_pairs={{8,0},{16,8},{24,16},{32,24},{40,32},{48,40},{56,48},{64,56},{72,6... | collective-permute-start | bytes 4232 | tf_op jit(solution)/shard_map/ppermute | solution.py:432
  150.7 3.0 %shard_map.119.gate_ref = bf16[768,640]{1,0:T(8,128)(2,1)S(1)} custom-call(bf16[768,2048]{1,0:T(8,128)(2,1)S(1)} %normalise.1.left_ref, bf16[2048,1408]{1,0:T(8,128)(2,1)S(1)} %bitcast.81), custom_call_target="tpu_custom_call" | custom-call | flops 3000000000 | bytes 8388608 | tf_op jit(solution)/shard_map/pallas_call | solution.py:239
  153.8 2.9 %hidden_units.1 = bf16[768,704]{1,0:T(8,128)(2,1)S(1)} custom-call(bf16[768,768]{1,0:T(8,128)(2,1)S(1)} %shard_map.118.value_ref, bf16[768,640]{1,0:T(8,128)(2,1)S(1)} %shard_map.119.gate_ref, f32[768,128]{1,0:T(8,128)S(1)} %get-tuple-element.57.same_ref, bf16[1,704]{1,0:T(2,128)(2,1)S(1)} %collective-permute-done.29.before_ref, ...), custom_call_target="tpu_custom_call" | custom-call | flops 2000000000 | bytes 4194304 | tf_op jit(solution)/shard_map/hidden_units/pallas_call | solution.py:298
  157.0 1.4 convolution_convert_fusion
  158.5 1.4 convolution_convert_fusion.1
  159.9 2.0 %collective-permute-done.32 = bf16[768,1024]{1,0:T(8,128)(2,1)S(1)} collective-permute-done((bf16[768,1024]{1,0:T(8,128)(2,1)S(1)}, bf16[768,1024]{1,0:T(8,128)(2,1)S(1)}, u32[]{:S(2)}, u32[]{:S(2)}) %collective-permute-start.32) | collective-permute-done | bytes 1572896 | tf_op jit(solution)/shard_map/ppermute | solution.py:45
  163.3 1.5 collective-permute-start.33
  164.8 10.0 %collective-permute-done.35 = bf16[768,256]{1,0:T(8,128)(2,1)S(1)} collective-permute-done((bf16[768,256]{1,0:T(8,128)(2,1)S(1)}, bf16[768,256]{1,0:T(8,128)(2,1)S(1)}, u32[]{:S(2)}, u32[]{:S(2)}) %collective-permute-start.35) | collective-permute-done | bytes 393248 | tf_op jit(solution)/shard_map/ppermute | solution.py:312
  174.7 2.1 %collective-permute-done.34 = bf16[768,256]{1,0:T(8,128)(2,1)S(1)} collective-permute-done((bf16[768,256]{1,0:T(8,128)(2,1)S(1)}, bf16[768,256]{1,0:T(8,128)(2,1)S(1)}, u32[]{:S(2)}, u32[]{:S(2)}) %collective-permute-start.34) | collective-permute-done | bytes 393248 | tf_op jit(solution)/shard_map/ppermute | solution.py:312
  176.9 7.3 %collective-permute-done.33 = bf16[768,256]{1,0:T(8,128)(2,1)S(1)} collective-permute-done((bf16[768,256]{1,0:T(8,128)(2,1)S(1)}, bf16[768,256]{1,0:T(8,128)(2,1)S(1)}, u32[]{:S(2)}, u32[]{:S(2)}) %collective-permute-start.33) | collective-permute-done | bytes 393248 | tf_op jit(solution)/shard_map/ppermute | solution.py:312
  184.1 1.0 add_convert_fusion.1
  (90 shorter events, 11.8 us)
Async XLA Ops:
  4.3 24.9 %collective-permute-start.9 = (bf16[64,1408]{1,0:T(8,128)(2,1)S(1)}, bf16[64,1408]{1,0:T(8,128)(2,1)S(1)}, u32[]{:S(2)}, u32[]{:S(2)}) collective-permute-start(bf16[64,1408]{1,0:T(8,128)(2,1)S(1)} %concatenate.13), channel_id=1, source_target_pairs={{0,8},{8,16},{16,24},{24,0},{1,9},{9,17},{17,25},{25,1},{2,10},{10... | collective-permute-start | bytes 540680 | tf_op jit(solution)/shard_map/ppermute | solution.py:41
  5.8 23.3 %collective-permute-start.10 = (bf16[64,1408]{1,0:T(8,128)(2,1)S(1)}, bf16[64,1408]{1,0:T(8,128)(2,1)S(1)}, u32[]{:S(2)}, u32[]{:S(2)}) collective-permute-start(bf16[64,1408]{1,0:T(8,128)(2,1)S(1)} %concatenate.13), channel_id=1, source_target_pairs={{0,16},{8,24},{16,0},{24,8},{1,17},{9,25},{17,1},{25,9},{2,18},{10... | collective-permute-start | bytes 540680 | tf_op jit(solution)/shard_map/ppermute | solution.py:41
  8.7 20.5 %collective-permute-start.11 = (bf16[64,1408]{1,0:T(8,128)(2,1)S(1)}, bf16[64,1408]{1,0:T(8,128)(2,1)S(1)}, u32[]{:S(2)}, u32[]{:S(2)}) collective-permute-start(bf16[64,1408]{1,0:T(8,128)(2,1)S(1)} %concatenate.13), channel_id=1, source_target_pairs={{0,24},{8,0},{16,8},{24,16},{1,25},{9,1},{17,9},{25,17},{2,26},{10... | collective-permute-start | bytes 540680 | tf_op jit(solution)/shard_map/ppermute | solution.py:41
  9.1 6.2 %collective-permute-start = (bf16[129,128]{1,0:T(8,128)(2,1)S(1)}, bf16[129,128]{1,0:T(8,128)(2,1)S(1)}, u32[]{:S(2)}, u32[]{:S(2)}) collective-permute-start(bf16[129,128]{1,0:T(8,128)(2,1)S(1)} %get-tuple-element.73), channel_id=1, source_target_pairs={{0,8},{8,16},{16,24},{24,32},{32,40},{40,48},{48,56},{56,64},{64,7... | collective-permute-start | bytes 99080 | tf_op jit(solution)/shard_map/ppermute | solution.py:346
  12.6 5.8 %collective-permute-start.1 = (bf16[129,128]{1,0:T(8,128)(2,1)S(1)}, bf16[129,128]{1,0:T(8,128)(2,1)S(1)}, u32[]{:S(2)}, u32[]{:S(2)}) collective-permute-start(bf16[129,128]{1,0:T(8,128)(2,1)S(1)} %get-tuple-element.72), channel_id=1, source_target_pairs={{8,0},{16,8},{24,16},{32,24},{40,32},{48,40},{56,48},{64,56},{72,6... | collective-permute-start | bytes 99080 | tf_op jit(solution)/shard_map/ppermute | solution.py:347
  18.4 1.2 copy-start
  19.6 1.0 copy-start.1
  20.6 0.7 copy-start.4
  29.1 44.9 %copy-start.5 = (bf16[64,704]{1,0:T(8,128)(2,1)S(1)}, bf16[64,704]{1,0:T(8,128)(2,1)}, u32[]{:S(2)}) copy-start(bf16[64,704]{1,0:T(8,128)(2,1)} %param.23) | copy-start | bytes 270340
  29.1 25.2 %collective-permute-start.2 = (bf16[4,768,256]{2,1,0:T(8,128)(2,1)S(1)}, bf16[4,768,256]{2,1,0:T(8,128)(2,1)S(1)}, u32[]{:S(2)}, u32[]{:S(2)}) collective-permute-start(bf16[4,768,256]{2,1,0:T(8,128)(2,1)S(1)} %get-tuple-element.33), channel_id=1, source_target_pairs={{0,1},{1,0},{2,3},{3,2},{4,5},{5,4},{6,7},{7,6},{8,9},{9,8},{10,11... | collective-permute-start | bytes 4718600 | tf_op jit(solution)/shard_map/ppermute | solution.py:45
  29.3 21.7 %collective-permute-start.12 = (bf16[256,1408]{1,0:T(8,128)(2,1)S(1)}, bf16[256,1408]{1,0:T(8,128)(2,1)}, u32[]{:S(2)}, u32[]{:S(2)}) collective-permute-start(bf16[256,1408]{1,0:T(8,128)(2,1)S(1)} %bitcast.88), channel_id=1, source_target_pairs={{0,32},{32,64},{64,96},{96,128},{128,160},{160,192},{192,224},{224... | collective-permute-start | bytes 2162696 | tf_op jit(solution)/shard_map/ppermute | solution.py:37
  30.2 20.8 %collective-permute-start.14 = (bf16[256,1408]{1,0:T(8,128)(2,1)S(1)}, bf16[256,1408]{1,0:T(8,128)(2,1)}, u32[]{:S(2)}, u32[]{:S(2)}) collective-permute-start(bf16[256,1408]{1,0:T(8,128)(2,1)S(1)} %bitcast.89), channel_id=1, source_target_pairs={{0,224},{32,0},{64,32},{96,64},{128,96},{160,128},{192,160},{224,1... | collective-permute-start | bytes 2162696 | tf_op jit(solution)/shard_map/ppermute | solution.py:37
  51.0 29.1 %collective-permute-start.13 = (bf16[256,1408]{1,0:T(8,128)(2,1)}, bf16[256,1408]{1,0:T(8,128)(2,1)S(1)}, u32[]{:S(2)}, u32[]{:S(2)}) collective-permute-start(bf16[256,1408]{1,0:T(8,128)(2,1)} %collective-permute-done.12), channel_id=1, source_target_pairs={{0,32},{32,64},{64,96},{96,128},{128,160},{160,192},{192,224},{224... | collective-permute-start | bytes 2162696 | tf_op jit(solution)/shard_map/ppermute | solution.py:37
  51.0 30.9 %collective-permute-start.15 = (bf16[256,1408]{1,0:T(8,128)(2,1)}, bf16[256,1408]{1,0:T(8,128)(2,1)}, u32[]{:S(2)}, u32[]{:S(2)}) collective-permute-start(bf16[256,1408]{1,0:T(8,128)(2,1)} %collective-permute-done.14), channel_id=1, source_target_pairs={{0,224},{32,0},{64,32},{96,64},{128,96},{160,128},{192,160},{224,1... | collective-permute-start | bytes 2162696 | tf_op jit(solution)/shard_map/ppermute | solution.py:37
  54.6 19.4 %collective-permute-start.5 = (bf16[768,256]{1,0:T(8,128)(2,1)S(1)}, bf16[768,256]{1,0:T(8,128)(2,1)}, u32[]{:S(2)}, u32[]{:S(2)}) collective-permute-start(bf16[768,256]{1,0:T(8,128)(2,1)S(1)} %get-tuple-element.37), channel_id=1, source_target_pairs={{0,6},{2,0},{4,2},{6,4},{1,7},{3,1},{5,3},{7,5},{8,14},{10,8},{12,... | collective-permute-start | bytes 1179656 | tf_op jit(solution)/shard_map/ppermute | solution.py:312
  57.7 16.3 %collective-permute-start.4 = (bf16[768,256]{1,0:T(8,128)(2,1)S(1)}, bf16[768,256]{1,0:T(8,128)(2,1)}, u32[]{:S(2)}, u32[]{:S(2)}) collective-permute-start(bf16[768,256]{1,0:T(8,128)(2,1)S(1)} %get-tuple-element.36), channel_id=1, source_target_pairs={{0,4},{2,6},{4,0},{6,2},{1,5},{3,7},{5,1},{7,3},{8,12},{10,14},{12... | collective-permute-start | bytes 1179656 | tf_op jit(solution)/shard_map/ppermute | solution.py:312
  58.3 19.5 %collective-permute-start.3 = (bf16[768,256]{1,0:T(8,128)(2,1)S(1)}, bf16[768,256]{1,0:T(8,128)(2,1)}, u32[]{:S(2)}, u32[]{:S(2)}) collective-permute-start(bf16[768,256]{1,0:T(8,128)(2,1)S(1)} %get-tuple-element.35), channel_id=1, source_target_pairs={{0,2},{2,4},{4,6},{6,0},{1,3},{3,5},{5,7},{7,1},{8,10},{10,12},{12... | collective-permute-start | bytes 1179656 | tf_op jit(solution)/shard_map/ppermute | solution.py:312
  74.0 13.2 %collective-permute-start.19 = (bf16[64,704]{1,0:T(8,128)(2,1)S(1)}, bf16[64,704]{1,0:T(8,128)(2,1)S(1)}, u32[]{:S(2)}, u32[]{:S(2)}) collective-permute-start(bf16[64,704]{1,0:T(8,128)(2,1)S(1)} %copy-done.5), channel_id=1, source_target_pairs={{0,32},{32,64},{64,96},{96,128},{128,160},{160,192},{192,224},{224... | collective-permute-start | bytes 270344 | tf_op jit(solution)/shard_map/ppermute | solution.py:37
  74.0 8.3 %collective-permute-start.21 = (bf16[64,704]{1,0:T(8,128)(2,1)S(1)}, bf16[64,704]{1,0:T(8,128)(2,1)S(1)}, u32[]{:S(2)}, u32[]{:S(2)}) collective-permute-start(bf16[64,704]{1,0:T(8,128)(2,1)S(1)} %copy-done.5), channel_id=1, source_target_pairs={{0,64},{32,96},{64,128},{96,160},{128,192},{160,224},{192,0},{224,... | collective-permute-start | bytes 270344 | tf_op jit(solution)/shard_map/ppermute | solution.py:37
  77.8 7.3 %collective-permute-start.22 = (bf16[64,704]{1,0:T(8,128)(2,1)S(1)}, bf16[64,704]{1,0:T(8,128)(2,1)S(1)}, u32[]{:S(2)}, u32[]{:S(2)}) collective-permute-start(bf16[64,704]{1,0:T(8,128)(2,1)S(1)} %copy-done.5), channel_id=1, source_target_pairs={{0,192},{32,224},{64,0},{96,32},{128,64},{160,96},{192,128},{224,1... | collective-permute-start | bytes 270344 | tf_op jit(solution)/shard_map/ppermute | solution.py:37
  80.1 12.2 %collective-permute-start.20 = (bf16[64,704]{1,0:T(8,128)(2,1)S(1)}, bf16[64,704]{1,0:T(8,128)(2,1)S(1)}, u32[]{:S(2)}, u32[]{:S(2)}) collective-permute-start(bf16[64,704]{1,0:T(8,128)(2,1)S(1)} %copy-done.5), channel_id=1, source_target_pairs={{0,224},{32,0},{64,32},{96,64},{128,96},{160,128},{192,160},{224,1... | collective-permute-start | bytes 270344 | tf_op jit(solution)/shard_map/ppermute | solution.py:37
  81.9 39.5 %collective-permute-start.17 = (bf16[256,1408]{1,0:T(8,128)(2,1)S(1)}, bf16[256,1408]{1,0:T(8,128)(2,1)S(1)}, u32[]{:S(2)}, u32[]{:S(2)}) collective-permute-start(bf16[256,1408]{1,0:T(8,128)(2,1)S(1)} %collective-permute-done.13), channel_id=1, source_target_pairs={{0,32},{32,64},{64,96},{96,128},{128,160},{160,192},{192,224},{224... | collective-permute-start | bytes 2162696 | tf_op jit(solution)/shard_map/ppermute | solution.py:37
  82.2 39.1 %collective-permute-start.18 = (bf16[256,1408]{1,0:T(8,128)(2,1)}, bf16[256,1408]{1,0:T(8,128)(2,1)S(1)}, u32[]{:S(2)}, u32[]{:S(2)}) collective-permute-start(bf16[256,1408]{1,0:T(8,128)(2,1)} %collective-permute-done.15), channel_id=1, source_target_pairs={{0,224},{32,0},{64,32},{96,64},{128,96},{160,128},{192,160},{224,1... | collective-permute-start | bytes 2162696 | tf_op jit(solution)/shard_map/ppermute | solution.py:37
  85.1 19.4 %collective-permute-start.6 = (bf16[768,256]{1,0:T(8,128)(2,1)S(1)}, bf16[768,256]{1,0:T(8,128)(2,1)S(1)}, u32[]{:S(2)}, u32[]{:S(2)}) collective-permute-start(bf16[768,256]{1,0:T(8,128)(2,1)S(1)} %add_convert_fusion.2.p0), channel_id=1, source_target_pairs={{0,2},{2,4},{4,6},{6,0},{1,3},{3,5},{5,7},{7,1},{8,10},{10,12},{12... | collective-permute-start | bytes 1179656 | tf_op jit(solution)/shard_map/ppermute | solution.py:312
  87.2 17.4 %collective-permute-start.7 = (bf16[768,256]{1,0:T(8,128)(2,1)S(1)}, bf16[768,256]{1,0:T(8,128)(2,1)S(1)}, u32[]{:S(2)}, u32[]{:S(2)}) collective-permute-start(bf16[768,256]{1,0:T(8,128)(2,1)S(1)} %add_convert_fusion.2.p0), channel_id=1, source_target_pairs={{0,4},{2,6},{4,0},{6,2},{1,5},{3,7},{5,1},{7,3},{8,12},{10,14},{12... | collective-permute-start | bytes 1179656 | tf_op jit(solution)/shard_map/ppermute | solution.py:312
  92.3 15.5 %collective-permute-start.8 = (bf16[768,256]{1,0:T(8,128)(2,1)S(1)}, bf16[768,256]{1,0:T(8,128)(2,1)S(1)}, u32[]{:S(2)}, u32[]{:S(2)}) collective-permute-start(bf16[768,256]{1,0:T(8,128)(2,1)S(1)} %add_convert_fusion.2.p0), channel_id=1, source_target_pairs={{0,6},{2,0},{4,2},{6,4},{1,7},{3,1},{5,3},{7,5},{8,14},{10,8},{12,... | collective-permute-start | bytes 1179656 | tf_op jit(solution)/shard_map/ppermute | solution.py:312
  104.6 5.8 %collective-permute-start.23 = (bf16[64,704]{1,0:T(8,128)(2,1)S(1)}, bf16[64,704]{1,0:T(8,128)(2,1)S(1)}, u32[]{:S(2)}, u32[]{:S(2)}) collective-permute-start(bf16[64,704]{1,0:T(8,128)(2,1)S(1)} %collective-permute-done.21), channel_id=1, source_target_pairs={{0,32},{32,64},{64,96},{96,128},{128,160},{160,192},{192,224},{224... | collective-permute-start | bytes 270344 | tf_op jit(solution)/shard_map/ppermute | solution.py:37
  104.6 6.4 %collective-permute-start.24 = (bf16[64,704]{1,0:T(8,128)(2,1)S(1)}, bf16[64,704]{1,0:T(8,128)(2,1)S(1)}, u32[]{:S(2)}, u32[]{:S(2)}) collective-permute-start(bf16[64,704]{1,0:T(8,128)(2,1)S(1)} %collective-permute-done.22), channel_id=1, source_target_pairs={{0,224},{32,0},{64,32},{96,64},{128,96},{160,128},{192,160},{224,1... | collective-permute-start | bytes 270344 | tf_op jit(solution)/shard_map/ppermute | solution.py:37
  107.8 13.9 %copy-start.2 = (f32[2048]{0:T(1024)S(1)}, f32[2048]{0:T(1024)}, u32[]{:S(2)}) copy-start(f32[2048]{0:T(1024)} %param.19) | copy-start | bytes 24580
  108.0 13.7 %collective-permute-start.16 = (bf16[4,768,256]{2,1,0:T(8,128)(2,1)S(1)}, bf16[4,768,256]{2,1,0:T(8,128)(2,1)S(1)}, u32[]{:S(2)}, u32[]{:S(2)}) collective-permute-start(bf16[4,768,256]{2,1,0:T(8,128)(2,1)S(1)} %pad_maximum_fusion), channel_id=1, source_target_pairs={{0,1},{1,0},{2,3},{3,2},{4,5},{5,4},{6,7},{7,6},{8,9},{9,8},{10,11... | collective-permute-start | bytes 4718600 | tf_op jit(solution)/shard_map/ppermute | solution.py:45
  110.4 6.7 %collective-permute-start.25 = (bf16[64,704]{1,0:T(8,128)(2,1)S(1)}, bf16[64,704]{1,0:T(8,128)(2,1)S(1)}, u32[]{:S(2)}, u32[]{:S(2)}) collective-permute-start(bf16[64,704]{1,0:T(8,128)(2,1)S(1)} %broadcast_select_fusion.2), channel_id=1, source_target_pairs={{0,64},{1,193},{2,66},{3,195},{4,68},{5,197},{6,70},{7,199},{8,72}... | collective-permute-start | bytes 270344 | tf_op jit(solution)/shard_map/ppermute | solution.py:33
  117.1 18.3 %collective-permute-start.26 = (bf16[8,64,704]{2,1,0:T(8,128)(2,1)S(1)}, bf16[8,64,704]{2,1,0:T(8,128)(2,1)S(1)}, u32[]{:S(2)}, u32[]{:S(2)}) collective-permute-start(bf16[8,64,704]{2,1,0:T(8,128)(2,1)S(1)} %bitcast_dynamic-update-slice_fusion.16), channel_id=1, source_target_pairs={{0,8},{8,16},{16,24},{24,0},{1,9},{9,17},{17,25},{25,1},{2,10},{10... | collective-permute-start | bytes 2162696 | tf_op jit(solution)/shard_map/ppermute | solution.py:41
  119.3 20.2 %collective-permute-start.27 = (bf16[8,64,704]{2,1,0:T(8,128)(2,1)S(1)}, bf16[8,64,704]{2,1,0:T(8,128)(2,1)S(1)}, u32[]{:S(2)}, u32[]{:S(2)}) collective-permute-start(bf16[8,64,704]{2,1,0:T(8,128)(2,1)S(1)} %bitcast_dynamic-update-slice_fusion.16), channel_id=1, source_target_pairs={{0,24},{8,0},{16,8},{24,16},{1,25},{9,1},{17,9},{25,17},{2,26},{10... | collective-permute-start | bytes 2162696 | tf_op jit(solution)/shard_map/ppermute | solution.py:41
  121.4 20.3 %collective-permute-start.28 = (bf16[256,1408]{1,0:T(8,128)(2,1)S(1)}, bf16[256,1408]{1,0:T(8,128)(2,1)S(1)}, u32[]{:S(2)}, u32[]{:S(2)}) collective-permute-start(bf16[256,1408]{1,0:T(8,128)(2,1)S(1)} %broadcast_select_fusion.1), channel_id=1, source_target_pairs={{0,32},{1,225},{2,34},{3,227},{4,36},{5,229},{6,38},{7,231},{8,40}... | collective-permute-start | bytes 2162696 | tf_op jit(solution)/shard_map/ppermute | solution.py:33
  139.8 16.9 %collective-permute-start.31 = (bf16[8,64,704]{2,1,0:T(8,128)(2,1)S(1)}, bf16[8,64,704]{2,1,0:T(8,128)(2,1)S(1)}, u32[]{:S(2)}, u32[]{:S(2)}) collective-permute-start(bf16[8,64,704]{2,1,0:T(8,128)(2,1)S(1)} %broadcast_select_fusion), channel_id=1, source_target_pairs={{0,8},{1,25},{2,10},{3,27},{4,12},{5,29},{6,14},{7,31},{8,16},{9,1... | collective-permute-start | bytes 2162696 | tf_op jit(solution)/shard_map/ppermute | solution.py:33
  144.9 8.9 %collective-permute-start.29 = (bf16[1,704]{1,0:T(2,128)(2,1)S(1)}, bf16[1,704]{1,0:T(2,128)(2,1)S(1)}, u32[]{:S(2)}, u32[]{:S(2)}) collective-permute-start(bf16[1,704]{1,0:T(2,128)(2,1)S(1)} %get-tuple-element.71), channel_id=1, source_target_pairs={{0,8},{8,16},{16,24},{24,32},{32,40},{40,48},{48,56},{56,64},{64,7... | collective-permute-start | bytes 4232 | tf_op jit(solution)/shard_map/ppermute | solution.py:431
  147.0 6.8 %copy-start.3 = (bf16[3,704]{1,0:T(4,128)(2,1)S(1)}, bf16[3,704]{1,0:T(4,128)(2,1)}, u32[]{:S(2)}) copy-start(bf16[3,704]{1,0:T(4,128)(2,1)} %taps_ref.1) | copy-start | bytes 12676
  147.0 6.8 %collective-permute-start.30 = (bf16[1,704]{1,0:T(2,128)(2,1)S(1)}, bf16[1,704]{1,0:T(2,128)(2,1)S(1)}, u32[]{:S(2)}, u32[]{:S(2)}) collective-permute-start(bf16[1,704]{1,0:T(2,128)(2,1)S(1)} %get-tuple-element.70), channel_id=1, source_target_pairs={{8,0},{16,8},{24,16},{32,24},{40,32},{48,40},{56,48},{64,56},{72,6... | collective-permute-start | bytes 4232 | tf_op jit(solution)/shard_map/ppermute | solution.py:432
  158.4 3.5 %collective-permute-start.32 = (bf16[768,1024]{1,0:T(8,128)(2,1)S(1)}, bf16[768,1024]{1,0:T(8,128)(2,1)S(1)}, u32[]{:S(2)}, u32[]{:S(2)}) collective-permute-start(bf16[768,1024]{1,0:T(8,128)(2,1)S(1)} %convolution_convert_fusion), channel_id=1, source_target_pairs={{0,1},{1,0},{2,3},{3,2},{4,5},{5,4},{6,7},{7,6},{8,9},{9,8},{10,11... | collective-permute-start | bytes 4718600 | tf_op jit(solution)/shard_map/ppermute | solution.py:45
  162.7 12.1 %collective-permute-start.35 = (bf16[768,256]{1,0:T(8,128)(2,1)S(1)}, bf16[768,256]{1,0:T(8,128)(2,1)S(1)}, u32[]{:S(2)}, u32[]{:S(2)}) collective-permute-start(bf16[768,256]{1,0:T(8,128)(2,1)S(1)} %get-tuple-element.68), channel_id=1, source_target_pairs={{0,6},{2,0},{4,2},{6,4},{1,7},{3,1},{5,3},{7,5},{8,14},{10,8},{12,... | collective-permute-start | bytes 1179656 | tf_op jit(solution)/shard_map/ppermute | solution.py:312
  163.3 13.5 %collective-permute-start.34 = (bf16[768,256]{1,0:T(8,128)(2,1)S(1)}, bf16[768,256]{1,0:T(8,128)(2,1)S(1)}, u32[]{:S(2)}, u32[]{:S(2)}) collective-permute-start(bf16[768,256]{1,0:T(8,128)(2,1)S(1)} %get-tuple-element.69), channel_id=1, source_target_pairs={{0,4},{2,6},{4,0},{6,2},{1,5},{3,7},{5,1},{7,3},{8,12},{10,14},{12... | collective-permute-start | bytes 1179656 | tf_op jit(solution)/shard_map/ppermute | solution.py:312
  163.3 20.8 %collective-permute-start.33 = (bf16[768,256]{1,0:T(8,128)(2,1)S(1)}, bf16[768,256]{1,0:T(8,128)(2,1)S(1)}, u32[]{:S(2)}, u32[]{:S(2)}) collective-permute-start(bf16[768,256]{1,0:T(8,128)(2,1)S(1)} %get-tuple-element.67), channel_id=1, source_target_pairs={{0,2},{2,4},{4,6},{6,0},{1,3},{3,5},{5,7},{7,1},{8,10},{10,12},{12... | collective-permute-start | bytes 1179656 | tf_op jit(solution)/shard_map/ppermute | solution.py:312

commit v6 on v5

--- a/solution.py
+++ b/solution.py
@@ -364,23 +364,22 @@
     def keep(full, plus, minus, k):
         return put(put(full, plus, (z - k) % NZ), minus, (z + k) % NZ)
 
-    theirs, mine, same = attention(order, sink_logits, queries, packed, low, high, w_out)
-    got = swap(theirs)
-
-    gathered = lax.optimization_barrier((*gathered, theirs))[:-1]
+    down1 = after(w_down_t, share)
+    near = ring_step(down1, down1)
+    far_plus = send_z(down1, 2)
+    far_minus = send_z(down1, -2)
+
     up_rows = put(jnp.zeros((NX, rows_w, width), share.dtype), share, x)
     for k, piece in enumerate(gathered):
         up_rows = put(up_rows, piece, (x - k - 1) % NX)
     up_rows = up_rows.reshape(NX * rows_w, width)
     plus1, minus1 = ring_step(up_rows, up_rows)
 
+    theirs, mine, same = attention(order, sink_logits, queries, packed, low, high, w_out)
+    got = swap(theirs)
+
     pairs = pair_sums(mine, got)
     sent = to_owners(pairs)
-
-    down1 = after(w_down_t, pairs[0])
-    near = ring_step(down1, down1)
-    far_plus = send_z(down1, 2)
-    far_minus = send_z(down1, -2)
 
     plus2, minus2 = ring_step(plus1, minus1)
     own_res = lax.dynamic_slice_in_dim(residual, tp * span, span, 1)
@@ -389,7 +388,7 @@
         summed = summed + block.astype(jnp.float32)
     mixed_own = (own_res.astype(jnp.float32) + summed).astype(jnp.bfloat16)
 
-    far_plus, far_minus = lax.optimization_barrier((far_plus, far_minus, mixed_own))[:2]
+    far_plus, far_minus = lax.optimization_barrier((far_plus, far_minus, pairs[0]))[:2]
     third = ring_step(far_plus, far_minus)
     last_down = send_apart(jnp.where(core == 0, far_plus, far_minus), 2, 0)
 

time: 188 us -> 178 us (0.947)
  the two profiles are of different devices: /device:TPU:2 before, /device:TPU:103 now
where the time goes in v6:
time: 178 us; the launch traced here: 177 us
  waiting for transfers between devices  85 us (48%)
  starting transfers between devices  52.3 us (29%)
  Pallas kernels  19.6 us (11%)
  local copies, waits for them, and re-layouts  11.6 us (7%)
  other arithmetic  5.39 us (3%)
  matrix products  2.85 us (2%)
    ppermute x9, waiting for transfers between devices, to_owners(): lax.ppermute(pairs[k], 'y', [(y, (y + k) % NY) for y in range(NY)])  49.7 us
    ppermute x12, waiting for transfers between devices, send_z(): return lax.ppermute(block, 'z', [(z, (z + k) % NZ) for z in range(NZ)])  18.5 us
    ppermute x12, starting transfers between devices, send_z(): return lax.ppermute(block, 'z', [(z, (z + k) % NZ) for z in range(NZ)])  15.2 us
    pallas_call x1, Pallas kernels, attention(): pl.pallas_call(attention_kernel, out_shape=[jax.ShapeDtypeStruct((NY, row...  7.75 us
    ppermute x1, starting transfers between devices, per_device(): before = lax.ppermute(up_value[-1:, :ff], ('z', 'x'), forward)  7.58 us
    ppermute x3, starting transfers between devices, swap(): return lax.ppermute(block, 'core', [(0, 1), (1, 0)])  7.36 us
    ppermute x1, starting transfers between devices, per_device(): low = lax.ppermute(packed[:, -WINDOW:], ('z', 'x'), forward)  7.13 us
    ppermute x9, starting transfers between devices, to_owners(): lax.ppermute(pairs[k], 'y', [(y, (y + k) % NY) for y in range(NY)])  6.9 us
  transfers between devices with their start and end apart: 36, of which 15 were waited for; matrix products, arithmetic and copies ran while one was open for 5% of the time, Pallas kernels for 11%

profile of v6, /device:TPU:103, one launch (start us, length us, event | category | flops | bytes accessed | tf_op | source)
XLA Modules:
  0.0 177.5 jit_solution(18427710558150937732)
XLA Ops:
  3.3 1.0 concatenate.13
  4.5 2.1 %collective-permute-start.10 = (bf16[64,1408]{1,0:T(8,128)(2,1)S(1)}, bf16[64,1408]{1,0:T(8,128)(2,1)S(1)}, u32[]{:S(2)}, u32[]{:S(2)}) collective-permute-start(bf16[64,1408]{1,0:T(8,128)(2,1)S(1)} %concatenate.13), channel_id=1, source_target_pairs={{0,16},{8,24},{16,0},{24,8},{1,17},{9,25},{17,1},{25,9},{2,18},{10... | collective-permute-start | bytes 540680 | tf_op jit(solution)/shard_map/ppermute | solution.py:41
  6.7 7.1 %collective-permute-start = (bf16[129,128]{1,0:T(8,128)(2,1)S(1)}, bf16[129,128]{1,0:T(8,128)(2,1)S(1)}, u32[]{:S(2)}, u32[]{:S(2)}) collective-permute-start(bf16[129,128]{1,0:T(8,128)(2,1)S(1)} %get-tuple-element.67), channel_id=1, source_target_pairs={{0,8},{8,16},{16,24},{24,32},{32,40},{40,48},{48,56},{56,64},{64,7... | collective-permute-start | bytes 99080 | tf_op jit(solution)/shard_map/ppermute | solution.py:346
  13.8 1.9 %collective-permute-start.1 = (bf16[129,128]{1,0:T(8,128)(2,1)S(1)}, bf16[129,128]{1,0:T(8,128)(2,1)S(1)}, u32[]{:S(2)}, u32[]{:S(2)}) collective-permute-start(bf16[129,128]{1,0:T(8,128)(2,1)S(1)} %get-tuple-element.66), channel_id=1, source_target_pairs={{8,0},{16,8},{24,16},{32,24},{40,32},{48,40},{56,48},{64,56},{72,6... | collective-permute-start | bytes 99080 | tf_op jit(solution)/shard_map/ppermute | solution.py:347
  16.1 5.7 %collective-permute-done.1.high_ref = bf16[129,128]{1,0:T(8,128)(2,1)S(1)} collective-permute-done((bf16[129,128]{1,0:T(8,128)(2,1)S(1)}, bf16[129,128]{1,0:T(8,128)(2,1)S(1)}, u32[]{:S(2)}, u32[]{:S(2)}) %collective-permute-start.1) | collective-permute-done | bytes 33056 | tf_op jit(solution)/shard_map/ppermute | solution.py:347
  21.8 1.2 copy-done
  23.1 1.0 copy-done.1
  24.7 7.8 %attention.1 = (bf16[4,768,256]{2,1,0:T(8,128)(2,1)S(1)}, bf16[4,768,256]{2,1,0:T(8,128)(2,1)S(1)}, f32[768,128]{1,0:T(8,128)S(1)}) custom-call(s32[16]{0:T(128)S(1)} %stack.76.at_ref, f32[4]{0:T(128)S(1)} %copy-done.4, bf16[768,256]{1,0:T(8,128)(2,1)S(1)} %copy-done.1, bf16[256,2048]{1,0:T(8,128)(2,1)S(1)} %copy-done, ...), custom_call_target="tpu_custom_call" | custom-call | flops 4000000000 | bytes 4194304 | tf_op jit(solution)/shard_map/attention/pallas_call | solution.py:152
  32.5 3.0 %collective-permute-start.2 = (bf16[4,768,256]{2,1,0:T(8,128)(2,1)S(1)}, bf16[4,768,256]{2,1,0:T(8,128)(2,1)S(1)}, u32[]{:S(2)}, u32[]{:S(2)}) collective-permute-start(bf16[4,768,256]{2,1,0:T(8,128)(2,1)S(1)} %get-tuple-element.30), channel_id=1, source_target_pairs={{0,1},{1,0},{2,3},{3,2},{4,5},{5,4},{6,7},{7,6},{8,9},{9,8},{10,11... | collective-permute-start | bytes 4718600 | tf_op jit(solution)/shard_map/ppermute | solution.py:45
  35.7 1.5 collective-permute-start.14
  37.2 2.4 %collective-permute-start.22 = (bf16[64,704]{1,0:T(8,128)(2,1)S(1)}, bf16[64,704]{1,0:T(8,128)(2,1)S(1)}, u32[]{:S(2)}, u32[]{:S(2)}) collective-permute-start(bf16[64,704]{1,0:T(8,128)(2,1)S(1)} %copy-done.7), channel_id=1, source_target_pairs={{0,192},{32,224},{64,0},{96,32},{128,64},{160,96},{192,128},{224,1... | collective-permute-start | bytes 270344 | tf_op jit(solution)/shard_map/ppermute | solution.py:37
  39.5 16.0 %collective-permute-done.12 = bf16[256,1408]{1,0:T(8,128)(2,1)} collective-permute-done((bf16[256,1408]{1,0:T(8,128)(2,1)S(1)}, bf16[256,1408]{1,0:T(8,128)(2,1)}, u32[]{:S(2)}, u32[]{:S(2)}) %collective-permute-start.12) | collective-permute-done | bytes 720928 | tf_op jit(solution)/shard_map/ppermute | solution.py:37
  55.6 1.3 collective-permute-done.14
  57.4 2.8 %collective-permute-start.5 = (bf16[768,256]{1,0:T(8,128)(2,1)S(1)}, bf16[768,256]{1,0:T(8,128)(2,1)}, u32[]{:S(2)}, u32[]{:S(2)}) collective-permute-start(bf16[768,256]{1,0:T(8,128)(2,1)S(1)} %get-tuple-element.34), channel_id=1, source_target_pairs={{0,6},{2,0},{4,2},{6,4},{1,7},{3,1},{5,3},{7,5},{8,14},{10,8},{12,... | collective-permute-start | bytes 1179656 | tf_op jit(solution)/shard_map/ppermute | solution.py:312
  61.3 6.5 %collective-permute-done.5 = bf16[768,256]{1,0:T(8,128)(2,1)} collective-permute-done((bf16[768,256]{1,0:T(8,128)(2,1)S(1)}, bf16[768,256]{1,0:T(8,128)(2,1)}, u32[]{:S(2)}, u32[]{:S(2)}) %collective-permute-start.5) | collective-permute-done | bytes 393248 | tf_op jit(solution)/shard_map/ppermute | solution.py:312
  67.8 2.8 %collective-permute-start.19 = (bf16[64,704]{1,0:T(8,128)(2,1)}, bf16[64,704]{1,0:T(8,128)(2,1)S(1)}, u32[]{:S(2)}, u32[]{:S(2)}) collective-permute-start(bf16[64,704]{1,0:T(8,128)(2,1)} %param.23), channel_id=1, source_target_pairs={{0,32},{32,64},{64,96},{96,128},{128,160},{160,192},{192,224},{224... | collective-permute-start | bytes 270344 | tf_op jit(solution)/shard_map/ppermute | solution.py:37
  70.7 10.6 %collective-permute-done.3 = bf16[768,256]{1,0:T(8,128)(2,1)} collective-permute-done((bf16[768,256]{1,0:T(8,128)(2,1)S(1)}, bf16[768,256]{1,0:T(8,128)(2,1)}, u32[]{:S(2)}, u32[]{:S(2)}) %collective-permute-start.3) | collective-permute-done | bytes 393248 | tf_op jit(solution)/shard_map/ppermute | solution.py:312
  81.3 2.5 %collective-permute-start.23 = (bf16[64,704]{1,0:T(8,128)(2,1)}, bf16[64,704]{1,0:T(8,128)(2,1)S(1)}, u32[]{:S(2)}, u32[]{:S(2)}) collective-permute-start(bf16[64,704]{1,0:T(8,128)(2,1)} %copy-done.5), channel_id=1, source_target_pairs={{0,32},{32,64},{64,96},{96,128},{128,160},{160,192},{192,224},{224... | collective-permute-start | bytes 270344 | tf_op jit(solution)/shard_map/ppermute | solution.py:37
  83.8 1.6 add_convert_fusion.2.p0
  85.7 2.6 %collective-permute-start.17 = (bf16[256,1408]{1,0:T(8,128)(2,1)S(1)}, bf16[256,1408]{1,0:T(8,128)(2,1)S(1)}, u32[]{:S(2)}, u32[]{:S(2)}) collective-permute-start(bf16[256,1408]{1,0:T(8,128)(2,1)S(1)} %collective-permute-done.13), channel_id=1, source_target_pairs={{0,32},{32,64},{64,96},{96,128},{128,160},{160,192},{192,224},{224... | collective-permute-start | bytes 2162696 | tf_op jit(solution)/shard_map/ppermute | solution.py:37
  89.0 1.2 collective-permute-done.24
  90.2 1.3 collective-permute-start.8
  91.5 3.0 %collective-permute-start.18 = (bf16[256,1408]{1,0:T(8,128)(2,1)}, bf16[256,1408]{1,0:T(8,128)(2,1)S(1)}, u32[]{:S(2)}, u32[]{:S(2)}) collective-permute-start(bf16[256,1408]{1,0:T(8,128)(2,1)} %collective-permute-done.15), channel_id=1, source_target_pairs={{0,224},{32,0},{64,32},{96,64},{128,96},{160,128},{192,160},{224,1... | collective-permute-start | bytes 2162696 | tf_op jit(solution)/shard_map/ppermute | solution.py:37
  94.5 13.0 %collective-permute-done.6.p1 = bf16[768,256]{1,0:T(8,128)(2,1)S(1)} collective-permute-done((bf16[768,256]{1,0:T(8,128)(2,1)S(1)}, bf16[768,256]{1,0:T(8,128)(2,1)S(1)}, u32[]{:S(2)}, u32[]{:S(2)}) %collective-permute-start.6) | collective-permute-done | bytes 393248 | tf_op jit(solution)/shard_map/ppermute | solution.py:312
  107.5 1.5 collective-permute-start.27
  109.1 2.8 %collective-permute-start.16 = (bf16[4,768,256]{2,1,0:T(8,128)(2,1)S(1)}, bf16[4,768,256]{2,1,0:T(8,128)(2,1)S(1)}, u32[]{:S(2)}, u32[]{:S(2)}) collective-permute-start(bf16[4,768,256]{2,1,0:T(8,128)(2,1)S(1)} %pad_maximum_fusion), channel_id=1, source_target_pairs={{0,1},{1,0},{2,3},{3,2},{4,5},{5,4},{6,7},{7,6},{8,9},{9,8},{10,11... | collective-permute-start | bytes 4718600 | tf_op jit(solution)/shard_map/ppermute | solution.py:45
  112.5 1.2 bitcast_dynamic-update-slice_fusion.10
  113.7 1.2 bitcast_dynamic-update-slice_fusion.9
  115.4 2.6 %normalise.1.left_ref = bf16[768,2048]{1,0:T(8,128)(2,1)S(1)} custom-call(s32[16]{0:T(128)S(1)} %stack.76.at_ref, bf16[768,256]{1,0:T(8,128)(2,1)S(1)} %add_convert_fusion.2.p0, bf16[768,256]{1,0:T(8,128)(2,1)S(1)} %collective-permute-done.6.p1, bf16[768,256]{1,0:T(8,128)(2,1)S(1)} %collective-permute-done.7.p2, ...), custom_call_target="tpu_custom_call" | custom-call | flops 2000000000 | bytes 6291456 | tf_op jit(solution)/shard_map/normalise/pallas_call | solution.py:214
  118.0 1.2 bitcast_dynamic-update-slice_fusion.7
  119.9 4.5 %collective-permute-done.26 = bf16[8,64,704]{2,1,0:T(8,128)(2,1)S(1)} collective-permute-done((bf16[8,64,704]{2,1,0:T(8,128)(2,1)S(1)}, bf16[8,64,704]{2,1,0:T(8,128)(2,1)S(1)}, u32[]{:S(2)}, u32[]{:S(2)}) %collective-permute-start.26) | collective-permute-done | bytes 720928 | tf_op jit(solution)/shard_map/ppermute | solution.py:41
  124.4 1.2 collective-permute-done.27
  125.9 1.0 collective-permute-done.28
  127.1 3.0 %shard_map.118.value_ref = bf16[768,768]{1,0:T(8,128)(2,1)S(1)} custom-call(bf16[768,2048]{1,0:T(8,128)(2,1)S(1)} %normalise.1.left_ref, bf16[2048,1408]{1,0:T(8,128)(2,1)S(1)} %bitcast.80), custom_call_target="tpu_custom_call" | custom-call | flops 3000000000 | bytes 8388608 | tf_op jit(solution)/shard_map/pallas_call | solution.py:239
  130.1 7.6 %collective-permute-start.29 = (bf16[1,704]{1,0:T(2,128)(2,1)S(1)}, bf16[1,704]{1,0:T(2,128)(2,1)S(1)}, u32[]{:S(2)}, u32[]{:S(2)}) collective-permute-start(bf16[1,704]{1,0:T(2,128)(2,1)S(1)} %get-tuple-element.65), channel_id=1, source_target_pairs={{0,8},{8,16},{16,24},{24,32},{32,40},{40,48},{48,56},{56,64},{64,7... | collective-permute-start | bytes 4232 | tf_op jit(solution)/shard_map/ppermute | solution.py:430
  137.7 1.9 %collective-permute-start.30 = (bf16[1,704]{1,0:T(2,128)(2,1)S(1)}, bf16[1,704]{1,0:T(2,128)(2,1)S(1)}, u32[]{:S(2)}, u32[]{:S(2)}) collective-permute-start(bf16[1,704]{1,0:T(2,128)(2,1)S(1)} %get-tuple-element.64), channel_id=1, source_target_pairs={{8,0},{16,8},{24,16},{32,24},{40,32},{48,40},{56,48},{64,56},{72,6... | collective-permute-start | bytes 4232 | tf_op jit(solution)/shard_map/ppermute | solution.py:431
  139.6 3.0 %shard_map.119.gate_ref = bf16[768,640]{1,0:T(8,128)(2,1)S(1)} custom-call(bf16[768,2048]{1,0:T(8,128)(2,1)S(1)} %normalise.1.left_ref, bf16[2048,1408]{1,0:T(8,128)(2,1)S(1)} %bitcast.81), custom_call_target="tpu_custom_call" | custom-call | flops 3000000000 | bytes 8388608 | tf_op jit(solution)/shard_map/pallas_call | solution.py:239
  142.7 2.7 %collective-permute-done.30.behind_ref = bf16[1,704]{1,0:T(2,128)(2,1)S(1)} collective-permute-done((bf16[1,704]{1,0:T(2,128)(2,1)S(1)}, bf16[1,704]{1,0:T(2,128)(2,1)S(1)}, u32[]{:S(2)}, u32[]{:S(2)}) %collective-permute-start.30) | collective-permute-done | bytes 1440 | tf_op jit(solution)/shard_map/ppermute | solution.py:431
  145.4 2.9 %hidden_units.1 = bf16[768,704]{1,0:T(8,128)(2,1)S(1)} custom-call(bf16[768,768]{1,0:T(8,128)(2,1)S(1)} %shard_map.118.value_ref, bf16[768,640]{1,0:T(8,128)(2,1)S(1)} %shard_map.119.gate_ref, f32[768,128]{1,0:T(8,128)S(1)} %get-tuple-element.51.same_ref, bf16[1,704]{1,0:T(2,128)(2,1)S(1)} %collective-permute-done.29.before_ref, ...), custom_call_target="tpu_custom_call" | custom-call | flops 2000000000 | bytes 4194304 | tf_op jit(solution)/shard_map/hidden_units/pallas_call | solution.py:298
  148.6 1.4 convolution_convert_fusion
  150.0 1.5 collective-permute-start.32
  151.5 1.4 convolution_convert_fusion.1
  152.9 1.6 collective-permute-done.32
  155.5 1.4 collective-permute-start.33
  156.9 8.8 %collective-permute-done.35 = bf16[768,256]{1,0:T(8,128)(2,1)S(1)} collective-permute-done((bf16[768,256]{1,0:T(8,128)(2,1)S(1)}, bf16[768,256]{1,0:T(8,128)(2,1)S(1)}, u32[]{:S(2)}, u32[]{:S(2)}) %collective-permute-start.35) | collective-permute-done | bytes 393248 | tf_op jit(solution)/shard_map/ppermute | solution.py:312
  165.7 1.6 collective-permute-done.34
  167.3 9.1 %collective-permute-done.33 = bf16[768,256]{1,0:T(8,128)(2,1)S(1)} collective-permute-done((bf16[768,256]{1,0:T(8,128)(2,1)S(1)}, bf16[768,256]{1,0:T(8,128)(2,1)S(1)}, u32[]{:S(2)}, u32[]{:S(2)}) %collective-permute-start.33) | collective-permute-done | bytes 393248 | tf_op jit(solution)/shard_map/ppermute | solution.py:312
  176.5 1.0 add_convert_fusion.1
  (96 shorter events, 10.6 us)
Async XLA Ops:
  4.3 31.2 %collective-permute-start.9 = (bf16[64,1408]{1,0:T(8,128)(2,1)S(1)}, bf16[64,1408]{1,0:T(8,128)(2,1)S(1)}, u32[]{:S(2)}, u32[]{:S(2)}) collective-permute-start(bf16[64,1408]{1,0:T(8,128)(2,1)S(1)} %concatenate.13), channel_id=1, source_target_pairs={{0,8},{8,16},{16,24},{24,0},{1,9},{9,17},{17,25},{25,1},{2,10},{10... | collective-permute-start | bytes 540680 | tf_op jit(solution)/shard_map/ppermute | solution.py:41
  4.5 31.0 %collective-permute-start.10 = (bf16[64,1408]{1,0:T(8,128)(2,1)S(1)}, bf16[64,1408]{1,0:T(8,128)(2,1)S(1)}, u32[]{:S(2)}, u32[]{:S(2)}) collective-permute-start(bf16[64,1408]{1,0:T(8,128)(2,1)S(1)} %concatenate.13), channel_id=1, source_target_pairs={{0,16},{8,24},{16,0},{24,8},{1,17},{9,25},{17,1},{25,9},{2,18},{10... | collective-permute-start | bytes 540680 | tf_op jit(solution)/shard_map/ppermute | solution.py:41
  6.7 28.9 %collective-permute-start.11 = (bf16[64,1408]{1,0:T(8,128)(2,1)S(1)}, bf16[64,1408]{1,0:T(8,128)(2,1)S(1)}, u32[]{:S(2)}, u32[]{:S(2)}) collective-permute-start(bf16[64,1408]{1,0:T(8,128)(2,1)S(1)} %concatenate.13), channel_id=1, source_target_pairs={{0,24},{8,0},{16,8},{24,16},{1,25},{9,1},{17,9},{25,17},{2,26},{10... | collective-permute-start | bytes 540680 | tf_op jit(solution)/shard_map/ppermute | solution.py:41
  6.7 9.4 %collective-permute-start = (bf16[129,128]{1,0:T(8,128)(2,1)S(1)}, bf16[129,128]{1,0:T(8,128)(2,1)S(1)}, u32[]{:S(2)}, u32[]{:S(2)}) collective-permute-start(bf16[129,128]{1,0:T(8,128)(2,1)S(1)} %get-tuple-element.67), channel_id=1, source_target_pairs={{0,8},{8,16},{16,24},{24,32},{32,40},{40,48},{48,56},{56,64},{64,7... | collective-permute-start | bytes 99080 | tf_op jit(solution)/shard_map/ppermute | solution.py:346
  13.8 8.0 %collective-permute-start.1 = (bf16[129,128]{1,0:T(8,128)(2,1)S(1)}, bf16[129,128]{1,0:T(8,128)(2,1)S(1)}, u32[]{:S(2)}, u32[]{:S(2)}) collective-permute-start(bf16[129,128]{1,0:T(8,128)(2,1)S(1)} %get-tuple-element.66), channel_id=1, source_target_pairs={{8,0},{16,8},{24,16},{32,24},{40,32},{48,40},{56,48},{64,56},{72,6... | collective-permute-start | bytes 99080 | tf_op jit(solution)/shard_map/ppermute | solution.py:347
  21.8 1.2 copy-start
  23.1 1.0 copy-start.1
  24.1 0.7 copy-start.4
  24.7 12.4 %copy-start.7 = (bf16[64,704]{1,0:T(8,128)(2,1)S(1)}, bf16[64,704]{1,0:T(8,128)(2,1)}, u32[]{:S(2)}) copy-start(bf16[64,704]{1,0:T(8,128)(2,1)} %param.23) | copy-start | bytes 270340
  32.5 24.6 %collective-permute-start.2 = (bf16[4,768,256]{2,1,0:T(8,128)(2,1)S(1)}, bf16[4,768,256]{2,1,0:T(8,128)(2,1)S(1)}, u32[]{:S(2)}, u32[]{:S(2)}) collective-permute-start(bf16[4,768,256]{2,1,0:T(8,128)(2,1)S(1)} %get-tuple-element.30), channel_id=1, source_target_pairs={{0,1},{1,0},{2,3},{3,2},{4,5},{5,4},{6,7},{7,6},{8,9},{9,8},{10,11... | collective-permute-start | bytes 4718600 | tf_op jit(solution)/shard_map/ppermute | solution.py:45
  35.6 20.0 %collective-permute-start.12 = (bf16[256,1408]{1,0:T(8,128)(2,1)S(1)}, bf16[256,1408]{1,0:T(8,128)(2,1)}, u32[]{:S(2)}, u32[]{:S(2)}) collective-permute-start(bf16[256,1408]{1,0:T(8,128)(2,1)S(1)} %bitcast.88), channel_id=1, source_target_pairs={{0,32},{32,64},{64,96},{96,128},{128,160},{160,192},{192,224},{224... | collective-permute-start | bytes 2162696 | tf_op jit(solution)/shard_map/ppermute | solution.py:37
  35.7 21.2 %collective-permute-start.14 = (bf16[256,1408]{1,0:T(8,128)(2,1)S(1)}, bf16[256,1408]{1,0:T(8,128)(2,1)}, u32[]{:S(2)}, u32[]{:S(2)}) collective-permute-start(bf16[256,1408]{1,0:T(8,128)(2,1)S(1)} %bitcast.89), channel_id=1, source_target_pairs={{0,224},{32,0},{64,32},{96,64},{128,96},{160,128},{192,160},{224,1... | collective-permute-start | bytes 2162696 | tf_op jit(solution)/shard_map/ppermute | solution.py:37
  37.2 23.0 %collective-permute-start.21 = (bf16[64,704]{1,0:T(8,128)(2,1)S(1)}, bf16[64,704]{1,0:T(8,128)(2,1)S(1)}, u32[]{:S(2)}, u32[]{:S(2)}) collective-permute-start(bf16[64,704]{1,0:T(8,128)(2,1)S(1)} %copy-done.7), channel_id=1, source_target_pairs={{0,64},{32,96},{64,128},{96,160},{128,192},{160,224},{192,0},{224,... | collective-permute-start | bytes 270344 | tf_op jit(solution)/shard_map/ppermute | solution.py:37
  37.2 23.4 %collective-permute-start.22 = (bf16[64,704]{1,0:T(8,128)(2,1)S(1)}, bf16[64,704]{1,0:T(8,128)(2,1)S(1)}, u32[]{:S(2)}, u32[]{:S(2)}) collective-permute-start(bf16[64,704]{1,0:T(8,128)(2,1)S(1)} %copy-done.7), channel_id=1, source_target_pairs={{0,192},{32,224},{64,0},{96,32},{128,64},{160,96},{192,128},{224,1... | collective-permute-start | bytes 270344 | tf_op jit(solution)/shard_map/ppermute | solution.py:37
  55.6 29.9 %collective-permute-start.13 = (bf16[256,1408]{1,0:T(8,128)(2,1)}, bf16[256,1408]{1,0:T(8,128)(2,1)S(1)}, u32[]{:S(2)}, u32[]{:S(2)}) collective-permute-start(bf16[256,1408]{1,0:T(8,128)(2,1)} %collective-permute-done.12), channel_id=1, source_target_pairs={{0,32},{32,64},{64,96},{96,128},{128,160},{160,192},{192,224},{224... | collective-permute-start | bytes 2162696 | tf_op jit(solution)/shard_map/ppermute | solution.py:37
  56.9 28.7 %collective-permute-start.15 = (bf16[256,1408]{1,0:T(8,128)(2,1)}, bf16[256,1408]{1,0:T(8,128)(2,1)}, u32[]{:S(2)}, u32[]{:S(2)}) collective-permute-start(bf16[256,1408]{1,0:T(8,128)(2,1)} %collective-permute-done.14), channel_id=1, source_target_pairs={{0,224},{32,0},{64,32},{96,64},{128,96},{160,128},{192,160},{224,1... | collective-permute-start | bytes 2162696 | tf_op jit(solution)/shard_map/ppermute | solution.py:37
  57.4 10.4 %collective-permute-start.5 = (bf16[768,256]{1,0:T(8,128)(2,1)S(1)}, bf16[768,256]{1,0:T(8,128)(2,1)}, u32[]{:S(2)}, u32[]{:S(2)}) collective-permute-start(bf16[768,256]{1,0:T(8,128)(2,1)S(1)} %get-tuple-element.34), channel_id=1, source_target_pairs={{0,6},{2,0},{4,2},{6,4},{1,7},{3,1},{5,3},{7,5},{8,14},{10,8},{12,... | collective-permute-start | bytes 1179656 | tf_op jit(solution)/shard_map/ppermute | solution.py:312
  60.2 0.6 copy-start.5
  60.2 10.4 %collective-permute-start.4 = (bf16[768,256]{1,0:T(8,128)(2,1)S(1)}, bf16[768,256]{1,0:T(8,128)(2,1)}, u32[]{:S(2)}, u32[]{:S(2)}) collective-permute-start(bf16[768,256]{1,0:T(8,128)(2,1)S(1)} %get-tuple-element.33), channel_id=1, source_target_pairs={{0,4},{2,6},{4,0},{6,2},{1,5},{3,7},{5,1},{7,3},{8,12},{10,14},{12... | collective-permute-start | bytes 1179656 | tf_op jit(solution)/shard_map/ppermute | solution.py:312
  60.9 20.4 %collective-permute-start.3 = (bf16[768,256]{1,0:T(8,128)(2,1)S(1)}, bf16[768,256]{1,0:T(8,128)(2,1)}, u32[]{:S(2)}, u32[]{:S(2)}) collective-permute-start(bf16[768,256]{1,0:T(8,128)(2,1)S(1)} %get-tuple-element.32), channel_id=1, source_target_pairs={{0,2},{2,4},{4,6},{6,0},{1,3},{3,5},{5,7},{7,1},{8,10},{10,12},{12... | collective-permute-start | bytes 1179656 | tf_op jit(solution)/shard_map/ppermute | solution.py:312
  61.3 24.4 %copy-start.8 = (bf16[64,704]{1,0:T(8,128)(2,1)S(1)}, bf16[64,704]{1,0:T(8,128)(2,1)}, u32[]{:S(2)}) copy-start(bf16[64,704]{1,0:T(8,128)(2,1)} %param.23) | copy-start | bytes 270340
  61.3 27.2 %copy-start.6 = (bf16[64,704]{1,0:T(8,128)(2,1)S(1)}, bf16[64,704]{1,0:T(8,128)(2,1)}, u32[]{:S(2)}) copy-start(bf16[64,704]{1,0:T(8,128)(2,1)} %copy-done.5) | copy-start | bytes 270340
  67.8 17.9 %collective-permute-start.19 = (bf16[64,704]{1,0:T(8,128)(2,1)}, bf16[64,704]{1,0:T(8,128)(2,1)S(1)}, u32[]{:S(2)}, u32[]{:S(2)}) collective-permute-start(bf16[64,704]{1,0:T(8,128)(2,1)} %param.23), channel_id=1, source_target_pairs={{0,32},{32,64},{64,96},{96,128},{128,160},{160,192},{192,224},{224... | collective-permute-start | bytes 270344 | tf_op jit(solution)/shard_map/ppermute | solution.py:37
  70.6 17.8 %collective-permute-start.20 = (bf16[64,704]{1,0:T(8,128)(2,1)}, bf16[64,704]{1,0:T(8,128)(2,1)S(1)}, u32[]{:S(2)}, u32[]{:S(2)}) collective-permute-start(bf16[64,704]{1,0:T(8,128)(2,1)} %param.23), channel_id=1, source_target_pairs={{0,224},{32,0},{64,32},{96,64},{128,96},{160,128},{192,160},{224,1... | collective-permute-start | bytes 270344 | tf_op jit(solution)/shard_map/ppermute | solution.py:37
  81.3 7.3 %collective-permute-start.23 = (bf16[64,704]{1,0:T(8,128)(2,1)}, bf16[64,704]{1,0:T(8,128)(2,1)S(1)}, u32[]{:S(2)}, u32[]{:S(2)}) collective-permute-start(bf16[64,704]{1,0:T(8,128)(2,1)} %copy-done.5), channel_id=1, source_target_pairs={{0,32},{32,64},{64,96},{96,128},{128,160},{160,192},{192,224},{224... | collective-permute-start | bytes 270344 | tf_op jit(solution)/shard_map/ppermute | solution.py:37
  85.4 4.8 %collective-permute-start.24 = (bf16[64,704]{1,0:T(8,128)(2,1)S(1)}, bf16[64,704]{1,0:T(8,128)(2,1)S(1)}, u32[]{:S(2)}, u32[]{:S(2)}) collective-permute-start(bf16[64,704]{1,0:T(8,128)(2,1)S(1)} %collective-permute-done.22), channel_id=1, source_target_pairs={{0,224},{32,0},{64,32},{96,64},{128,96},{160,128},{192,160},{224,1... | collective-permute-start | bytes 270344 | tf_op jit(solution)/shard_map/ppermute | solution.py:37
  85.5 6.0 %collective-permute-start.25 = (bf16[64,704]{1,0:T(8,128)(2,1)S(1)}, bf16[64,704]{1,0:T(8,128)(2,1)S(1)}, u32[]{:S(2)}, u32[]{:S(2)}) collective-permute-start(bf16[64,704]{1,0:T(8,128)(2,1)S(1)} %broadcast_select_fusion.2), channel_id=1, source_target_pairs={{0,64},{1,193},{2,66},{3,195},{4,68},{5,197},{6,70},{7,199},{8,72}... | collective-permute-start | bytes 270344 | tf_op jit(solution)/shard_map/ppermute | solution.py:33
  85.7 29.2 %collective-permute-start.17 = (bf16[256,1408]{1,0:T(8,128)(2,1)S(1)}, bf16[256,1408]{1,0:T(8,128)(2,1)S(1)}, u32[]{:S(2)}, u32[]{:S(2)}) collective-permute-start(bf16[256,1408]{1,0:T(8,128)(2,1)S(1)} %collective-permute-done.13), channel_id=1, source_target_pairs={{0,32},{32,64},{64,96},{96,128},{128,160},{160,192},{192,224},{224... | collective-permute-start | bytes 2162696 | tf_op jit(solution)/shard_map/ppermute | solution.py:37
  88.4 19.1 %collective-permute-start.6 = (bf16[768,256]{1,0:T(8,128)(2,1)S(1)}, bf16[768,256]{1,0:T(8,128)(2,1)S(1)}, u32[]{:S(2)}, u32[]{:S(2)}) collective-permute-start(bf16[768,256]{1,0:T(8,128)(2,1)S(1)} %add_convert_fusion.2.p0), channel_id=1, source_target_pairs={{0,2},{2,4},{4,6},{6,0},{1,3},{3,5},{5,7},{7,1},{8,10},{10,12},{12... | collective-permute-start | bytes 1179656 | tf_op jit(solution)/shard_map/ppermute | solution.py:312
  88.6 18.9 %collective-permute-start.7 = (bf16[768,256]{1,0:T(8,128)(2,1)S(1)}, bf16[768,256]{1,0:T(8,128)(2,1)S(1)}, u32[]{:S(2)}, u32[]{:S(2)}) collective-permute-start(bf16[768,256]{1,0:T(8,128)(2,1)S(1)} %add_convert_fusion.2.p0), channel_id=1, source_target_pairs={{0,4},{2,6},{4,0},{6,2},{1,5},{3,7},{5,1},{7,3},{8,12},{10,14},{12... | collective-permute-start | bytes 1179656 | tf_op jit(solution)/shard_map/ppermute | solution.py:312
  90.2 18.7 %collective-permute-start.8 = (bf16[768,256]{1,0:T(8,128)(2,1)S(1)}, bf16[768,256]{1,0:T(8,128)(2,1)S(1)}, u32[]{:S(2)}, u32[]{:S(2)}) collective-permute-start(bf16[768,256]{1,0:T(8,128)(2,1)S(1)} %add_convert_fusion.2.p0), channel_id=1, source_target_pairs={{0,6},{2,0},{4,2},{6,4},{1,7},{3,1},{5,3},{7,5},{8,14},{10,8},{12,... | collective-permute-start | bytes 1179656 | tf_op jit(solution)/shard_map/ppermute | solution.py:312
  91.5 23.4 %collective-permute-start.18 = (bf16[256,1408]{1,0:T(8,128)(2,1)}, bf16[256,1408]{1,0:T(8,128)(2,1)S(1)}, u32[]{:S(2)}, u32[]{:S(2)}) collective-permute-start(bf16[256,1408]{1,0:T(8,128)(2,1)} %collective-permute-done.15), channel_id=1, source_target_pairs={{0,224},{32,0},{64,32},{96,64},{128,96},{160,128},{192,160},{224,1... | collective-permute-start | bytes 2162696 | tf_op jit(solution)/shard_map/ppermute | solution.py:37
  107.5 16.9 %collective-permute-start.26 = (bf16[8,64,704]{2,1,0:T(8,128)(2,1)S(1)}, bf16[8,64,704]{2,1,0:T(8,128)(2,1)S(1)}, u32[]{:S(2)}, u32[]{:S(2)}) collective-permute-start(bf16[8,64,704]{2,1,0:T(8,128)(2,1)S(1)} %bitcast_dynamic-update-slice_fusion.16), channel_id=1, source_target_pairs={{0,8},{8,16},{16,24},{24,0},{1,9},{9,17},{17,25},{25,1},{2,10},{10... | collective-permute-start | bytes 2162696 | tf_op jit(solution)/shard_map/ppermute | solution.py:41
  107.5 18.1 %collective-permute-start.27 = (bf16[8,64,704]{2,1,0:T(8,128)(2,1)S(1)}, bf16[8,64,704]{2,1,0:T(8,128)(2,1)S(1)}, u32[]{:S(2)}, u32[]{:S(2)}) collective-permute-start(bf16[8,64,704]{2,1,0:T(8,128)(2,1)S(1)} %bitcast_dynamic-update-slice_fusion.16), channel_id=1, source_target_pairs={{0,24},{8,0},{16,8},{24,16},{1,25},{9,1},{17,9},{25,17},{2,26},{10... | collective-permute-start | bytes 2162696 | tf_op jit(solution)/shard_map/ppermute | solution.py:41
  109.1 6.2 %collective-permute-start.16 = (bf16[4,768,256]{2,1,0:T(8,128)(2,1)S(1)}, bf16[4,768,256]{2,1,0:T(8,128)(2,1)S(1)}, u32[]{:S(2)}, u32[]{:S(2)}) collective-permute-start(bf16[4,768,256]{2,1,0:T(8,128)(2,1)S(1)} %pad_maximum_fusion), channel_id=1, source_target_pairs={{0,1},{1,0},{2,3},{3,2},{4,5},{5,4},{6,7},{7,6},{8,9},{9,8},{10,11... | collective-permute-start | bytes 4718600 | tf_op jit(solution)/shard_map/ppermute | solution.py:45
  112.4 3.0 %copy-start.2 = (f32[2048]{0:T(1024)S(1)}, f32[2048]{0:T(1024)}, u32[]{:S(2)}) copy-start(f32[2048]{0:T(1024)} %param.19) | copy-start | bytes 24580
  115.0 11.9 %collective-permute-start.28 = (bf16[256,1408]{1,0:T(8,128)(2,1)S(1)}, bf16[256,1408]{1,0:T(8,128)(2,1)S(1)}, u32[]{:S(2)}, u32[]{:S(2)}) collective-permute-start(bf16[256,1408]{1,0:T(8,128)(2,1)S(1)} %broadcast_select_fusion.1), channel_id=1, source_target_pairs={{0,32},{1,225},{2,34},{3,227},{4,36},{5,229},{6,38},{7,231},{8,40}... | collective-permute-start | bytes 2162696 | tf_op jit(solution)/shard_map/ppermute | solution.py:33
  125.8 22.4 %collective-permute-start.31 = (bf16[8,64,704]{2,1,0:T(8,128)(2,1)S(1)}, bf16[8,64,704]{2,1,0:T(8,128)(2,1)S(1)}, u32[]{:S(2)}, u32[]{:S(2)}) collective-permute-start(bf16[8,64,704]{2,1,0:T(8,128)(2,1)S(1)} %broadcast_select_fusion), channel_id=1, source_target_pairs={{0,8},{1,25},{2,10},{3,27},{4,12},{5,29},{6,14},{7,31},{8,16},{9,1... | collective-permute-start | bytes 2162696 | tf_op jit(solution)/shard_map/ppermute | solution.py:33
  130.1 12.6 %collective-permute-start.29 = (bf16[1,704]{1,0:T(2,128)(2,1)S(1)}, bf16[1,704]{1,0:T(2,128)(2,1)S(1)}, u32[]{:S(2)}, u32[]{:S(2)}) collective-permute-start(bf16[1,704]{1,0:T(2,128)(2,1)S(1)} %get-tuple-element.65), channel_id=1, source_target_pairs={{0,8},{8,16},{16,24},{24,32},{32,40},{40,48},{48,56},{56,64},{64,7... | collective-permute-start | bytes 4232 | tf_op jit(solution)/shard_map/ppermute | solution.py:430
  137.7 7.7 %copy-start.3 = (bf16[3,704]{1,0:T(4,128)(2,1)S(1)}, bf16[3,704]{1,0:T(4,128)(2,1)}, u32[]{:S(2)}) copy-start(bf16[3,704]{1,0:T(4,128)(2,1)} %taps_ref.1) | copy-start | bytes 12676
  137.7 7.7 %collective-permute-start.30 = (bf16[1,704]{1,0:T(2,128)(2,1)S(1)}, bf16[1,704]{1,0:T(2,128)(2,1)S(1)}, u32[]{:S(2)}, u32[]{:S(2)}) collective-permute-start(bf16[1,704]{1,0:T(2,128)(2,1)S(1)} %get-tuple-element.64), channel_id=1, source_target_pairs={{8,0},{16,8},{24,16},{32,24},{40,32},{48,40},{56,48},{64,56},{72,6... | collective-permute-start | bytes 4232 | tf_op jit(solution)/shard_map/ppermute | solution.py:431
  150.0 4.5 %collective-permute-start.32 = (bf16[768,1024]{1,0:T(8,128)(2,1)S(1)}, bf16[768,1024]{1,0:T(8,128)(2,1)S(1)}, u32[]{:S(2)}, u32[]{:S(2)}) collective-permute-start(bf16[768,1024]{1,0:T(8,128)(2,1)S(1)} %convolution_convert_fusion), channel_id=1, source_target_pairs={{0,1},{1,0},{2,3},{3,2},{4,5},{5,4},{6,7},{7,6},{8,9},{9,8},{10,11... | collective-permute-start | bytes 4718600 | tf_op jit(solution)/shard_map/ppermute | solution.py:45
  155.3 10.4 %collective-permute-start.35 = (bf16[768,256]{1,0:T(8,128)(2,1)S(1)}, bf16[768,256]{1,0:T(8,128)(2,1)S(1)}, u32[]{:S(2)}, u32[]{:S(2)}) collective-permute-start(bf16[768,256]{1,0:T(8,128)(2,1)S(1)} %get-tuple-element.62), channel_id=1, source_target_pairs={{0,6},{2,0},{4,2},{6,4},{1,7},{3,1},{5,3},{7,5},{8,14},{10,8},{12,... | collective-permute-start | bytes 1179656 | tf_op jit(solution)/shard_map/ppermute | solution.py:312
  155.4 11.9 %collective-permute-start.34 = (bf16[768,256]{1,0:T(8,128)(2,1)S(1)}, bf16[768,256]{1,0:T(8,128)(2,1)S(1)}, u32[]{:S(2)}, u32[]{:S(2)}) collective-permute-start(bf16[768,256]{1,0:T(8,128)(2,1)S(1)} %get-tuple-element.63), channel_id=1, source_target_pairs={{0,4},{2,6},{4,0},{6,2},{1,5},{3,7},{5,1},{7,3},{8,12},{10,14},{12... | collective-permute-start | bytes 1179656 | tf_op jit(solution)/shard_map/ppermute | solution.py:312
  155.5 21.0 %collective-permute-start.33 = (bf16[768,256]{1,0:T(8,128)(2,1)S(1)}, bf16[768,256]{1,0:T(8,128)(2,1)S(1)}, u32[]{:S(2)}, u32[]{:S(2)}) collective-permute-start(bf16[768,256]{1,0:T(8,128)(2,1)S(1)} %get-tuple-element.61), channel_id=1, source_target_pairs={{0,2},{2,4},{4,6},{6,0},{1,3},{3,5},{5,7},{7,1},{8,10},{10,12},{12... | collective-permute-start | bytes 1179656 | tf_op jit(solution)/shard_map/ppermute | solution.py:312
